TPU v7x, 256 devices: a whole 4x4x8 slice. The times are simulated.
256 devices in a mesh: ep: 64 (over z, y, core), tp: 4 (over x).
Axes of the slice: x: 4, y: 4, z: 8, core: 2. Of those that a mesh axis runs over, the one named last changes fastest.
Arguments:
- queries: bfloat16 [32768, 1536], P('ep', 'tp'), may hold values from -6 to 6
- keys: bfloat16 [32768, 1536], P('ep', 'tp'), may hold values from -6 to 6
- values: bfloat16 [32768, 1536], P('ep', 'tp'), may hold values from -6 to 6
- decay_gate_logits: float32 [32768, 12], P('ep', 'tp'), may hold values from -6 to 6
- correction_logits: bfloat16 [32768, 12], P('ep', 'tp'), may hold values from -6 to 6
- head_decay_speed: float32 [12], P('tp'), may hold values from 0 to 1
- position_log_decay: float32 [32768, 12], P('ep', 'tp'), may hold values from -1 to 0
- head_output_gain: float32 [128], replicated, may hold values from 0.1 to 1.9
- mixer_output_weight: bfloat16 [1536, 2048], P('tp'), may hold values from -0.15625 to 0.15625
- expert_input_tokens: bfloat16 [32768, 2048], P(('ep', 'tp')), may hold values from -6 to 6
- expert_norm_gain: float32 [2048], replicated, may hold values from 0.1 to 1.9
- routes: int32 [32768, 2], P(('ep', 'tp')), may hold values from 0 to 63, all different within a row; in each aligned block of 128 rows (0 to 127, 128 to 255, ...) at most 6 rows name the same one
- chosen_expert_weight: float32 [32768, 2], P(('ep', 'tp')), may hold values from 0.25 to 2.5
- routed_gate_weight: bfloat16 [64, 2048, 1024], P('ep', None, 'tp'), may hold values from -0.125 to 0.125
- routed_up_weight: bfloat16 [64, 2048, 1024], P('ep', None, 'tp'), may hold values from -0.125 to 0.125
- routed_down_weight: bfloat16 [64, 1024, 2048], P('ep', 'tp'), may hold values from -0.1875 to 0.1875
- common_gate_weight: bfloat16 [2048, 1024], P(None, 'tp'), may hold values from -0.125 to 0.125
- common_up_weight: bfloat16 [2048, 1024], P(None, 'tp'), may hold values from -0.125 to 0.125
- common_down_weight: bfloat16 [1024, 2048], P('tp'), may hold values from -0.1875 to 0.1875
Outputs:
- mixer_out: bfloat16 [32768, 2048], P(('ep', 'tp'))
- moe_out: bfloat16 [32768, 2048], P(('ep', 'tp'))
Inputs may be any that keep to these rules, and one draw needn't show every extreme that they name: `routes`: each row names 2 different experts; the rows of one device name no expert more than 6 times, and some device names some expert exactly 6 times.
All inputs are finite; a program needn't handle non-finite values.
Results may differ from a plain program's by a relative error of at most 0.017.
Values may be sent and summed in bfloat16 or wider, within the bound.
A program may use at most 128 MiB of HBM per device.

v0:
```python
import functools

import jax
import jax.numpy as jnp
from jax import lax
from jax.experimental import pallas as pl
from jax.experimental.pallas import tpu as pltpu
from jax.sharding import Mesh
from jax.sharding import PartitionSpec as P


EP = ("ep_0", "ep_1", "ep_2")
EP_TP = ("ep_0", "ep_1", "ep_2", "tp")


EPS = 1e-06
F32 = jnp.float32
BF16 = jnp.bfloat16
LANES = 128
MESH = pl.DeviceIdType.MESH


def halves(x):
    hi = x.astype(BF16)
    return hi, (x - hi.astype(F32)).astype(BF16)


def thirds(x):
    hi = x.astype(BF16)
    rest = x - hi.astype(F32)
    mid = rest.astype(BF16)
    return hi, mid, (rest - mid.astype(F32)).astype(BF16)


def mm(a, b):
    return jnp.dot(a, b, preferred_element_type=F32)


def dot3(a, b):
    ah, al = halves(a)
    bh, bl = halves(b)
    return mm(jnp.concatenate([ah, ah, al], 1), jnp.concatenate([bh, bl, bh], 0))


def dot2(a, b):
    ah, al = halves(a)
    return mm(jnp.concatenate([ah, al], 1), jnp.concatenate([b, b], 0))


def unit_lower_inverse(low, row, col):
    eye = (row == col).astype(F32)
    base = jnp.where((row >> 3) == (col >> 3), low, 0.0)
    squared = dot3(base, base)
    fourth = dot3(squared, squared)
    inv = eye - base
    inv = inv + dot3(inv, squared)
    inv = inv + dot3(inv, fourth)
    for bit in (3, 4, 5):
        across = jnp.where(
            ((row >> (bit + 1)) == (col >> (bit + 1))) & ((row >> bit) != (col >> bit)), low, 0.0
        )
        inv = inv - dot3(inv, dot3(across, inv))
    return inv


def local_mixer_kernel(
    q_ref, k_ref, v_ref, gate_ref, corr_ref, speed_ref, plog_ref, qt_ref, ol_ref, tr_ref, in_ref
):
    head = pl.program_id(0)
    heads, rows = gate_ref.shape
    pair = 128
    here = lax.broadcasted_iota(jnp.int32, (heads, rows), 0) == head

    log_gate = (
        -speed_ref[...]
        * (jnp.maximum(gate_ref[...], 0.0) + jnp.log1p(jnp.exp(-jnp.abs(gate_ref[...]))))
        + plog_ref[...]
    )
    beta_all = 1.0 / (1.0 + jnp.exp(-corr_ref[...].astype(F32)))
    g_row = jnp.sum(jnp.where(here, log_gate, 0.0), axis=0, keepdims=True)
    beta_row_all = jnp.sum(jnp.where(here, beta_all, 0.0), axis=0, keepdims=True)

    row = lax.broadcasted_iota(jnp.int32, (pair, pair), 0)
    col = lax.broadcasted_iota(jnp.int32, (pair, pair), 1)
    same = (row >> 6) == (col >> 6)
    causal = same & (row >= col)
    strict = same & (row > col)
    first = col < 64
    ones = (same & (row <= col)).astype(BF16)
    ones = jnp.concatenate([ones, ones, ones], 0)

    packs = []
    for p in range(rows // pair):
        at = pl.ds(p * pair, pair)
        qb, kb, vb = q_ref[at, :], k_ref[at, :], v_ref[at, :]
        qf, kf = qb.astype(F32), kb.astype(F32)
        rq = lax.rsqrt(jnp.sum(qf * qf, axis=1, keepdims=True) + EPS) * (pair**-0.5)
        rk = lax.rsqrt(jnp.sum(kf * kf, axis=1, keepdims=True) + EPS)
        g_mat = jnp.broadcast_to(g_row[:, p * pair : (p + 1) * pair], (pair, pair))
        c_row = mm(jnp.concatenate(thirds(g_mat), 1), ones)
        c_mat = c_row.T
        last0, last1 = c_mat[63:64, :], c_mat[127:128, :]
        rk_row = jnp.broadcast_to(rk, (pair, pair)).T
        beta_row = jnp.broadcast_to(beta_row_all[:, p * pair : (p + 1) * pair], (pair, pair))
        beta = beta_row.T
        gram = lax.dot_general(
            jnp.concatenate([kb, qb], 0), kb, (((1,), (1,)), ((), ())), preferred_element_type=F32
        )
        decay = jnp.exp(jnp.where(causal, c_mat - c_row, -jnp.inf)) * rk_row
        low = jnp.where(strict, gram[:pair] * decay * (beta * rk), 0.0)
        scores = gram[pair:] * decay * rq
        inv = unit_lower_inverse(low, row, col)
        scale = beta_row * inv
        uw = jnp.concatenate(
            [dot2(scale, vb), dot2(scale * (jnp.exp(c_row) * rk_row), kb)], 1
        )
        suw = dot3(scores, uw)
        pq = qf * (rq * jnp.exp(c_mat)) - suw[:, pair:]
        tail = jnp.exp(jnp.where(first, last0, last1) - c_row)
        kt = kf.T * (tail * rk_row)
        kk = jnp.concatenate([jnp.where(first, kt, 0.0), jnp.where(first, 0.0, kt)], 0)
        mw = dot3(kk, uw)
        packs.append((suw[:, :pair], pq, mw, jnp.exp(last0), jnp.exp(last1)))

    ab = jnp.concatenate([(row == col).astype(F32), jnp.zeros((pair, pair), F32)], 1)
    for p, (su, pq, mw, keep0, keep1) in enumerate(packs):
        for b, keep in enumerate((keep0, keep1)):
            blk = slice(b * 64, (b + 1) * 64)
            at = pl.ds(p * pair + b * 64, 64)
            part = mw[b * pair : (b + 1) * pair]
            got = dot3(jnp.concatenate([pq[blk], part[:, pair:]], 0), ab)
            qt_ref[0, at, :] = got[:64, :pair]
            ol_ref[0, at, :] = got[:64, pair:] + su[blk]
            keep2 = jnp.concatenate([keep, keep], 1)
            ab = (
                keep2 * ab
                - got[64:]
                + jnp.concatenate([jnp.zeros((pair, pair), F32), part[:, :pair]], 1)
            )
    tr_ref[0] = ab[:, :pair]
    in_ref[0] = ab[:, pair:]


def local_mixer(queries, keys, values, gate, corr, speed, plog):
    rows, width = queries.shape
    heads = gate.shape[0]
    d = width // heads
    by_head = pl.BlockSpec((rows, d), lambda h: (0, h))
    whole = pl.BlockSpec((heads, rows), lambda h: (0, 0))
    return pl.pallas_call(
        local_mixer_kernel,
        grid=(heads,),
        in_specs=[
            by_head,
            by_head,
            by_head,
            whole,
            whole,
            pl.BlockSpec((heads, 1), lambda h: (0, 0)),
            whole,
        ],
        out_specs=[
            pl.BlockSpec((1, rows, d), lambda h: (h, 0, 0)),
            pl.BlockSpec((1, rows, d), lambda h: (h, 0, 0)),
            pl.BlockSpec((1, d, d), lambda h: (h, 0, 0)),
            pl.BlockSpec((1, d, d), lambda h: (h, 0, 0)),
        ],
        out_shape=[
            jax.ShapeDtypeStruct((heads, rows, d), F32),
            jax.ShapeDtypeStruct((heads, rows, d), F32),
            jax.ShapeDtypeStruct((heads, d, d), F32),
            jax.ShapeDtypeStruct((heads, d, d), F32),
        ],
        cost_estimate=pl.CostEstimate(flops=30_000_000_000, bytes_accessed=4_000_000, transcendentals=0),
        name="local_mixer",
    )(queries, keys, values, gate, corr, speed.reshape(heads, 1), plog)


def entry_state_kernel(
    t_ref, i_ref, xn_ref, s_ref, group_ref, send_x, recv_x, keep_x, own, peer, ypack, zpack,
    send_c, recv_c, send_y, recv_y, send_yc, recv_yc,
    send_r, recv_r, send_l, recv_l, send_rc, recv_rc, send_lc, recv_lc,
):
    heads, d, _ = t_ref.shape
    half = d // 2
    nz, ny = zpack.shape[0], ypack.shape[0]
    z, y, c = lax.axis_index("ep_0"), lax.axis_index("ep_1"), lax.axis_index("ep_2")
    other = {"ep_2": 1 - c}
    right, left = {"ep_0": lax.rem(z + 1, nz)}, {"ep_0": lax.rem(z + nz - 1, nz)}
    across = [{"ep_1": lax.rem(y + k, ny)} for k in range(1, ny)]
    members, me = group_ref.shape[0], lax.axis_index("tp")
    fellows = [{"tp": lax.rem(me + k, members)} for k in range(1, members)]

    barrier = pltpu.get_barrier_semaphore()
    for who in (other, right, left, *across, *fellows):
        pl.semaphore_signal(barrier, inc=1, device_id=who, device_id_type=MESH)
    pl.semaphore_wait(barrier, 3 + len(across) + len(fellows))

    def send(src, dst, send_sem, recv_sem, who):
        return pltpu.make_async_remote_copy(
            src_ref=src, dst_ref=dst, send_sem=send_sem, recv_sem=recv_sem,
            device_id=who, device_id_type=MESH,
        )

    def store(ref, h, both):
        both = both.astype(BF16)
        ref[0, h] = both[:half]
        ref[1, h] = both[half:]

    def load(ref, h):
        return jnp.concatenate([ref[0, h], ref[1, h]], 0)

    def after(pack, so_far):
        hi, lo = halves(so_far)
        t = pack[:, :d]
        return mm(jnp.concatenate([t, t], 1), jnp.concatenate([hi, lo], 0))

    def added(pack):
        return pack[:, d:].astype(F32)

    tokens = [
        send(xn_ref, group_ref.at[me], send_x.at[k], recv_x.at[k], who)
        for k, who in enumerate(fellows)
    ]
    kept = pltpu.make_async_copy(xn_ref, group_ref.at[me], keep_x)

    nothing = jnp.zeros((d, d), F32)
    for h in range(heads):
        store(own, h, jnp.concatenate([t_ref[h], i_ref[h]], 1))
    swap = send(own, peer, send_c, recv_c, other)
    swap.start()
    for copy in tokens:
        copy.start()
    kept.start()
    swap.wait()
    for h in range(heads):
        mine, theirs = load(own, h), load(peer, h)
        early = jnp.where(c == 0, mine.astype(F32), theirs.astype(F32)).astype(BF16)
        late = jnp.where(c == 0, theirs.astype(F32), mine.astype(F32)).astype(BF16)
        both = mm(late[:, :d], early) + jnp.concatenate([nothing, added(late)], 1)
        store(ypack.at[y], h, both)

    out = [
        send(ypack.at[y, c], ypack.at[y, c], send_y.at[k - 1], recv_y.at[k - 1], across[k - 1])
        for k in range(1, ny)
    ]
    for copy in out:
        copy.start()
    over = []
    for k in range(1, ny):
        slot = ypack.at[lax.rem(y + ny - k, ny), c]
        out[k - 1].wait_recv()
        over.append(send(slot, slot, send_yc.at[k - 1], recv_yc.at[k - 1], other))
        over[-1].start()
    for copy in out:
        copy.wait_send()
    for copy in over:
        copy.wait()
    for h in range(heads):
        both = load(ypack.at[0], h).astype(F32)
        for k in range(1, ny):
            pack = load(ypack.at[k], h)
            both = after(pack, both) + jnp.concatenate([nothing, added(pack)], 1)
        store(zpack.at[z], h, both)

    def going(r, h, sign, who, send_sem, recv_sem):
        slot = zpack.at[lax.rem(z + nz - sign * (r - 1), nz), c, h]
        return send(slot, slot, send_sem.at[r - 1, h], recv_sem.at[r - 1, h], who)

    def shared_with_other(r, h, sign, send_sem, recv_sem):
        slot = zpack.at[lax.rem(z + nz - sign * r, nz), c, h]
        return send(slot, slot, send_sem.at[r - 1, h], recv_sem.at[r - 1, h], other)

    rings = (
        (nz // 2, 1, right, send_r, recv_r, send_rc, recv_rc),
        ((nz - 1) // 2, -1, left, send_l, recv_l, send_lc, recv_lc),
    )
    pending = []
    for rounds, sign, who, ss, rs, _, _ in rings:
        for h in range(heads):
            if rounds > 0:
                going(1, h, sign, who, ss, rs).start()
    for r in range(1, nz // 2 + 1):
        for h in range(heads):
            for rounds, sign, who, ss, rs, sc, rc in rings:
                if r > rounds:
                    continue
                copy = going(r, h, sign, who, ss, rs)
                copy.wait_recv()
                pending.append((copy, False))
                if r < rounds:
                    going(r + 1, h, sign, who, ss, rs).start()
                hand = shared_with_other(r, h, sign, sc, rc)
                hand.start()
                pending.append((hand, True))
    for copy, both_ways in pending:
        copy.wait_send()
        if both_ways:
            copy.wait_recv()

    for h in range(heads):
        s_ref[h] = nothing
    for k in range(nz - 1):
        for h in range(heads):
            pack = load(zpack.at[k], h)
            s_ref[h] = jnp.where(k < z, after(pack, s_ref[h]) + added(pack), s_ref[h])
    for k in range(ny - 1):
        for h in range(heads):
            pack = load(ypack.at[k], h)
            s_ref[h] = jnp.where(k < y, after(pack, s_ref[h]) + added(pack), s_ref[h])
    for h in range(heads):
        pack = load(peer, h)
        s_ref[h] = jnp.where(c == 1, after(pack, s_ref[h]) + added(pack), s_ref[h])
    kept.wait()
    for copy in tokens:
        copy.wait()


def entry_state(trans, inject, xn):
    heads, d, _ = trans.shape
    nz, ny = lax.axis_size("ep_0"), lax.axis_size("ep_1")
    half = (2, heads, d // 2, 2 * d)
    dma = pltpu.SemaphoreType.DMA
    rounds = max(nz // 2, 1)
    members = lax.axis_size("tp")
    vmem = pl.BlockSpec(memory_space=pltpu.VMEM)
    return pl.pallas_call(
        entry_state_kernel,
        in_specs=[vmem, vmem, pl.BlockSpec(memory_space=pl.ANY)],
        out_specs=[vmem, pl.BlockSpec(memory_space=pl.ANY)],
        out_shape=[
            jax.ShapeDtypeStruct((heads, d, d), F32),
            jax.ShapeDtypeStruct((members, *xn.shape), BF16),
        ],
        scratch_shapes=[
            dma((max(members - 1, 1),)), dma((max(members - 1, 1),)), dma,
            pltpu.VMEM(half, BF16),
            pltpu.VMEM(half, BF16),
            pltpu.VMEM((ny, *half), BF16),
            pltpu.VMEM((nz, *half), BF16),
            dma, dma,
            dma((max(ny - 1, 1),)), dma((max(ny - 1, 1),)), dma((max(ny - 1, 1),)), dma((max(ny - 1, 1),)),
            *[dma((rounds, heads)) for _ in range(8)],
        ],
        compiler_params=pltpu.CompilerParams(collective_id=0, has_side_effects=True),
        cost_estimate=pl.CostEstimate(flops=30_000_000_000, bytes_accessed=4_000_000, transcendentals=0),
        name="entry_state",
    )(trans, inject, xn)


def parts_kernel(
    me_ref, qt_ref, ol_ref, state_ref, gain_ref, w_ref, x_ref, gate_ref, up_ref, down_ref, *out_refs
):
    heads, tile, _ = qt_ref.shape
    normed = []
    for h in range(heads):
        out = dot3(qt_ref[h], state_ref[h]) + ol_ref[h]
        out = out * lax.rsqrt(jnp.mean(out * out, axis=1, keepdims=True) + EPS) * gain_ref[...]
        normed.append(out.astype(BF16))
    mixer = mm(jnp.concatenate(normed, 1), w_ref[...]).astype(BF16)
    x = x_ref[0]
    hidden = gated(mm(x, gate_ref[...]), mm(x, up_ref[...]))
    shared = mm(hidden, down_ref[...]).astype(BF16)
    for r, out_ref in enumerate(out_refs):

        @pl.when(pl.program_id(0) == r)
        def _():
            out_ref[:tile] = mixer
            out_ref[tile:] = shared


def parts_for_peers(me, peers, qt, ol, state, gain, w, group, gate, up, down):
    heads, rows, d = qt.shape
    width = w.shape[1]
    tile = rows // peers

    def whole(x):
        return pl.BlockSpec(x.shape, lambda r, me: (0,) * x.ndim)

    def turn(r, me):
        return lax.rem(me[0] + r, peers)

    gain = gain.reshape(1, d)
    return pl.pallas_call(
        parts_kernel,
        grid_spec=pltpu.PrefetchScalarGridSpec(
            num_scalar_prefetch=1,
            grid=(peers,),
            in_specs=[
                pl.BlockSpec((heads, tile, d), lambda r, me: (0, turn(r, me), 0)),
                pl.BlockSpec((heads, tile, d), lambda r, me: (0, turn(r, me), 0)),
                whole(state),
                whole(gain),
                whole(w),
                pl.BlockSpec((1, tile, group.shape[2]), lambda r, me: (turn(r, me), 0, 0)),
                whole(gate),
                whole(up),
                whole(down),
            ],
            out_specs=[pl.BlockSpec((2 * tile, width), lambda r, me: (0, 0))] * peers,
        ),
        out_shape=[jax.ShapeDtypeStruct((2 * tile, width), BF16)] * peers,
        cost_estimate=pl.CostEstimate(flops=6_000_000_000, bytes_accessed=12_000_000, transcendentals=0),
        name="parts_for_peers",
    )(me, qt, ol, state, gain, w, group, gate, up, down)


def near_experts_kernel(in_ref, *refs):
    shards_ = len(refs) // 3 - 2
    hbm, (x_ref, out_ref, wide, gates, ups, downs) = refs[: 3 * shards_], refs[3 * shards_ : -1]
    sems = refs[-1]
    rows, width = x_ref.shape
    cuts = width // LANES
    tile = 128
    copies = [
        [
            pltpu.make_async_copy(hbm[3 * m + k], held.at[m], sems.at[m, k])
            for k, held in enumerate((gates, ups, downs))
        ]
        for m in range(shards_)
    ]
    for shard in copies:
        for copy in shard:
            copy.start()
    for t in range(rows // tile):
        wide[...] = in_ref[t * tile * cuts : (t + 1) * tile * cuts, :].astype(F32)
        x_ref[t * tile : (t + 1) * tile, :] = gathered(wide, tile, cuts)
    for m in range(shards_):
        for copy in copies[m]:
            copy.wait()

        def one(t, carry):
            at = pl.ds(pl.multiple_of(t * tile, tile), tile)
            x = x_ref[at, :]
            part = mm(gated(mm(x, gates[m]), mm(x, ups[m])), downs[m])
            out_ref[at, :] = part if m == 0 else out_ref[at, :] + part
            return carry

        lax.fori_loop(0, rows // tile, one, 0)


def near_experts(spread_in, shards_):
    weights = [w for shard in shards_ for w in shard]
    width, hidden = shards_[0][0].shape
    rows = spread_in.shape[0] * LANES // width
    count = len(shards_)
    vmem = pl.BlockSpec(memory_space=pltpu.VMEM)
    return pl.pallas_call(
        near_experts_kernel,
        in_specs=[vmem] + [pl.BlockSpec(memory_space=pl.ANY)] * len(weights),
        out_specs=[vmem, vmem],
        out_shape=[
            jax.ShapeDtypeStruct((rows, width), BF16),
            jax.ShapeDtypeStruct((rows, width), F32),
        ],
        scratch_shapes=[
            pltpu.VMEM((128 * width // LANES, LANES), F32),
            pltpu.VMEM((count, width, hidden), BF16),
            pltpu.VMEM((count, width, hidden), BF16),
            pltpu.VMEM((count, hidden, width), BF16),
            pltpu.SemaphoreType.DMA((count, 3)),
        ],
        cost_estimate=pl.CostEstimate(flops=5_000_000_000, bytes_accessed=16_000_000, transcendentals=0),
        name="near_experts",
    )(spread_in, *weights)


def far_expert_kernel(x_ref, near_ref, *refs):
    hbm, (out_ref, wide, near, gate, up, down, sems) = (near_ref, *refs[:4]), refs[4:]
    half = up.shape[0] // 2
    rows, width = x_ref.shape
    cuts = width // LANES
    tile = 128
    spots = (near, gate, up.at[:half], up.at[half:], down)
    copies = [
        pltpu.make_async_copy(src, dst, sems.at[k]) for k, (src, dst) in enumerate(zip(hbm, spots))
    ]
    for k in (1, 2, 3, 4, 0):
        copies[k].start()
    for k in (1, 2, 3, 4, 0):
        copies[k].wait()

    def one(t, carry):
        at = pl.ds(pl.multiple_of(t * tile, tile), tile)
        x = x_ref[at, :]
        total = near[at, :] + mm(gated(mm(x, gate[...]), mm(x, up[...])), down[...])
        spread(wide, tile, 0, total)
        spot = pl.ds(pl.multiple_of(t * (tile * cuts), tile * cuts), tile * cuts)
        out_ref[spot, :] = wide[...].astype(BF16)
        return carry

    lax.fori_loop(0, rows // tile, one, 0)


def far_expert(x, near, gate, up0, up1, down):
    rows, width = x.shape
    hidden = gate.shape[1]
    cuts = width // LANES
    vmem = pl.BlockSpec(memory_space=pltpu.VMEM)
    return pl.pallas_call(
        far_expert_kernel,
        in_specs=[vmem] + [pl.BlockSpec(memory_space=pl.ANY)] * 5,
        out_specs=vmem,
        out_shape=jax.ShapeDtypeStruct((rows * cuts, LANES), BF16),
        scratch_shapes=[
            pltpu.VMEM((128 * cuts, LANES), F32),
            pltpu.VMEM((rows, width), F32),
            pltpu.VMEM((width, hidden), BF16),
            pltpu.VMEM((width, hidden), BF16),
            pltpu.VMEM((hidden, width), BF16),
            pltpu.SemaphoreType.DMA((5,)),
        ],
        cost_estimate=pl.CostEstimate(flops=2_000_000_000, bytes_accessed=12_000_000, transcendentals=0),
        name="far_expert",
    )(x, near, gate, up0, up1, down)


def spread(wide, rows, start, values):
    cuts = values.shape[1] // LANES
    for c in range(cuts):
        wide[pl.ds(start * cuts + c, rows, stride=cuts), :] = values[:, c * LANES : (c + 1) * LANES]


def gathered(wide, rows, cuts):
    return jnp.concatenate(
        [wide[pl.ds(c, rows, stride=cuts), :].astype(BF16) for c in range(cuts)], 1
    )


def dispatch_kernel(capacity, x_ref, gain_ref, routes_ref, weight_ref, xn_ref, out_ref, mix_ref, wide):
    tokens, width = x_ref.shape
    slots = mix_ref.shape[1]
    x = x_ref[...].astype(F32)
    xn = (x * lax.rsqrt(jnp.mean(x * x, axis=1, keepdims=True) + EPS) * gain_ref[...]).astype(BF16)
    xn_ref[...] = xn
    expert = lax.broadcasted_iota(jnp.int32, (LANES, tokens), 0)
    first, second = expert == routes_ref[0:1, :], expert == routes_ref[1:2, :]
    chosen = (first | second).astype(BF16)
    token = lax.broadcasted_iota(jnp.int32, (tokens, tokens), 0)
    later = lax.broadcasted_iota(jnp.int32, (tokens, tokens), 1)
    place = mm(chosen, (token < later).astype(BF16)) + (expert * capacity).astype(F32)
    s0 = jnp.sum(jnp.where(first, place, 0.0), axis=0, keepdims=True)
    s1 = jnp.sum(jnp.where(second, place, 0.0), axis=0, keepdims=True)
    step = 128
    cuts = width // LANES
    for base in range(0, slots, step):
        slot = (lax.broadcasted_iota(jnp.int32, (step, tokens), 0) + base).astype(F32)
        is0, is1 = slot == s0, slot == s1
        spread(wide, step, 0, mm((is0 | is1).astype(BF16), xn))
        out_ref[base * cuts : (base + step) * cuts, :] = wide[...].astype(BF16)
        mix = jnp.where(is0, weight_ref[0:1, :], 0.0) + jnp.where(is1, weight_ref[1:2, :], 0.0)
        mix_ref[:, base : base + step] = mix.T


def dispatch(x, gain, routes, weight, slots, capacity):
    tokens, width = x.shape
    cuts = width // LANES
    return pl.pallas_call(
        functools.partial(dispatch_kernel, capacity),
        out_shape=[
            jax.ShapeDtypeStruct((tokens, width), BF16),
            jax.ShapeDtypeStruct((slots * cuts, LANES), BF16),
            jax.ShapeDtypeStruct((tokens, slots), F32),
        ],
        scratch_shapes=[pltpu.VMEM((128 * cuts, LANES), F32)],
        name="dispatch",
    )(x, gain.reshape(1, width), routes, weight)


def mixer_sum_kernel(*refs):
    *part_refs, out_ref = refs
    total = part_refs[0][...].astype(F32)
    for part in part_refs[1:]:
        total = total + part[...].astype(F32)
    out_ref[...] = total.astype(BF16)


def mixer_sum(parts):
    rows, width = parts[0].shape
    half = pl.BlockSpec((rows // 2, width), lambda c: (0, 0))
    return pl.pallas_call(
        mixer_sum_kernel,
        grid=(1,),
        in_specs=[half] * len(parts),
        out_specs=half,
        out_shape=jax.ShapeDtypeStruct((rows // 2, width), BF16),
        cost_estimate=pl.CostEstimate(flops=1_000_000_000, bytes_accessed=3_000_000, transcendentals=0),
        name="mixer_sum",
    )(*parts)


def combine_kernel(*refs):
    *part_refs, back_ref, mix_ref, out_ref, wide, total = refs
    rows = mix_ref.shape[1]
    cuts = total.shape[1] // LANES
    step = pl.program_id(0)

    @pl.when(step == 0)
    def _():
        shared = part_refs[0][...].astype(F32)
        for part in part_refs[1:]:
            shared = shared + part[...].astype(F32)
        total[...] = shared

    wide[...] = back_ref[...].astype(F32)
    total[...] += dot2(mix_ref[...], gathered(wide, rows, cuts))

    @pl.when(step == pl.num_programs(0) - 1)
    def _():
        out_ref[...] = total[...].astype(BF16)


def combine(parts, back, mix):
    tokens, slots = mix.shape
    width = parts[0].shape[1]
    cuts = width // LANES
    tile = 128
    return pl.pallas_call(
        combine_kernel,
        grid=(slots // tile,),
        in_specs=[pl.BlockSpec((tokens, width), lambda c: (1, 0))] * len(parts)
        + [
            pl.BlockSpec((tile * cuts, LANES), lambda c: (c, 0)),
            pl.BlockSpec((tokens, tile), lambda c: (0, c)),
        ],
        out_specs=pl.BlockSpec((tokens, width), lambda c: (0, 0)),
        out_shape=jax.ShapeDtypeStruct((tokens, width), BF16),
        scratch_shapes=[pltpu.VMEM((tile * cuts, LANES), F32), pltpu.VMEM((tokens, width), F32)],
        name="combine",
    )(*parts, back, mix)


def ring(axis):
    peers = lax.axis_size(axis)
    return (
        [(i, (i + 1) % peers) for i in range(peers)],
        [(i, (i - 1) % peers) for i in range(peers)],
    )


def neighbours_shards(shard, axis):
    right, left = ring(axis)
    from_left = [lax.ppermute(w, axis, right) for w in shard]
    from_right = [lax.ppermute(w, axis, left) for w in shard]
    return from_left, from_right


def far_shard(from_left, from_right, axis):
    right, left = ring(axis)
    half = from_left[1].shape[0] // 2
    return (
        lax.ppermute(from_left[0], axis, right),
        lax.ppermute(from_left[1][:half], axis, right),
        lax.ppermute(from_right[1][half:], axis, left),
        lax.ppermute(from_right[2], axis, left),
    )


def gated(gate_val, up_val):
    return (jax.nn.silu(gate_val) * up_val).astype(BF16)


def shards(
    queries,
    keys,
    values,
    decay_gate_logits,
    correction_logits,
    head_decay_speed,
    position_log_decay,
    head_output_gain,
    mixer_output_weight,
    expert_input_tokens,
    expert_norm_gain,
    routes,
    chosen_expert_weight,
    routed_gate_weight,
    routed_up_weight,
    routed_down_weight,
    common_gate_weight,
    common_up_weight,
    common_down_weight,
):
    experts = lax.axis_size(EP)
    tokens, _ = expert_input_tokens.shape
    own = (routed_gate_weight[0], routed_up_weight[0], routed_down_weight[0])
    from_left, from_right = neighbours_shards(own, "tp")

    capacity = 3 * tokens * routes.shape[1] // (2 * experts)
    xn, outgoing, mix = dispatch(
        expert_input_tokens,
        expert_norm_gain,
        routes.T,
        chosen_expert_weight.T,
        experts * capacity,
        capacity,
    )

    def to_peers(x):
        parts = x.reshape(experts, -1, LANES)
        return lax.all_to_all(parts, EP, split_axis=0, concat_axis=0, tiled=True).reshape(-1, LANES)

    arrived = to_peers(outgoing)

    qt, ol, trans, inject = local_mixer(
        queries,
        keys,
        values,
        decay_gate_logits.T,
        correction_logits.T,
        head_decay_speed,
        position_log_decay.T,
    )
    state, group = entry_state(trans, inject, xn)
    state, from_left, from_right = lax.optimization_barrier((state, from_left, from_right))
    far = far_shard(from_left, from_right, "tp")
    me = lax.axis_index("tp").astype(jnp.int32).reshape(1)
    parts = parts_for_peers(
        me,
        lax.axis_size("tp"),
        qt,
        ol,
        state,
        head_output_gain,
        mixer_output_weight,
        group,
        common_gate_weight,
        common_up_weight,
        common_down_weight,
    )
    rows, near = near_experts(arrived, (own, from_left, from_right))
    parts, near = lax.optimization_barrier((parts, near))
    peers = lax.axis_size("tp")
    got = [parts[0]] + [
        lax.ppermute(parts[r], "tp", [(i, (i + r) % peers) for i in range(peers)])
        for r in range(1, peers)
    ]
    slot_sums = far_expert(rows, near, *far)
    back = to_peers(slot_sums)
    return (mixer_sum(got), combine(got, back, mix))


def solution(mesh):
    finer = Mesh(mesh.devices.reshape(8, 4, 2, mesh.shape["tp"]), ("ep_0", "ep_1", "ep_2", "tp"))
    placed = (
        P(EP, "tp"),
        P(EP, "tp"),
        P(EP, "tp"),
        P(EP, "tp"),
        P(EP, "tp"),
        P("tp"),
        P(EP, "tp"),
        P(),
        P("tp", None),
        P(EP_TP, None),
        P(),
        P(EP_TP, None),
        P(EP_TP, None),
        P(EP, None, "tp"),
        P(EP, None, "tp"),
        P(EP, "tp", None),
        P(None, "tp"),
        P(None, "tp"),
        P("tp", None),
    )
    return jax.shard_map(
        shards,
        mesh=finer,
        in_specs=placed,
        out_specs=(P(EP_TP, None), P(EP_TP, None)),
        check_vma=False,
    )
```

profile of v0, /device:TPU:8, one launch (start us, length us, event | category | flops | bytes accessed | tf_op | source)
XLA Modules:
  0.0 224.4 jit_solution(14043467287667839906)
XLA Ops:
  0.6 1.6 collective-permute-start
  2.2 1.7 collective-permute-start.3
  3.9 0.3 collective-permute-start.1
  4.2 3.0 %collective-permute-start.4 = (bf16[2048,256]{1,0:T(8,128)(2,1)}, bf16[2048,256]{1,0:T(8,128)(2,1)}, u32[]{:S(2)}, u32[]{:S(2)}) collective-permute-start(bf16[2048,256]{1,0:T(8,128)(2,1)} %bitcast.28), channel_id=1, source_target_pairs={{0,3},{1,0},{2,1},{3,2},{4,7},{5,4},{6,5},{7,6},{8,11},{9,8},{10,9... | collective-permute-start | bytes 3145736 | tf_op jit(solution)/shard_map/ppermute | solution.py:644
  7.2 0.0 collective-permute-start.2
  7.2 3.8 %dispatch.1 = (bf16[128,2048]{1,0:T(8,128)(2,1)}, bf16[6144,128]{1,0:T(8,128)(2,1)}, f32[128,384]{1,0:T(8,128)}) custom-call(bf16[128,2048]{1,0:T(8,128)(2,1)} %x_ref.1, f32[1,2048]{1,0:T(1,128)} %bitcast.20, s32[2,128]{1,0:T(2,128)} %bitcast.21, f32[2,128]{1,0:T(2,128)} %bitcast.22), custom_call_target="tpu_custom_call" | custom-call | tf_op jit(solution)/shard_map/dispatch/pallas_call | solution.py:558
  11.0 12.2 %all-to-all-start = ((bf16[64,96,128]{2,1,0:T(8,128)(2,1)}), bf16[64,96,128]{2,1,0:T(8,128)(2,1)S(1)}, u32[]{:S(2)}, u32[]{:S(2)}) async-start(bf16[64,96,128]{2,1,0:T(8,128)(2,1)} %bitcast.19), calls=%async_computation | async-start | bytes 3145728 | tf_op jit(solution)/shard_map/all_to_all | solution.py:701
  23.2 0.0 copy-done.6
  23.2 0.7 copy.21.speed_ref
  23.9 32.0 %local_mixer.1 = (f32[3,512,128]{2,1,0:T(8,128)}, f32[3,512,128]{2,1,0:T(8,128)}, f32[3,128,128]{2,1,0:T(8,128)}, f32[3,128,128]{2,1,0:T(8,128)}) custom-call(bf16[512,384]{1,0:T(8,128)(2,1)} %q_ref.1, bf16[512,384]{1,0:T(8,128)(2,1)} %k_ref.1, bf16[512,384]{1,0:T(8,128)(2,1)} %v_ref.1, f32[3,512]{1,0:T(4,128)} %bitcast.33, bf16[3,512]{1,0:T(4,128)(2,1)} %bitcast.35, ...), custom_call_target="tpu_custom_call" | custom-call | flops 30000001024 | bytes 4000000 | tf_op jit(solution)/shard_map/local_mixer/pallas_call | solution.py:150
  55.9 0.0 collective-permute-done.refs_3_
  55.9 3.5 %collective-permute-start.5 = (bf16[256,2048]{1,0:T(8,128)(2,1)}, bf16[256,2048]{1,0:T(8,128)(2,1)}, u32[]{:S(2)}, u32[]{:S(2)}) collective-permute-start(bf16[256,2048]{1,0:T(8,128)(2,1)} %bitcast.31), channel_id=1, source_target_pairs={{0,3},{1,0},{2,1},{3,2},{4,7},{5,4},{6,5},{7,6},{8,11},{9,8},{10,9... | collective-permute-start | bytes 3145736 | tf_op jit(solution)/shard_map/ppermute | solution.py:644
  59.4 47.2 %entry_state.1 = (f32[3,128,128]{2,1,0:T(8,128)}, bf16[4,128,2048]{2,1,0:T(8,128)(2,1)}) custom-call(f32[3,128,128]{2,1,0:T(8,128)} %get-tuple-element.31.t_ref, f32[3,128,128]{2,1,0:T(8,128)} %get-tuple-element.32.i_ref, bf16[128,2048]{1,0:T(8,128)(2,1)} %get-tuple-element.33.xn_ref), custom_call_target="tpu_custom_call" | custom-call | flops 30000001024 | bytes 4000000 | tf_op jit(solution)/shard_map/entry_state/pallas_call | solution.py:327
  106.6 0.0 collective-permute-done.1.refs_4_
  106.6 0.0 copy-start.5
  106.6 0.0 collective-permute-done.2.refs_5_
  106.6 0.0 collective-permute-done.3.refs_6_
  106.6 0.0 collective-permute-done.4.refs_7_
  106.6 0.0 collective-permute-done.5.refs_8_
  106.7 1.0 copy-done.5
  107.6 0.0 collective-permute-start.9
  107.6 3.7 %collective-permute-start.12 = (bf16[256,2048]{1,0:T(8,128)(2,1)}, bf16[256,2048]{1,0:T(8,128)(2,1)}, u32[]{:S(2)}, u32[]{:S(2)}) collective-permute-start(bf16[256,2048]{1,0:T(8,128)(2,1)} %collective-permute-done.5.refs_8_), channel_id=1, source_target_pairs={{0,3},{1,0},{2,1},{3,2},{4,7},{5,4},{6,5},{7,6},{8,11},{9,8},{10,9... | collective-permute-start | bytes 3145736 | tf_op jit(solution)/shard_map/ppermute | solution.py:655
  111.3 1.9 slice.6
  113.2 0.0 collective-permute-start.10
  113.2 1.9 slice.7
  115.0 3.2 %collective-permute-start.11 = (bf16[1024,256]{1,0:T(8,128)(2,1)}, bf16[1024,256]{1,0:T(8,128)(2,1)}, u32[]{:S(2)}, u32[]{:S(2)}) collective-permute-start(bf16[1024,256]{1,0:T(8,128)(2,1)} %slice.7), channel_id=1, source_target_pairs={{0,3},{1,0},{2,1},{3,2},{4,7},{5,4},{6,5},{7,6},{8,11},{9,8},{10,9... | collective-permute-start | bytes 1572872 | tf_op jit(solution)/shard_map/ppermute | solution.py:654
  118.3 10.4 %parts_for_peers.1 = (bf16[256,2048]{1,0:T(8,128)(2,1)}, bf16[256,2048]{1,0:T(8,128)(2,1)}, bf16[256,2048]{1,0:T(8,128)(2,1)}, bf16[256,2048]{1,0:T(8,128)(2,1)}) custom-call(s32[1]{0:T(128)} %bitcast.me_ref, f32[3,512,128]{2,1,0:T(8,128)} %get-tuple-element.29.qt_ref, f32[3,512,128]{2,1,0:T(8,128)} %get-tuple-element.30.ol_ref, ...), custom_call_target="tpu_custom_call" | custom-call | flops 6000000000 | bytes 12000000 | tf_op jit(solution)/shard_map/parts_for_peers/pallas_call | solution.py:384
  128.7 0.0 all-to-all-done
  128.7 1.2 copy-done.2
  129.9 11.3 %near_experts.1 = (bf16[384,2048]{1,0:T(8,128)(2,1)}, f32[384,2048]{1,0:T(8,128)}) custom-call(bf16[6144,128]{1,0:T(8,128)(2,1)} %bitcast.18, bf16[2048,256]{1,0:T(8,128)(2,1)} %bitcast.26, bf16[2048,256]{1,0:T(8,128)(2,1)} %bitcast.29, bf16[256,2048]{1,0:T(8,128)(2,1)} %bitcast.32, bf16[2048,256]{1,0:T(8,128)(2,1)} %collective-permute-done.refs_3_, ...), custom_call_target="tpu_custom_call" | custom-call | flops 5000000000 | bytes 16000000 | tf_op jit(solution)/shard_map/near_experts/pallas_call | solution.py:448
  141.2 4.1 %collective-permute-done.10.refs_1_ = bf16[1024,256]{1,0:T(8,128)(2,1)S(1)} collective-permute-done((bf16[1024,256]{1,0:T(8,128)(2,1)}, bf16[1024,256]{1,0:T(8,128)(2,1)S(1)}, u32[]{:S(2)}, u32[]{:S(2)}) %collective-permute-start.10) | collective-permute-done | bytes 524320 | tf_op jit(solution)/shard_map/ppermute | solution.py:653
  145.3 0.0 collective-permute-done.11.refs_2_
  145.3 0.0 collective-permute-done.9.refs_0_
  145.3 0.0 collective-permute-done.12.refs_3_
  145.4 0.8 copy-done.4
  146.1 0.3 copy-done.3
  146.5 8.3 %far_expert.1 = bf16[6144,128]{1,0:T(8,128)(2,1)} custom-call(bf16[384,2048]{1,0:T(8,128)(2,1)} %get-tuple-element.53.x_ref, f32[384,2048]{1,0:T(8,128)} %get-tuple-element.54.near_ref, bf16[2048,256]{1,0:T(8,128)(2,1)} %copy-done.3, bf16[1024,256]{1,0:T(8,128)(2,1)} %copy-done.4, bf16[1024,256]{1,0:T(8,128)(2,1)} %collective-permute-done.11.refs_2_, ...), custom_call_target="tpu_custom_call" | custom-call | flops 2000000000 | bytes 12000000 | tf_op jit(solution)/shard_map/far_expert/pallas_call | solution.py:500
  154.7 10.3 %all-to-all-start.1 = ((bf16[64,96,128]{2,1,0:T(8,128)(2,1)}), bf16[64,96,128]{2,1,0:T(8,128)(2,1)S(1)}, u32[]{:S(2)}, u32[]{:S(2)}) async-start(bf16[64,96,128]{2,1,0:T(8,128)(2,1)} %bitcast.16), calls=%async_computation.1 | async-start | bytes 3145728 | tf_op jit(solution)/shard_map/all_to_all | solution.py:701
  165.1 1.4 collective-permute-start.6
  166.4 3.3 %collective-permute-start.7 = (bf16[256,2048]{1,0:T(8,128)(2,1)}, bf16[256,2048]{1,0:T(8,128)(2,1)}, u32[]{:S(2)}, u32[]{:S(2)}) collective-permute-start(bf16[256,2048]{1,0:T(8,128)(2,1)} %get-tuple-element.51), channel_id=1, source_target_pairs={{0,2},{1,3},{2,0},{3,1},{4,6},{5,7},{6,4},{7,5},{8,10},{9,11},{10,... | collective-permute-start | bytes 3145736 | tf_op jit(solution)/shard_map/ppermute | solution.py:735
  169.7 1.1 collective-permute-start.8
  170.9 21.1 %collective-permute-done.6.refs_1_ = bf16[256,2048]{1,0:T(8,128)(2,1)S(1)} collective-permute-done((bf16[256,2048]{1,0:T(8,128)(2,1)}, bf16[256,2048]{1,0:T(8,128)(2,1)S(1)}, u32[]{:S(2)}, u32[]{:S(2)}) %collective-permute-start.6) | collective-permute-done | bytes 1048608 | tf_op jit(solution)/shard_map/ppermute | solution.py:735
  192.0 23.7 %collective-permute-done.7.refs_2_ = bf16[256,2048]{1,0:T(8,128)(2,1)} collective-permute-done((bf16[256,2048]{1,0:T(8,128)(2,1)}, bf16[256,2048]{1,0:T(8,128)(2,1)}, u32[]{:S(2)}, u32[]{:S(2)}) %collective-permute-start.7) | collective-permute-done | bytes 1048608 | tf_op jit(solution)/shard_map/ppermute | solution.py:735
  215.7 0.0 collective-permute-done.8.refs_3_
  215.7 2.6 %mixer_sum.1 = bf16[128,2048]{1,0:T(8,128)(2,1)} custom-call(bf16[256,2048]{1,0:T(8,128)(2,1)} %get-tuple-element.49.refs_0_, bf16[256,2048]{1,0:T(8,128)(2,1)} %copy-done.1, bf16[256,2048]{1,0:T(8,128)(2,1)} %collective-permute-done.7.refs_2_, bf16[256,2048]{1,0:T(8,128)(2,1)} %collective-permute-done.8.refs_3_), custom_call_target="tpu_custom_call" | custom-call | flops 1000000000 | bytes 3000000 | tf_op jit(solution)/shard_map/mixer_sum/pallas_call | solution.py:581
  218.2 0.0 all-to-all-done.1
  218.2 1.2 copy-done
  219.4 5.0 %combine.1 = bf16[128,2048]{1,0:T(8,128)(2,1)} custom-call(bf16[256,2048]{1,0:T(8,128)(2,1)} %get-tuple-element.49.refs_0_, bf16[256,2048]{1,0:T(8,128)(2,1)} %copy-done.1, bf16[256,2048]{1,0:T(8,128)(2,1)} %collective-permute-done.7.refs_2_, bf16[256,2048]{1,0:T(8,128)(2,1)} %collective-permute-done.8.refs_3_, bf16[6144,128]{1,0:T(8,128)(2,1)} %bitcast.17, ...), custom_call_target="tpu_custom_call" | custom-call | tf_op jit(solution)/shard_map/combine/pallas_call | solution.py:618
  (7 shorter events, 0.0 us)
Async XLA Ops:
  0.6 55.2 %collective-permute-start = (bf16[2048,256]{1,0:T(8,128)(2,1)}, bf16[2048,256]{1,0:T(8,128)(2,1)}, u32[]{:S(2)}, u32[]{:S(2)}) collective-permute-start(bf16[2048,256]{1,0:T(8,128)(2,1)} %bitcast.24), channel_id=1, source_target_pairs={{0,1},{1,2},{2,3},{3,0},{4,5},{5,6},{6,7},{7,4},{8,9},{9,10},{10,1... | collective-permute-start | bytes 3145736 | tf_op jit(solution)/shard_map/ppermute | solution.py:643
  2.2 104.4 %collective-permute-start.3 = (bf16[2048,256]{1,0:T(8,128)(2,1)}, bf16[2048,256]{1,0:T(8,128)(2,1)}, u32[]{:S(2)}, u32[]{:S(2)}) collective-permute-start(bf16[2048,256]{1,0:T(8,128)(2,1)} %bitcast.25), channel_id=1, source_target_pairs={{0,3},{1,0},{2,1},{3,2},{4,7},{5,4},{6,5},{7,6},{8,11},{9,8},{10,9... | collective-permute-start | bytes 3145736 | tf_op jit(solution)/shard_map/ppermute | solution.py:644
  3.9 102.6 %collective-permute-start.1 = (bf16[2048,256]{1,0:T(8,128)(2,1)}, bf16[2048,256]{1,0:T(8,128)(2,1)S(1)}, u32[]{:S(2)}, u32[]{:S(2)}) collective-permute-start(bf16[2048,256]{1,0:T(8,128)(2,1)} %bitcast.27), channel_id=1, source_target_pairs={{0,1},{1,2},{2,3},{3,0},{4,5},{5,6},{6,7},{7,4},{8,9},{9,10},{10,1... | collective-permute-start | bytes 3145736 | tf_op jit(solution)/shard_map/ppermute | solution.py:643
  4.2 102.4 %collective-permute-start.4 = (bf16[2048,256]{1,0:T(8,128)(2,1)}, bf16[2048,256]{1,0:T(8,128)(2,1)}, u32[]{:S(2)}, u32[]{:S(2)}) collective-permute-start(bf16[2048,256]{1,0:T(8,128)(2,1)} %bitcast.28), channel_id=1, source_target_pairs={{0,3},{1,0},{2,1},{3,2},{4,7},{5,4},{6,5},{7,6},{8,11},{9,8},{10,9... | collective-permute-start | bytes 3145736 | tf_op jit(solution)/shard_map/ppermute | solution.py:644
  7.2 99.4 %collective-permute-start.2 = (bf16[256,2048]{1,0:T(8,128)(2,1)}, bf16[256,2048]{1,0:T(8,128)(2,1)}, u32[]{:S(2)}, u32[]{:S(2)}) collective-permute-start(bf16[256,2048]{1,0:T(8,128)(2,1)} %bitcast.30), channel_id=1, source_target_pairs={{0,1},{1,2},{2,3},{3,0},{4,5},{5,6},{6,7},{7,4},{8,9},{9,10},{10,1... | collective-permute-start | bytes 3145736 | tf_op jit(solution)/shard_map/ppermute | solution.py:643
  11.0 12.2 %copy-start.6 = (f32[3]{0:T(128)S(1)}, f32[3]{0:T(128)}, u32[]{:S(2)}) copy-start(f32[3]{0:T(128)} %param.24) | copy-start | bytes 40
  11.0 117.8 %all-to-all-start = ((bf16[64,96,128]{2,1,0:T(8,128)(2,1)}), bf16[64,96,128]{2,1,0:T(8,128)(2,1)S(1)}, u32[]{:S(2)}, u32[]{:S(2)}) async-start(bf16[64,96,128]{2,1,0:T(8,128)(2,1)} %bitcast.19), calls=%async_computation | async-start | bytes 3145728 | tf_op jit(solution)/shard_map/all_to_all | solution.py:701
  55.9 50.8 %collective-permute-start.5 = (bf16[256,2048]{1,0:T(8,128)(2,1)}, bf16[256,2048]{1,0:T(8,128)(2,1)}, u32[]{:S(2)}, u32[]{:S(2)}) collective-permute-start(bf16[256,2048]{1,0:T(8,128)(2,1)} %bitcast.31), channel_id=1, source_target_pairs={{0,3},{1,0},{2,1},{3,2},{4,7},{5,4},{6,5},{7,6},{8,11},{9,8},{10,9... | collective-permute-start | bytes 3145736 | tf_op jit(solution)/shard_map/ppermute | solution.py:644
  106.6 1.0 copy-start.5
  107.6 37.7 %collective-permute-start.9 = (bf16[2048,256]{1,0:T(8,128)(2,1)}, bf16[2048,256]{1,0:T(8,128)(2,1)S(1)}, u32[]{:S(2)}, u32[]{:S(2)}) collective-permute-start(bf16[2048,256]{1,0:T(8,128)(2,1)} %collective-permute-done.refs_3_), channel_id=1, source_target_pairs={{0,1},{1,2},{2,3},{3,0},{4,5},{5,6},{6,7},{7,4},{8,9},{9,10},{10,1... | collective-permute-start | bytes 3145736 | tf_op jit(solution)/shard_map/ppermute | solution.py:652
  107.6 37.7 %collective-permute-start.12 = (bf16[256,2048]{1,0:T(8,128)(2,1)}, bf16[256,2048]{1,0:T(8,128)(2,1)}, u32[]{:S(2)}, u32[]{:S(2)}) collective-permute-start(bf16[256,2048]{1,0:T(8,128)(2,1)} %collective-permute-done.5.refs_8_), channel_id=1, source_target_pairs={{0,3},{1,0},{2,1},{3,2},{4,7},{5,4},{6,5},{7,6},{8,11},{9,8},{10,9... | collective-permute-start | bytes 3145736 | tf_op jit(solution)/shard_map/ppermute | solution.py:655
  113.2 32.2 %collective-permute-start.10 = (bf16[1024,256]{1,0:T(8,128)(2,1)}, bf16[1024,256]{1,0:T(8,128)(2,1)S(1)}, u32[]{:S(2)}, u32[]{:S(2)}) collective-permute-start(bf16[1024,256]{1,0:T(8,128)(2,1)} %slice.6), channel_id=1, source_target_pairs={{0,1},{1,2},{2,3},{3,0},{4,5},{5,6},{6,7},{7,4},{8,9},{9,10},{10,1... | collective-permute-start | bytes 1572872 | tf_op jit(solution)/shard_map/ppermute | solution.py:653
  115.0 30.3 %collective-permute-start.11 = (bf16[1024,256]{1,0:T(8,128)(2,1)}, bf16[1024,256]{1,0:T(8,128)(2,1)}, u32[]{:S(2)}, u32[]{:S(2)}) collective-permute-start(bf16[1024,256]{1,0:T(8,128)(2,1)} %slice.7), channel_id=1, source_target_pairs={{0,3},{1,0},{2,1},{3,2},{4,7},{5,4},{6,5},{7,6},{8,11},{9,8},{10,9... | collective-permute-start | bytes 1572872 | tf_op jit(solution)/shard_map/ppermute | solution.py:654
  128.7 1.2 copy-start.2
  145.3 0.8 copy-start.4
  145.3 1.1 copy-start.3
  154.7 63.5 %all-to-all-start.1 = ((bf16[64,96,128]{2,1,0:T(8,128)(2,1)}), bf16[64,96,128]{2,1,0:T(8,128)(2,1)S(1)}, u32[]{:S(2)}, u32[]{:S(2)}) async-start(bf16[64,96,128]{2,1,0:T(8,128)(2,1)} %bitcast.16), calls=%async_computation.1 | async-start | bytes 3145728 | tf_op jit(solution)/shard_map/all_to_all | solution.py:701
  165.1 26.9 %collective-permute-start.6 = (bf16[256,2048]{1,0:T(8,128)(2,1)}, bf16[256,2048]{1,0:T(8,128)(2,1)S(1)}, u32[]{:S(2)}, u32[]{:S(2)}) collective-permute-start(bf16[256,2048]{1,0:T(8,128)(2,1)} %get-tuple-element.50), channel_id=1, source_target_pairs={{0,1},{1,2},{2,3},{3,0},{4,5},{5,6},{6,7},{7,4},{8,9},{9,10},{10,1... | collective-permute-start | bytes 3145736 | tf_op jit(solution)/shard_map/ppermute | solution.py:735
  166.4 49.2 %collective-permute-start.7 = (bf16[256,2048]{1,0:T(8,128)(2,1)}, bf16[256,2048]{1,0:T(8,128)(2,1)}, u32[]{:S(2)}, u32[]{:S(2)}) collective-permute-start(bf16[256,2048]{1,0:T(8,128)(2,1)} %get-tuple-element.51), channel_id=1, source_target_pairs={{0,2},{1,3},{2,0},{3,1},{4,6},{5,7},{6,4},{7,5},{8,10},{9,11},{10,... | collective-permute-start | bytes 3145736 | tf_op jit(solution)/shard_map/ppermute | solution.py:735
  169.7 45.9 %collective-permute-start.8 = (bf16[256,2048]{1,0:T(8,128)(2,1)}, bf16[256,2048]{1,0:T(8,128)(2,1)}, u32[]{:S(2)}, u32[]{:S(2)}) collective-permute-start(bf16[256,2048]{1,0:T(8,128)(2,1)} %get-tuple-element.52), channel_id=1, source_target_pairs={{0,3},{1,0},{2,1},{3,2},{4,7},{5,4},{6,5},{7,6},{8,11},{9,8},{10,9... | collective-permute-start | bytes 3145736 | tf_op jit(solution)/shard_map/ppermute | solution.py:735
  192.0 23.7 %copy-start.1 = (bf16[256,2048]{1,0:T(8,128)(2,1)}, bf16[256,2048]{1,0:T(8,128)(2,1)S(1)}, u32[]{:S(2)}) copy-start(bf16[256,2048]{1,0:T(8,128)(2,1)S(1)} %collective-permute-done.6.refs_1_) | copy-start | bytes 3145732
  218.2 1.2 copy-start
where the time goes:
time: 225 us; the launch traced here: 224 us
  Pallas kernels  121 us (54%)
  waiting for transfers between devices  48.9 us (22%)
  starting transfers between devices  45.3 us (20%)
  local copies, waits for them, and re-layouts  8.84 us (4%)
    pallas_call x1, Pallas kernels, entry_state(): pl.pallas_call(entry_state_kernel, in_specs=[vmem, vmem, pl.BlockSpec(mem...  47.2 us
    ppermute x3, waiting for transfers between devices, shards(): lax.ppermute(parts[r], 'tp', [(i, (i + r) % peers) for i in range(peers)])  44.8 us
    pallas_call x1, Pallas kernels, local_mixer(): pl.pallas_call(local_mixer_kernel, grid=(heads,), in_specs=[by_head, by_h...  32 us
    all_to_all x2, starting transfers between devices, to_peers(): lax.all_to_all(parts, EP, split_axis=0, concat_axis=0, tiled=True)  22.5 us
    pallas_call x1, Pallas kernels, near_experts(): pl.pallas_call(near_experts_kernel, in_specs=[vmem] + [pl.BlockSpec(memor...  11.3 us
    pallas_call x1, Pallas kernels, parts_for_peers(): pl.pallas_call(parts_kernel, grid_spec=pltpu.PrefetchScalarGridSpec(num_s...  10.4 us
    pallas_call x1, Pallas kernels, far_expert(): pl.pallas_call(far_expert_kernel, in_specs=[vmem] + [pl.BlockSpec(memory_...  8.28 us
    ppermute x3, starting transfers between devices, neighbours_shards(): from_right = [lax.ppermute(w, axis, left) for w in shard]  8.19 us
  transfers between devices with their start and end apart: 15, of which 3 were waited for; matrix products, arithmetic and copies ran while one was open for 2% of the time, Pallas kernels for 48%

commit v1 on v0

--- a/solution.py
+++ b/solution.py
@@ -47,24 +47,25 @@
     return mm(jnp.concatenate([ah, al], 1), jnp.concatenate([b, b], 0))
 
 
-def unit_lower_inverse(low, row, col):
+def unit_lower_inverses(lows, row, col):
     eye = (row == col).astype(F32)
-    base = jnp.where((row >> 3) == (col >> 3), low, 0.0)
-    squared = dot3(base, base)
-    fourth = dot3(squared, squared)
-    inv = eye - base
-    inv = inv + dot3(inv, squared)
-    inv = inv + dot3(inv, fourth)
+    near = (row >> 3) == (col >> 3)
+    base = [jnp.where(near, low, 0.0) for low in lows]
+    squared = [dot3(x, x) for x in base]
+    inv = [eye - x for x in base]
+    fourth = [dot3(x, x) for x in squared]
+    inv = [x + dot3(x, y) for x, y in zip(inv, squared)]
+    inv = [x + dot3(x, y) for x, y in zip(inv, fourth)]
     for bit in (3, 4, 5):
-        across = jnp.where(
-            ((row >> (bit + 1)) == (col >> (bit + 1))) & ((row >> bit) != (col >> bit)), low, 0.0
-        )
-        inv = inv - dot3(inv, dot3(across, inv))
+        between = ((row >> (bit + 1)) == (col >> (bit + 1))) & ((row >> bit) != (col >> bit))
+        right = [dot3(jnp.where(between, low, 0.0), x) for low, x in zip(lows, inv)]
+        inv = [x - dot3(x, y) for x, y in zip(inv, right)]
     return inv
 
 
 def local_mixer_kernel(
-    q_ref, k_ref, v_ref, gate_ref, corr_ref, speed_ref, plog_ref, qt_ref, ol_ref, tr_ref, in_ref
+    q_ref, k_ref, v_ref, gate_ref, corr_ref, speed_ref, plog_ref, qt_ref, ol_ref, tr_ref, in_ref,
+    su_all, pq_all, mw_all, keep_all,
 ):
     head = pl.program_id(0)
     heads, rows = gate_ref.shape
@@ -89,56 +90,82 @@
     ones = (same & (row <= col)).astype(BF16)
     ones = jnp.concatenate([ones, ones, ones], 0)
 
-    packs = []
-    for p in range(rows // pair):
-        at = pl.ds(p * pair, pair)
-        qb, kb, vb = q_ref[at, :], k_ref[at, :], v_ref[at, :]
-        qf, kf = qb.astype(F32), kb.astype(F32)
-        rq = lax.rsqrt(jnp.sum(qf * qf, axis=1, keepdims=True) + EPS) * (pair**-0.5)
-        rk = lax.rsqrt(jnp.sum(kf * kf, axis=1, keepdims=True) + EPS)
-        g_mat = jnp.broadcast_to(g_row[:, p * pair : (p + 1) * pair], (pair, pair))
-        c_row = mm(jnp.concatenate(thirds(g_mat), 1), ones)
-        c_mat = c_row.T
-        last0, last1 = c_mat[63:64, :], c_mat[127:128, :]
-        rk_row = jnp.broadcast_to(rk, (pair, pair)).T
-        beta_row = jnp.broadcast_to(beta_row_all[:, p * pair : (p + 1) * pair], (pair, pair))
-        beta = beta_row.T
-        gram = lax.dot_general(
-            jnp.concatenate([kb, qb], 0), kb, (((1,), (1,)), ((), ())), preferred_element_type=F32
+    pairs = range(rows // pair)
+    span = [slice(p * pair, (p + 1) * pair) for p in pairs]
+    qb, kb, vb = [[ref[at, :] for at in span] for ref in (q_ref, k_ref, v_ref)]
+    gram = [
+        lax.dot_general(
+            jnp.concatenate([k, q], 0), k, (((1,), (1,)), ((), ())), preferred_element_type=F32
         )
-        decay = jnp.exp(jnp.where(causal, c_mat - c_row, -jnp.inf)) * rk_row
-        low = jnp.where(strict, gram[:pair] * decay * (beta * rk), 0.0)
-        scores = gram[pair:] * decay * rq
-        inv = unit_lower_inverse(low, row, col)
-        scale = beta_row * inv
-        uw = jnp.concatenate(
-            [dot2(scale, vb), dot2(scale * (jnp.exp(c_row) * rk_row), kb)], 1
-        )
-        suw = dot3(scores, uw)
-        pq = qf * (rq * jnp.exp(c_mat)) - suw[:, pair:]
-        tail = jnp.exp(jnp.where(first, last0, last1) - c_row)
-        kt = kf.T * (tail * rk_row)
-        kk = jnp.concatenate([jnp.where(first, kt, 0.0), jnp.where(first, 0.0, kt)], 0)
-        mw = dot3(kk, uw)
-        packs.append((suw[:, :pair], pq, mw, jnp.exp(last0), jnp.exp(last1)))
-
-    ab = jnp.concatenate([(row == col).astype(F32), jnp.zeros((pair, pair), F32)], 1)
-    for p, (su, pq, mw, keep0, keep1) in enumerate(packs):
-        for b, keep in enumerate((keep0, keep1)):
-            blk = slice(b * 64, (b + 1) * 64)
-            at = pl.ds(p * pair + b * 64, 64)
-            part = mw[b * pair : (b + 1) * pair]
-            got = dot3(jnp.concatenate([pq[blk], part[:, pair:]], 0), ab)
-            qt_ref[0, at, :] = got[:64, :pair]
-            ol_ref[0, at, :] = got[:64, pair:] + su[blk]
-            keep2 = jnp.concatenate([keep, keep], 1)
-            ab = (
-                keep2 * ab
-                - got[64:]
-                + jnp.concatenate([jnp.zeros((pair, pair), F32), part[:, :pair]], 1)
-            )
-    tr_ref[0] = ab[:, :pair]
-    in_ref[0] = ab[:, pair:]
+        for k, q in zip(kb, qb)
+    ]
+    c_row = [
+        mm(jnp.concatenate(thirds(jnp.broadcast_to(g_row[:, at], (pair, pair))), 1), ones)
+        for at in span
+    ]
+    c_mat = [c.T for c in c_row]
+    qf, kf = [x.astype(F32) for x in qb], [x.astype(F32) for x in kb]
+    rq = [
+        lax.rsqrt(jnp.sum(x * x, axis=1, keepdims=True) + EPS) * (pair**-0.5) for x in qf
+    ]
+    rk = [lax.rsqrt(jnp.sum(x * x, axis=1, keepdims=True) + EPS) for x in kf]
+    rk_row = [jnp.broadcast_to(x, (pair, pair)).T for x in rk]
+    beta_row = [jnp.broadcast_to(beta_row_all[:, at], (pair, pair)) for at in span]
+    beta = [x.T for x in beta_row]
+    decay = [
+        jnp.exp(jnp.where(causal, cm - cr, -jnp.inf)) * r for cm, cr, r in zip(c_mat, c_row, rk_row)
+    ]
+    low = [
+        jnp.where(strict, g[:pair] * d * (b * r), 0.0) for g, d, b, r in zip(gram, decay, beta, rk)
+    ]
+    scores = [g[pair:] * d * r for g, d, r in zip(gram, decay, rq)]
+    inv = unit_lower_inverses(low, row, col)
+    scale = [b * x for b, x in zip(beta_row, inv)]
+    u = [dot2(x, v) for x, v in zip(scale, vb)]
+    w = [dot2(x * (jnp.exp(c) * r), k) for x, c, r, k in zip(scale, c_row, rk_row, kb)]
+    uw = [jnp.concatenate([x, y], 1) for x, y in zip(u, w)]
+    last = [(c[63:64, :], c[127:128, :]) for c in c_mat]
+    kt = [
+        k.T * (jnp.exp(jnp.where(first, l[0], l[1]) - c) * r)
+        for k, l, c, r in zip(kf, last, c_row, rk_row)
+    ]
+    suw = [dot3(x, y) for x, y in zip(scores, uw)]
+    mw = [
+        dot3(jnp.concatenate([jnp.where(first, x, 0.0), jnp.where(first, 0.0, x)], 0), y)
+        for x, y in zip(kt, uw)
+    ]
+    pq = [x * (r * jnp.exp(c)) - y[:, pair:] for x, r, c, y in zip(qf, rq, c_mat, suw)]
+    for p in pairs:
+        su_all[head, p] = suw[p][:, :pair]
+        pq_all[head, p] = pq[p]
+        mw_all[head, p] = mw[p]
+        keep_all[head, p] = jnp.concatenate([jnp.exp(x) for x in last[p]], 0)
+
+    @pl.when(head == heads - 1)
+    def _():
+        nothing = jnp.zeros((pair, pair), F32)
+        ab = [jnp.concatenate([(row == col).astype(F32), nothing], 1) for _ in range(heads)]
+        for p in pairs:
+            for b in range(2):
+                blk = slice(b * 64, (b + 1) * 64)
+                at = pl.ds(p * pair + b * 64, 64)
+                part = [mw_all[h, p, b * pair : (b + 1) * pair, :] for h in range(heads)]
+                got = [
+                    dot3(jnp.concatenate([pq_all[h, p, blk, :], part[h][:, pair:]], 0), ab[h])
+                    for h in range(heads)
+                ]
+                for h in range(heads):
+                    qt_ref[h, at, :] = got[h][:64, :pair]
+                    ol_ref[h, at, :] = got[h][:64, pair:] + su_all[h, p, blk, :]
+                    keep = keep_all[h, p, b : b + 1, :]
+                    ab[h] = (
+                        jnp.concatenate([keep, keep], 1) * ab[h]
+                        - got[h][64:]
+                        + jnp.concatenate([nothing, part[h][:, :pair]], 1)
+                    )
+        for h in range(heads):
+            tr_ref[h] = ab[h][:, :pair]
+            in_ref[h] = ab[h][:, pair:]
 
 
 def local_mixer(queries, keys, values, gate, corr, speed, plog):
@@ -160,10 +187,16 @@
             whole,
         ],
         out_specs=[
-            pl.BlockSpec((1, rows, d), lambda h: (h, 0, 0)),
-            pl.BlockSpec((1, rows, d), lambda h: (h, 0, 0)),
-            pl.BlockSpec((1, d, d), lambda h: (h, 0, 0)),
-            pl.BlockSpec((1, d, d), lambda h: (h, 0, 0)),
+            pl.BlockSpec((heads, rows, d), lambda h: (0, 0, 0)),
+            pl.BlockSpec((heads, rows, d), lambda h: (0, 0, 0)),
+            pl.BlockSpec((heads, d, d), lambda h: (0, 0, 0)),
+            pl.BlockSpec((heads, d, d), lambda h: (0, 0, 0)),
+        ],
+        scratch_shapes=[
+            pltpu.VMEM((heads, rows // 128, 128, d), F32),
+            pltpu.VMEM((heads, rows // 128, 128, d), F32),
+            pltpu.VMEM((heads, rows // 128, 2 * d, 2 * d), F32),
+            pltpu.VMEM((heads, rows // 128, 2, d), F32),
         ],
         out_shape=[
             jax.ShapeDtypeStruct((heads, rows, d), F32),
@@ -177,7 +210,7 @@
 
 
 def entry_state_kernel(
-    t_ref, i_ref, xn_ref, s_ref, group_ref, send_x, recv_x, keep_x, own, peer, ypack, zpack,
+    t_ref, i_ref, s_ref, own, peer, ypack, zpack,
     send_c, recv_c, send_y, recv_y, send_yc, recv_yc,
     send_r, recv_r, send_l, recv_l, send_rc, recv_rc, send_lc, recv_lc,
 ):
@@ -188,13 +221,11 @@
     other = {"ep_2": 1 - c}
     right, left = {"ep_0": lax.rem(z + 1, nz)}, {"ep_0": lax.rem(z + nz - 1, nz)}
     across = [{"ep_1": lax.rem(y + k, ny)} for k in range(1, ny)]
-    members, me = group_ref.shape[0], lax.axis_index("tp")
-    fellows = [{"tp": lax.rem(me + k, members)} for k in range(1, members)]
 
     barrier = pltpu.get_barrier_semaphore()
-    for who in (other, right, left, *across, *fellows):
+    for who in (other, right, left, *across):
         pl.semaphore_signal(barrier, inc=1, device_id=who, device_id_type=MESH)
-    pl.semaphore_wait(barrier, 3 + len(across) + len(fellows))
+    pl.semaphore_wait(barrier, 3 + len(across))
 
     def send(src, dst, send_sem, recv_sem, who):
         return pltpu.make_async_remote_copy(
@@ -218,20 +249,11 @@
     def added(pack):
         return pack[:, d:].astype(F32)
 
-    tokens = [
-        send(xn_ref, group_ref.at[me], send_x.at[k], recv_x.at[k], who)
-        for k, who in enumerate(fellows)
-    ]
-    kept = pltpu.make_async_copy(xn_ref, group_ref.at[me], keep_x)
-
     nothing = jnp.zeros((d, d), F32)
     for h in range(heads):
         store(own, h, jnp.concatenate([t_ref[h], i_ref[h]], 1))
     swap = send(own, peer, send_c, recv_c, other)
     swap.start()
-    for copy in tokens:
-        copy.start()
-    kept.start()
     swap.wait()
     for h in range(heads):
         mine, theirs = load(own, h), load(peer, h)
@@ -311,29 +333,21 @@
     for h in range(heads):
         pack = load(peer, h)
         s_ref[h] = jnp.where(c == 1, after(pack, s_ref[h]) + added(pack), s_ref[h])
-    kept.wait()
-    for copy in tokens:
-        copy.wait()
-
-
-def entry_state(trans, inject, xn):
+
+
+def entry_state(trans, inject):
     heads, d, _ = trans.shape
     nz, ny = lax.axis_size("ep_0"), lax.axis_size("ep_1")
     half = (2, heads, d // 2, 2 * d)
     dma = pltpu.SemaphoreType.DMA
     rounds = max(nz // 2, 1)
-    members = lax.axis_size("tp")
     vmem = pl.BlockSpec(memory_space=pltpu.VMEM)
     return pl.pallas_call(
         entry_state_kernel,
-        in_specs=[vmem, vmem, pl.BlockSpec(memory_space=pl.ANY)],
-        out_specs=[vmem, pl.BlockSpec(memory_space=pl.ANY)],
-        out_shape=[
-            jax.ShapeDtypeStruct((heads, d, d), F32),
-            jax.ShapeDtypeStruct((members, *xn.shape), BF16),
-        ],
+        in_specs=[vmem, vmem],
+        out_specs=vmem,
+        out_shape=jax.ShapeDtypeStruct((heads, d, d), F32),
         scratch_shapes=[
-            dma((max(members - 1, 1),)), dma((max(members - 1, 1),)), dma,
             pltpu.VMEM(half, BF16),
             pltpu.VMEM(half, BF16),
             pltpu.VMEM((ny, *half), BF16),
@@ -345,64 +359,66 @@
         compiler_params=pltpu.CompilerParams(collective_id=0, has_side_effects=True),
         cost_estimate=pl.CostEstimate(flops=30_000_000_000, bytes_accessed=4_000_000, transcendentals=0),
         name="entry_state",
-    )(trans, inject, xn)
-
-
-def parts_kernel(
-    me_ref, qt_ref, ol_ref, state_ref, gain_ref, w_ref, x_ref, gate_ref, up_ref, down_ref, *out_refs
-):
-    heads, tile, _ = qt_ref.shape
+    )(trans, inject)
+
+
+def parts_kernel(peers, me_ref, qt_ref, ol_ref, state_ref, gain_ref, w_ref, *refs):
+    hbm, refs = refs[: peers + 3], refs[peers + 3 :]
+    out_refs, (x, gate, up, down, sems) = refs[:peers], refs[peers:]
+    heads, rows, _ = qt_ref.shape
+    tile = rows // peers
+    spots = [x.at[r * tile : (r + 1) * tile] for r in range(peers)] + [gate, up, down]
+    copies = [
+        pltpu.make_async_copy(src, dst, sems.at[k]) for k, (src, dst) in enumerate(zip(hbm, spots))
+    ]
+    for copy in copies:
+        copy.start()
+    turns = [
+        pl.ds(pl.multiple_of(lax.rem(me_ref[0] + r, peers) * tile, tile), tile)
+        for r in range(peers)
+    ]
     normed = []
     for h in range(heads):
-        out = dot3(qt_ref[h], state_ref[h]) + ol_ref[h]
+        qt = jnp.concatenate([qt_ref[h, at, :] for at in turns], 0)
+        ol = jnp.concatenate([ol_ref[h, at, :] for at in turns], 0)
+        out = dot3(qt, state_ref[h]) + ol
         out = out * lax.rsqrt(jnp.mean(out * out, axis=1, keepdims=True) + EPS) * gain_ref[...]
         normed.append(out.astype(BF16))
     mixer = mm(jnp.concatenate(normed, 1), w_ref[...]).astype(BF16)
-    x = x_ref[0]
-    hidden = gated(mm(x, gate_ref[...]), mm(x, up_ref[...]))
-    shared = mm(hidden, down_ref[...]).astype(BF16)
-    for r, out_ref in enumerate(out_refs):
-
-        @pl.when(pl.program_id(0) == r)
-        def _():
-            out_ref[:tile] = mixer
-            out_ref[tile:] = shared
-
-
-def parts_for_peers(me, peers, qt, ol, state, gain, w, group, gate, up, down):
-    heads, rows, d = qt.shape
+    for r in range(peers):
+        out_refs[r][:tile] = mixer[r * tile : (r + 1) * tile]
+    for copy in copies:
+        copy.wait()
+    hidden = gated(mm(x[...], gate[...]), mm(x[...], up[...]))
+    shared = mm(hidden, down[...]).astype(BF16)
+    for r in range(peers):
+        out_refs[r][tile:] = shared[r * tile : (r + 1) * tile]
+
+
+def parts_for_peers(me, qt, ol, state, gain, w, tokens, gate, up, down):
+    _, rows, d = qt.shape
     width = w.shape[1]
+    peers = len(tokens)
     tile = rows // peers
-
-    def whole(x):
-        return pl.BlockSpec(x.shape, lambda r, me: (0,) * x.ndim)
-
-    def turn(r, me):
-        return lax.rem(me[0] + r, peers)
-
-    gain = gain.reshape(1, d)
+    vmem = pl.BlockSpec(memory_space=pltpu.VMEM)
+    kept = (*tokens, gate, up, down)
     return pl.pallas_call(
-        parts_kernel,
-        grid_spec=pltpu.PrefetchScalarGridSpec(
-            num_scalar_prefetch=1,
-            grid=(peers,),
-            in_specs=[
-                pl.BlockSpec((heads, tile, d), lambda r, me: (0, turn(r, me), 0)),
-                pl.BlockSpec((heads, tile, d), lambda r, me: (0, turn(r, me), 0)),
-                whole(state),
-                whole(gain),
-                whole(w),
-                pl.BlockSpec((1, tile, group.shape[2]), lambda r, me: (turn(r, me), 0, 0)),
-                whole(gate),
-                whole(up),
-                whole(down),
-            ],
-            out_specs=[pl.BlockSpec((2 * tile, width), lambda r, me: (0, 0))] * peers,
-        ),
+        functools.partial(parts_kernel, peers),
+        in_specs=[pl.BlockSpec(memory_space=pltpu.SMEM)]
+        + [vmem] * 5
+        + [pl.BlockSpec(memory_space=pl.ANY)] * len(kept),
+        out_specs=[vmem] * peers,
         out_shape=[jax.ShapeDtypeStruct((2 * tile, width), BF16)] * peers,
+        scratch_shapes=[
+            pltpu.VMEM((rows, width), BF16),
+            pltpu.VMEM(gate.shape, BF16),
+            pltpu.VMEM(up.shape, BF16),
+            pltpu.VMEM(down.shape, BF16),
+            pltpu.SemaphoreType.DMA((len(kept),)),
+        ],
         cost_estimate=pl.CostEstimate(flops=6_000_000_000, bytes_accessed=12_000_000, transcendentals=0),
         name="parts_for_peers",
-    )(me, qt, ol, state, gain, w, group, gate, up, down)
+    )(me, qt, ol, state, gain.reshape(1, d), w, *kept)
 
 
 def near_experts_kernel(in_ref, *refs):
@@ -428,15 +444,9 @@
     for m in range(shards_):
         for copy in copies[m]:
             copy.wait()
-
-        def one(t, carry):
-            at = pl.ds(pl.multiple_of(t * tile, tile), tile)
-            x = x_ref[at, :]
-            part = mm(gated(mm(x, gates[m]), mm(x, ups[m])), downs[m])
-            out_ref[at, :] = part if m == 0 else out_ref[at, :] + part
-            return carry
-
-        lax.fori_loop(0, rows // tile, one, 0)
+        x = x_ref[...]
+        part = mm(gated(mm(x, gates[m]), mm(x, ups[m])), downs[m])
+        out_ref[...] = part if m == 0 else out_ref[...] + part
 
 
 def near_experts(spread_in, shards_):
@@ -477,19 +487,16 @@
     ]
     for k in (1, 2, 3, 4, 0):
         copies[k].start()
-    for k in (1, 2, 3, 4, 0):
+    for k in (1, 2, 3):
         copies[k].wait()
-
-    def one(t, carry):
-        at = pl.ds(pl.multiple_of(t * tile, tile), tile)
-        x = x_ref[at, :]
-        total = near[at, :] + mm(gated(mm(x, gate[...]), mm(x, up[...])), down[...])
-        spread(wide, tile, 0, total)
-        spot = pl.ds(pl.multiple_of(t * (tile * cuts), tile * cuts), tile * cuts)
-        out_ref[spot, :] = wide[...].astype(BF16)
-        return carry
-
-    lax.fori_loop(0, rows // tile, one, 0)
+    x = x_ref[...]
+    hidden = gated(mm(x, gate[...]), mm(x, up[...]))
+    for k in (4, 0):
+        copies[k].wait()
+    for t in range(rows // tile):
+        at = slice(t * tile, (t + 1) * tile)
+        spread(wide, tile, 0, near[at, :] + mm(hidden[at], down[...]))
+        out_ref[t * tile * cuts : (t + 1) * tile * cuts, :] = wide[...].astype(BF16)
 
 
 def far_expert(x, near, gate, up0, up1, down):
@@ -700,7 +707,13 @@
         parts = x.reshape(experts, -1, LANES)
         return lax.all_to_all(parts, EP, split_axis=0, concat_axis=0, tiled=True).reshape(-1, LANES)
 
+    peers = lax.axis_size("tp")
+
+    def shift(r):
+        return [(i, (i + r) % peers) for i in range(peers)]
+
     arrived = to_peers(outgoing)
+    group = [xn] + [lax.ppermute(xn, "tp", shift(peers - r)) for r in range(1, peers)]
 
     qt, ol, trans, inject = local_mixer(
         queries,
@@ -711,13 +724,12 @@
         head_decay_speed,
         position_log_decay.T,
     )
-    state, group = entry_state(trans, inject, xn)
+    state = entry_state(trans, inject)
     state, from_left, from_right = lax.optimization_barrier((state, from_left, from_right))
     far = far_shard(from_left, from_right, "tp")
     me = lax.axis_index("tp").astype(jnp.int32).reshape(1)
     parts = parts_for_peers(
         me,
-        lax.axis_size("tp"),
         qt,
         ol,
         state,
@@ -729,11 +741,9 @@
         common_down_weight,
     )
     rows, near = near_experts(arrived, (own, from_left, from_right))
-    parts, near = lax.optimization_barrier((parts, near))
-    peers = lax.axis_size("tp")
+    parts, far, near = lax.optimization_barrier((parts, far, near))
     got = [parts[0]] + [
-        lax.ppermute(parts[r], "tp", [(i, (i + r) % peers) for i in range(peers)])
-        for r in range(1, peers)
+        lax.ppermute(parts[r], "tp", shift(r)) for r in range(1, peers)
     ]
     slot_sums = far_expert(rows, near, *far)
     back = to_peers(slot_sums)

time: 225 us -> 227 us (level)
  waiting for transfers between devices: 48.9 us -> 88 us
  Pallas kernels: 121 us -> 85.6 us
    ppermute x3, waiting for transfers between devices: 0.01 us -> 29.6 us  [neighbours_shards(): from_left = [lax.ppermute(w, axis, right) for w in shard]]
    pallas_call x1, Pallas kernels: 32 us -> 13.7 us  [local_mixer(): pl.pallas_call(local_mixer_kernel, grid=(heads,), in_specs=[by_head, by_h...]
    pallas_call x2, Pallas kernels: 57.7 us -> 44.4 us  [the longest x1 35.9 us: entry_state(): pl.pallas_call(entry_state_kernel, in_specs=[vmem, vmem], out_specs=vmem,...]
    ppermute x1, waiting for transfers between devices: 4.07 us -> 11.8 us  [far_shard(): lax.ppermute(from_left[1][:half], axis, right)]
    ppermute x3 -> x6, waiting for transfers between devices: 44.8 us -> 46.6 us  [the longest x3 46.6 us: shards(): lax.ppermute(parts[r], 'tp', shift(r))]
    ppermute x3 -> x6, starting transfers between devices: 5.79 us -> 7.26 us  [the longest x3 3.95 us: shards(): lax.ppermute(xn, 'tp', shift(peers - r))]
  transfers between devices with their start and end apart: 15 -> 18, of which waited for: 3 -> 5; matrix products, arithmetic and copies ran while one was open for 2% -> 2% of each run, Pallas kernels for 48% -> 33%
where the time goes in v1:
time: 227 us; the launch traced here: 226 us
  waiting for transfers between devices  88 us (39%)
  Pallas kernels  85.6 us (38%)
  starting transfers between devices  43.8 us (19%)
  local copies, waits for them, and re-layouts  8.21 us (4%)
    ppermute x3, waiting for transfers between devices, shards(): lax.ppermute(parts[r], 'tp', shift(r))  46.6 us
    pallas_call x1, Pallas kernels, entry_state(): pl.pallas_call(entry_state_kernel, in_specs=[vmem, vmem], out_specs=vmem,...  35.9 us
    ppermute x3, waiting for transfers between devices, neighbours_shards(): from_left = [lax.ppermute(w, axis, right) for w in shard]  29.6 us
    all_to_all x2, starting transfers between devices, to_peers(): lax.all_to_all(parts, EP, split_axis=0, concat_axis=0, tiled=True)  20.6 us
    pallas_call x1, Pallas kernels, local_mixer(): pl.pallas_call(local_mixer_kernel, grid=(heads,), in_specs=[by_head, by_h...  13.7 us
    ppermute x1, waiting for transfers between devices, far_shard(): lax.ppermute(from_left[1][:half], axis, right)  11.8 us
    pallas_call x1, Pallas kernels, near_experts(): pl.pallas_call(near_experts_kernel, in_specs=[vmem] + [pl.BlockSpec(memor...  9.29 us
    pallas_call x1, Pallas kernels, parts_for_peers(): pl.pallas_call(functools.partial(parts_kernel, peers), in_specs=[pl.Block...  8.45 us
  transfers between devices with their start and end apart: 18, of which 5 were waited for; matrix products, arithmetic and copies ran while one was open for 2% of the time, Pallas kernels for 33%

profile of v1, /device:TPU:8, one launch (start us, length us, event | category | flops | bytes accessed | tf_op | source)
XLA Modules:
  0.0 226.3 jit_solution(18331687746289476599)
XLA Ops:
  0.6 1.6 collective-permute-start
  2.2 1.7 collective-permute-start.3
  3.9 0.3 collective-permute-start.1
  4.2 3.0 %collective-permute-start.4 = (bf16[2048,256]{1,0:T(8,128)(2,1)}, bf16[2048,256]{1,0:T(8,128)(2,1)}, u32[]{:S(2)}, u32[]{:S(2)}) collective-permute-start(bf16[2048,256]{1,0:T(8,128)(2,1)} %bitcast.28), channel_id=1, source_target_pairs={{0,3},{1,0},{2,1},{3,2},{4,7},{5,4},{6,5},{7,6},{8,11},{9,8},{10,9... | collective-permute-start | bytes 3145736 | tf_op jit(solution)/shard_map/ppermute | solution.py:651
  7.2 0.0 collective-permute-start.2
  7.2 3.8 %dispatch.1 = (bf16[128,2048]{1,0:T(8,128)(2,1)}, bf16[6144,128]{1,0:T(8,128)(2,1)}, f32[128,384]{1,0:T(8,128)}) custom-call(bf16[128,2048]{1,0:T(8,128)(2,1)} %x_ref.1, f32[1,2048]{1,0:T(1,128)} %bitcast.20, s32[2,128]{1,0:T(2,128)} %bitcast.21, f32[2,128]{1,0:T(2,128)} %bitcast.22), custom_call_target="tpu_custom_call" | custom-call | tf_op jit(solution)/shard_map/dispatch/pallas_call | solution.py:565
  11.0 12.2 %all-to-all-start = ((bf16[64,96,128]{2,1,0:T(8,128)(2,1)}), bf16[64,96,128]{2,1,0:T(8,128)(2,1)S(1)}, u32[]{:S(2)}, u32[]{:S(2)}) async-start(bf16[64,96,128]{2,1,0:T(8,128)(2,1)} %bitcast.19), calls=%async_computation | async-start | bytes 3145728 | tf_op jit(solution)/shard_map/all_to_all | solution.py:708
  23.3 0.7 copy.21.speed_ref
  23.9 13.7 %local_mixer.1 = (f32[3,512,128]{2,1,0:T(8,128)}, f32[3,512,128]{2,1,0:T(8,128)}, f32[3,128,128]{2,1,0:T(8,128)}, f32[3,128,128]{2,1,0:T(8,128)}) custom-call(bf16[512,384]{1,0:T(8,128)(2,1)} %q_ref.1, bf16[512,384]{1,0:T(8,128)(2,1)} %k_ref.1, bf16[512,384]{1,0:T(8,128)(2,1)} %v_ref.1, f32[3,512]{1,0:T(4,128)} %bitcast.33, bf16[3,512]{1,0:T(4,128)(2,1)} %bitcast.35, ...), custom_call_target="tpu_custom_call" | custom-call | flops 30000001024 | bytes 4000000 | tf_op jit(solution)/shard_map/local_mixer/pallas_call | solution.py:177
  37.6 3.3 %collective-permute-start.5 = (bf16[256,2048]{1,0:T(8,128)(2,1)}, bf16[256,2048]{1,0:T(8,128)(2,1)}, u32[]{:S(2)}, u32[]{:S(2)}) collective-permute-start(bf16[256,2048]{1,0:T(8,128)(2,1)} %bitcast.31), channel_id=1, source_target_pairs={{0,3},{1,0},{2,1},{3,2},{4,7},{5,4},{6,5},{7,6},{8,11},{9,8},{10,9... | collective-permute-start | bytes 3145736 | tf_op jit(solution)/shard_map/ppermute | solution.py:651
  40.9 9.7 %collective-permute-done.1.refs_4_ = bf16[2048,256]{1,0:T(8,128)(2,1)S(1)} collective-permute-done((bf16[2048,256]{1,0:T(8,128)(2,1)}, bf16[2048,256]{1,0:T(8,128)(2,1)S(1)}, u32[]{:S(2)}, u32[]{:S(2)}) %collective-permute-start.1) | collective-permute-done | bytes 1048608 | tf_op jit(solution)/shard_map/ppermute | solution.py:650
  50.6 1.5 collective-permute-start.6
  52.2 19.9 %collective-permute-done.2.refs_5_ = bf16[256,2048]{1,0:T(8,128)(2,1)} collective-permute-done((bf16[256,2048]{1,0:T(8,128)(2,1)}, bf16[256,2048]{1,0:T(8,128)(2,1)}, u32[]{:S(2)}, u32[]{:S(2)}) %collective-permute-start.2) | collective-permute-done | bytes 1048608 | tf_op jit(solution)/shard_map/ppermute | solution.py:650
  72.1 1.8 collective-permute-start.7
  73.9 0.0 collective-permute-done.3.refs_6_
  73.9 0.6 collective-permute-start.8
  74.5 35.9 %entry_state.1.state_ref = f32[3,128,128]{2,1,0:T(8,128)} custom-call(f32[3,128,128]{2,1,0:T(8,128)} %get-tuple-element.33.t_ref, f32[3,128,128]{2,1,0:T(8,128)} %get-tuple-element.34.i_ref), custom_call_target="tpu_custom_call" | custom-call | flops 30000001024 | bytes 4000000 | tf_op jit(solution)/shard_map/entry_state/pallas_call | solution.py:345
  110.4 0.0 collective-permute-done.4.refs_7_
  110.5 0.0 collective-permute-done.5.refs_8_
  110.5 2.7 %collective-permute-start.12 = (bf16[256,2048]{1,0:T(8,128)(2,1)}, bf16[256,2048]{1,0:T(8,128)(2,1)S(1)}, u32[]{:S(2)}, u32[]{:S(2)}) collective-permute-start(bf16[256,2048]{1,0:T(8,128)(2,1)} %collective-permute-done.5.refs_8_), channel_id=1, source_target_pairs={{0,3},{1,0},{2,1},{3,2},{4,7},{5,4},{6,5},{7,6},{8,11},{9,8},{10,9... | collective-permute-start | bytes 3145736 | tf_op jit(solution)/shard_map/ppermute | solution.py:662
  113.2 1.9 slice.6
  115.1 1.9 slice.7
  116.9 0.0 collective-permute-done.6.refs_1_
  116.9 0.5 collective-permute-start.10
  117.4 0.0 collective-permute-done.7.refs_2_
  117.4 2.8 %collective-permute-start.11 = (bf16[1024,256]{1,0:T(8,128)(2,1)}, bf16[1024,256]{1,0:T(8,128)(2,1)}, u32[]{:S(2)}, u32[]{:S(2)}) collective-permute-start(bf16[1024,256]{1,0:T(8,128)(2,1)} %slice.7), channel_id=1, source_target_pairs={{0,3},{1,0},{2,1},{3,2},{4,7},{5,4},{6,5},{7,6},{8,11},{9,8},{10,9... | collective-permute-start | bytes 1572872 | tf_op jit(solution)/shard_map/ppermute | solution.py:661
  120.3 0.0 collective-permute-done.8.refs_3_
  120.3 8.4 %parts_for_peers.1 = (bf16[256,2048]{1,0:T(8,128)(2,1)}, bf16[256,2048]{1,0:T(8,128)(2,1)}, bf16[256,2048]{1,0:T(8,128)(2,1)}, bf16[256,2048]{1,0:T(8,128)(2,1)}) custom-call(s32[1]{0:T(128)} %bitcast.me_ref, f32[3,512,128]{2,1,0:T(8,128)} %get-tuple-element.31.qt_ref, f32[3,512,128]{2,1,0:T(8,128)} %get-tuple-element.32.ol_ref, ...), custom_call_target="tpu_custom_call" | custom-call | flops 6000000000 | bytes 12000000 | tf_op jit(solution)/shard_map/parts_for_peers/pallas_call | solution.py:405
  128.7 1.2 copy-done.2
  129.9 9.3 %near_experts.1 = (bf16[384,2048]{1,0:T(8,128)(2,1)}, f32[384,2048]{1,0:T(8,128)}) custom-call(bf16[6144,128]{1,0:T(8,128)(2,1)} %bitcast.18, bf16[2048,256]{1,0:T(8,128)(2,1)} %bitcast.26, bf16[2048,256]{1,0:T(8,128)(2,1)} %bitcast.29, bf16[256,2048]{1,0:T(8,128)(2,1)} %bitcast.32, bf16[2048,256]{1,0:T(8,128)(2,1)} %collective-permute-done.refs_3_, ...), custom_call_target="tpu_custom_call" | custom-call | flops 5000000000 | bytes 16000000 | tf_op jit(solution)/shard_map/near_experts/pallas_call | solution.py:458
  139.2 11.8 %collective-permute-done.10.refs_1_ = bf16[1024,256]{1,0:T(8,128)(2,1)S(1)} collective-permute-done((bf16[1024,256]{1,0:T(8,128)(2,1)}, bf16[1024,256]{1,0:T(8,128)(2,1)S(1)}, u32[]{:S(2)}, u32[]{:S(2)}) %collective-permute-start.10) | collective-permute-done | bytes 524320 | tf_op jit(solution)/shard_map/ppermute | solution.py:660
  151.0 0.0 collective-permute-done.11.refs_2_
  151.0 0.0 collective-permute-done.12.refs_3_
  151.0 0.8 copy-done.4
  151.8 0.4 copy-done.3
  152.2 6.9 %far_expert.1 = bf16[6144,128]{1,0:T(8,128)(2,1)} custom-call(bf16[384,2048]{1,0:T(8,128)(2,1)} %get-tuple-element.53.x_ref, f32[384,2048]{1,0:T(8,128)} %get-tuple-element.54.near_ref, bf16[2048,256]{1,0:T(8,128)(2,1)} %collective-permute-done.9.refs_0_, bf16[1024,256]{1,0:T(8,128)(2,1)} %copy-done.4, bf16[1024,256]{1,0:T(8,128)(2,1)} %collective-permute-done.11.refs_2_, ...), custom_call_target="tpu_custom_call" | custom-call | flops 2000000000 | bytes 12000000 | tf_op jit(solution)/shard_map/far_expert/pallas_call | solution.py:507
  159.1 8.4 %all-to-all-start.1 = ((bf16[64,96,128]{2,1,0:T(8,128)(2,1)}), bf16[64,96,128]{2,1,0:T(8,128)(2,1)S(1)}, u32[]{:S(2)}, u32[]{:S(2)}) async-start(bf16[64,96,128]{2,1,0:T(8,128)(2,1)} %bitcast.16), calls=%async_computation.1 | async-start | bytes 3145728 | tf_op jit(solution)/shard_map/all_to_all | solution.py:708
  167.4 0.1 collective-permute-start.13
  167.5 1.7 collective-permute-start.14
  169.2 1.6 collective-permute-start.15
  170.8 45.8 %collective-permute-done.13.refs_1_ = bf16[256,2048]{1,0:T(8,128)(2,1)S(1)} collective-permute-done((bf16[256,2048]{1,0:T(8,128)(2,1)}, bf16[256,2048]{1,0:T(8,128)(2,1)S(1)}, u32[]{:S(2)}, u32[]{:S(2)}) %collective-permute-start.13) | collective-permute-done | bytes 1048608 | tf_op jit(solution)/shard_map/ppermute | solution.py:746
  216.6 0.0 collective-permute-done.14.refs_2_
  216.6 0.7 collective-permute-done.15.refs_3_
  217.3 0.2 copy-done.1
  217.6 2.6 %mixer_sum.1 = bf16[128,2048]{1,0:T(8,128)(2,1)} custom-call(bf16[256,2048]{1,0:T(8,128)(2,1)} %get-tuple-element.49.refs_0_, bf16[256,2048]{1,0:T(8,128)(2,1)} %copy-done.1, bf16[256,2048]{1,0:T(8,128)(2,1)} %collective-permute-done.14.refs_2_, bf16[256,2048]{1,0:T(8,128)(2,1)} %collective-permute-done.15.refs_3_), custom_call_target="tpu_custom_call" | custom-call | flops 1000000000 | bytes 3000000 | tf_op jit(solution)/shard_map/mixer_sum/pallas_call | solution.py:588
  220.1 0.0 all-to-all-done.1
  220.1 1.2 copy-done
  221.3 5.0 %combine.1 = bf16[128,2048]{1,0:T(8,128)(2,1)} custom-call(bf16[256,2048]{1,0:T(8,128)(2,1)} %get-tuple-element.49.refs_0_, bf16[256,2048]{1,0:T(8,128)(2,1)} %copy-done.1, bf16[256,2048]{1,0:T(8,128)(2,1)} %collective-permute-done.14.refs_2_, bf16[256,2048]{1,0:T(8,128)(2,1)} %collective-permute-done.15.refs_3_, bf16[6144,128]{1,0:T(8,128)(2,1)} %bitcast.17, ...), custom_call_target="tpu_custom_call" | custom-call | tf_op jit(solution)/shard_map/combine/pallas_call | solution.py:625
  (13 shorter events, 0.0 us)
Async XLA Ops:
  0.6 37.0 %collective-permute-start = (bf16[2048,256]{1,0:T(8,128)(2,1)}, bf16[2048,256]{1,0:T(8,128)(2,1)}, u32[]{:S(2)}, u32[]{:S(2)}) collective-permute-start(bf16[2048,256]{1,0:T(8,128)(2,1)} %bitcast.24), channel_id=1, source_target_pairs={{0,1},{1,2},{2,3},{3,0},{4,5},{5,6},{6,7},{7,4},{8,9},{9,10},{10,1... | collective-permute-start | bytes 3145736 | tf_op jit(solution)/shard_map/ppermute | solution.py:650
  2.2 71.7 %collective-permute-start.3 = (bf16[2048,256]{1,0:T(8,128)(2,1)}, bf16[2048,256]{1,0:T(8,128)(2,1)}, u32[]{:S(2)}, u32[]{:S(2)}) collective-permute-start(bf16[2048,256]{1,0:T(8,128)(2,1)} %bitcast.25), channel_id=1, source_target_pairs={{0,3},{1,0},{2,1},{3,2},{4,7},{5,4},{6,5},{7,6},{8,11},{9,8},{10,9... | collective-permute-start | bytes 3145736 | tf_op jit(solution)/shard_map/ppermute | solution.py:651
  3.9 46.7 %collective-permute-start.1 = (bf16[2048,256]{1,0:T(8,128)(2,1)}, bf16[2048,256]{1,0:T(8,128)(2,1)S(1)}, u32[]{:S(2)}, u32[]{:S(2)}) collective-permute-start(bf16[2048,256]{1,0:T(8,128)(2,1)} %bitcast.27), channel_id=1, source_target_pairs={{0,1},{1,2},{2,3},{3,0},{4,5},{5,6},{6,7},{7,4},{8,9},{9,10},{10,1... | collective-permute-start | bytes 3145736 | tf_op jit(solution)/shard_map/ppermute | solution.py:650
  4.2 106.2 %collective-permute-start.4 = (bf16[2048,256]{1,0:T(8,128)(2,1)}, bf16[2048,256]{1,0:T(8,128)(2,1)}, u32[]{:S(2)}, u32[]{:S(2)}) collective-permute-start(bf16[2048,256]{1,0:T(8,128)(2,1)} %bitcast.28), channel_id=1, source_target_pairs={{0,3},{1,0},{2,1},{3,2},{4,7},{5,4},{6,5},{7,6},{8,11},{9,8},{10,9... | collective-permute-start | bytes 3145736 | tf_op jit(solution)/shard_map/ppermute | solution.py:651
  7.2 64.9 %collective-permute-start.2 = (bf16[256,2048]{1,0:T(8,128)(2,1)}, bf16[256,2048]{1,0:T(8,128)(2,1)}, u32[]{:S(2)}, u32[]{:S(2)}) collective-permute-start(bf16[256,2048]{1,0:T(8,128)(2,1)} %bitcast.30), channel_id=1, source_target_pairs={{0,1},{1,2},{2,3},{3,0},{4,5},{5,6},{6,7},{7,4},{8,9},{9,10},{10,1... | collective-permute-start | bytes 3145736 | tf_op jit(solution)/shard_map/ppermute | solution.py:650
  11.0 12.2 %copy-start.6 = (f32[3]{0:T(128)S(1)}, f32[3]{0:T(128)}, u32[]{:S(2)}) copy-start(f32[3]{0:T(128)} %param.24) | copy-start | bytes 40
  11.0 117.7 %all-to-all-start = ((bf16[64,96,128]{2,1,0:T(8,128)(2,1)}), bf16[64,96,128]{2,1,0:T(8,128)(2,1)S(1)}, u32[]{:S(2)}, u32[]{:S(2)}) async-start(bf16[64,96,128]{2,1,0:T(8,128)(2,1)} %bitcast.19), calls=%async_computation | async-start | bytes 3145728 | tf_op jit(solution)/shard_map/all_to_all | solution.py:708
  37.6 72.8 %collective-permute-start.5 = (bf16[256,2048]{1,0:T(8,128)(2,1)}, bf16[256,2048]{1,0:T(8,128)(2,1)}, u32[]{:S(2)}, u32[]{:S(2)}) collective-permute-start(bf16[256,2048]{1,0:T(8,128)(2,1)} %bitcast.31), channel_id=1, source_target_pairs={{0,3},{1,0},{2,1},{3,2},{4,7},{5,4},{6,5},{7,6},{8,11},{9,8},{10,9... | collective-permute-start | bytes 3145736 | tf_op jit(solution)/shard_map/ppermute | solution.py:651
  50.6 59.8 %copy-start.5 = (bf16[2048,256]{1,0:T(8,128)(2,1)}, bf16[2048,256]{1,0:T(8,128)(2,1)S(1)}, u32[]{:S(2)}) copy-start(bf16[2048,256]{1,0:T(8,128)(2,1)S(1)} %collective-permute-done.1.refs_4_) | copy-start | bytes 3145732
  50.6 66.3 %collective-permute-start.6 = (bf16[128,2048]{1,0:T(8,128)(2,1)}, bf16[128,2048]{1,0:T(8,128)(2,1)}, u32[]{:S(2)}, u32[]{:S(2)}) collective-permute-start(bf16[128,2048]{1,0:T(8,128)(2,1)} %get-tuple-element.36.refs_0_), channel_id=1, source_target_pairs={{0,3},{1,0},{2,1},{3,2},{4,7},{5,4},{6,5},{7,6},{8,11},{9,8},{10,9... | collective-permute-start | bytes 1572872 | tf_op jit(solution)/shard_map/ppermute | solution.py:716
  72.1 45.3 %collective-permute-start.7 = (bf16[128,2048]{1,0:T(8,128)(2,1)}, bf16[128,2048]{1,0:T(8,128)(2,1)}, u32[]{:S(2)}, u32[]{:S(2)}) collective-permute-start(bf16[128,2048]{1,0:T(8,128)(2,1)} %get-tuple-element.36.refs_0_), channel_id=1, source_target_pairs={{0,2},{1,3},{2,0},{3,1},{4,6},{5,7},{6,4},{7,5},{8,10},{9,11},{10,... | collective-permute-start | bytes 1572872 | tf_op jit(solution)/shard_map/ppermute | solution.py:716
  73.9 46.4 %collective-permute-start.8 = (bf16[128,2048]{1,0:T(8,128)(2,1)}, bf16[128,2048]{1,0:T(8,128)(2,1)}, u32[]{:S(2)}, u32[]{:S(2)}) collective-permute-start(bf16[128,2048]{1,0:T(8,128)(2,1)} %get-tuple-element.36.refs_0_), channel_id=1, source_target_pairs={{0,1},{1,2},{2,3},{3,0},{4,5},{5,6},{6,7},{7,4},{8,9},{9,10},{10,1... | collective-permute-start | bytes 1572872 | tf_op jit(solution)/shard_map/ppermute | solution.py:716
  110.5 40.5 %collective-permute-start.12 = (bf16[256,2048]{1,0:T(8,128)(2,1)}, bf16[256,2048]{1,0:T(8,128)(2,1)S(1)}, u32[]{:S(2)}, u32[]{:S(2)}) collective-permute-start(bf16[256,2048]{1,0:T(8,128)(2,1)} %collective-permute-done.5.refs_8_), channel_id=1, source_target_pairs={{0,3},{1,0},{2,1},{3,2},{4,7},{5,4},{6,5},{7,6},{8,11},{9,8},{10,9... | collective-permute-start | bytes 3145736 | tf_op jit(solution)/shard_map/ppermute | solution.py:662
  113.2 37.8 %collective-permute-start.9 = (bf16[2048,256]{1,0:T(8,128)(2,1)}, bf16[2048,256]{1,0:T(8,128)(2,1)}, u32[]{:S(2)}, u32[]{:S(2)}) collective-permute-start(bf16[2048,256]{1,0:T(8,128)(2,1)} %collective-permute-done.refs_3_), channel_id=1, source_target_pairs={{0,1},{1,2},{2,3},{3,0},{4,5},{5,6},{6,7},{7,4},{8,9},{9,10},{10,1... | collective-permute-start | bytes 3145736 | tf_op jit(solution)/shard_map/ppermute | solution.py:659
  116.9 34.0 %collective-permute-start.10 = (bf16[1024,256]{1,0:T(8,128)(2,1)}, bf16[1024,256]{1,0:T(8,128)(2,1)S(1)}, u32[]{:S(2)}, u32[]{:S(2)}) collective-permute-start(bf16[1024,256]{1,0:T(8,128)(2,1)} %slice.6), channel_id=1, source_target_pairs={{0,1},{1,2},{2,3},{3,0},{4,5},{5,6},{6,7},{7,4},{8,9},{9,10},{10,1... | collective-permute-start | bytes 1572872 | tf_op jit(solution)/shard_map/ppermute | solution.py:660
  117.4 33.6 %collective-permute-start.11 = (bf16[1024,256]{1,0:T(8,128)(2,1)}, bf16[1024,256]{1,0:T(8,128)(2,1)}, u32[]{:S(2)}, u32[]{:S(2)}) collective-permute-start(bf16[1024,256]{1,0:T(8,128)(2,1)} %slice.7), channel_id=1, source_target_pairs={{0,3},{1,0},{2,1},{3,2},{4,7},{5,4},{6,5},{7,6},{8,11},{9,8},{10,9... | collective-permute-start | bytes 1572872 | tf_op jit(solution)/shard_map/ppermute | solution.py:661
  128.7 1.2 copy-start.2
  151.0 0.8 copy-start.4
  151.0 1.2 copy-start.3
  159.1 61.1 %all-to-all-start.1 = ((bf16[64,96,128]{2,1,0:T(8,128)(2,1)}), bf16[64,96,128]{2,1,0:T(8,128)(2,1)S(1)}, u32[]{:S(2)}, u32[]{:S(2)}) async-start(bf16[64,96,128]{2,1,0:T(8,128)(2,1)} %bitcast.16), calls=%async_computation.1 | async-start | bytes 3145728 | tf_op jit(solution)/shard_map/all_to_all | solution.py:708
  167.4 49.1 %collective-permute-start.13 = (bf16[256,2048]{1,0:T(8,128)(2,1)}, bf16[256,2048]{1,0:T(8,128)(2,1)S(1)}, u32[]{:S(2)}, u32[]{:S(2)}) collective-permute-start(bf16[256,2048]{1,0:T(8,128)(2,1)} %get-tuple-element.50), channel_id=1, source_target_pairs={{0,1},{1,2},{2,3},{3,0},{4,5},{5,6},{6,7},{7,4},{8,9},{9,10},{10,1... | collective-permute-start | bytes 3145736 | tf_op jit(solution)/shard_map/ppermute | solution.py:746
  167.5 49.1 %collective-permute-start.14 = (bf16[256,2048]{1,0:T(8,128)(2,1)}, bf16[256,2048]{1,0:T(8,128)(2,1)}, u32[]{:S(2)}, u32[]{:S(2)}) collective-permute-start(bf16[256,2048]{1,0:T(8,128)(2,1)} %get-tuple-element.51), channel_id=1, source_target_pairs={{0,2},{1,3},{2,0},{3,1},{4,6},{5,7},{6,4},{7,5},{8,10},{9,11},{10,... | collective-permute-start | bytes 3145736 | tf_op jit(solution)/shard_map/ppermute | solution.py:746
  169.2 48.1 %collective-permute-start.15 = (bf16[256,2048]{1,0:T(8,128)(2,1)}, bf16[256,2048]{1,0:T(8,128)(2,1)}, u32[]{:S(2)}, u32[]{:S(2)}) collective-permute-start(bf16[256,2048]{1,0:T(8,128)(2,1)} %get-tuple-element.52), channel_id=1, source_target_pairs={{0,3},{1,0},{2,1},{3,2},{4,7},{5,4},{6,5},{7,6},{8,11},{9,8},{10,9... | collective-permute-start | bytes 3145736 | tf_op jit(solution)/shard_map/ppermute | solution.py:746
  216.6 1.0 copy-start.1
  220.1 1.2 copy-start

commit v2 on v1

--- a/solution.py
+++ b/solution.py
@@ -18,6 +18,7 @@
 BF16 = jnp.bfloat16
 LANES = 128
 MESH = pl.DeviceIdType.MESH
+ALL_VMEM = pltpu.CompilerParams(vmem_limit_bytes=67_043_328)
 
 
 def halves(x):
@@ -205,6 +206,7 @@
             jax.ShapeDtypeStruct((heads, d, d), F32),
         ],
         cost_estimate=pl.CostEstimate(flops=30_000_000_000, bytes_accessed=4_000_000, transcendentals=0),
+        compiler_params=ALL_VMEM,
         name="local_mixer",
     )(queries, keys, values, gate, corr, speed.reshape(heads, 1), plog)
 
@@ -356,7 +358,9 @@
             dma((max(ny - 1, 1),)), dma((max(ny - 1, 1),)), dma((max(ny - 1, 1),)), dma((max(ny - 1, 1),)),
             *[dma((rounds, heads)) for _ in range(8)],
         ],
-        compiler_params=pltpu.CompilerParams(collective_id=0, has_side_effects=True),
+        compiler_params=pltpu.CompilerParams(
+            collective_id=0, has_side_effects=True, vmem_limit_bytes=67_043_328
+        ),
         cost_estimate=pl.CostEstimate(flops=30_000_000_000, bytes_accessed=4_000_000, transcendentals=0),
         name="entry_state",
     )(trans, inject)
@@ -417,13 +421,14 @@
             pltpu.SemaphoreType.DMA((len(kept),)),
         ],
         cost_estimate=pl.CostEstimate(flops=6_000_000_000, bytes_accessed=12_000_000, transcendentals=0),
+        compiler_params=ALL_VMEM,
         name="parts_for_peers",
     )(me, qt, ol, state, gain.reshape(1, d), w, *kept)
 
 
 def near_experts_kernel(in_ref, *refs):
     shards_ = len(refs) // 3 - 2
-    hbm, (x_ref, out_ref, wide, gates, ups, downs) = refs[: 3 * shards_], refs[3 * shards_ : -1]
+    hbm, (x_ref, out_ref, gates, ups, downs) = refs[: 3 * shards_], refs[3 * shards_ : -1]
     sems = refs[-1]
     rows, width = x_ref.shape
     cuts = width // LANES
@@ -439,8 +444,9 @@
         for copy in shard:
             copy.start()
     for t in range(rows // tile):
-        wide[...] = in_ref[t * tile * cuts : (t + 1) * tile * cuts, :].astype(F32)
-        x_ref[t * tile : (t + 1) * tile, :] = gathered(wide, tile, cuts)
+        x_ref[t * tile : (t + 1) * tile, :] = gathered(
+            in_ref[t * tile * cuts : (t + 1) * tile * cuts, :], cuts
+        )
     for m in range(shards_):
         for copy in copies[m]:
             copy.wait()
@@ -464,77 +470,127 @@
             jax.ShapeDtypeStruct((rows, width), F32),
         ],
         scratch_shapes=[
-            pltpu.VMEM((128 * width // LANES, LANES), F32),
             pltpu.VMEM((count, width, hidden), BF16),
             pltpu.VMEM((count, width, hidden), BF16),
             pltpu.VMEM((count, hidden, width), BF16),
             pltpu.SemaphoreType.DMA((count, 3)),
         ],
         cost_estimate=pl.CostEstimate(flops=5_000_000_000, bytes_accessed=16_000_000, transcendentals=0),
+        compiler_params=ALL_VMEM,
         name="near_experts",
     )(spread_in, *weights)
 
 
-def far_expert_kernel(x_ref, near_ref, *refs):
-    hbm, (out_ref, wide, near, gate, up, down, sems) = (near_ref, *refs[:4]), refs[4:]
-    half = up.shape[0] // 2
-    rows, width = x_ref.shape
-    cuts = width // LANES
-    tile = 128
-    spots = (near, gate, up.at[:half], up.at[half:], down)
-    copies = [
-        pltpu.make_async_copy(src, dst, sems.at[k]) for k, (src, dst) in enumerate(zip(hbm, spots))
-    ]
-    for k in (1, 2, 3, 4, 0):
-        copies[k].start()
-    for k in (1, 2, 3):
-        copies[k].wait()
+def far_hidden_kernel(x_ref, gate_ref, up_ref, out_ref):
     x = x_ref[...]
-    hidden = gated(mm(x, gate[...]), mm(x, up[...]))
-    for k in (4, 0):
-        copies[k].wait()
-    for t in range(rows // tile):
-        at = slice(t * tile, (t + 1) * tile)
-        spread(wide, tile, 0, near[at, :] + mm(hidden[at], down[...]))
-        out_ref[t * tile * cuts : (t + 1) * tile * cuts, :] = wide[...].astype(BF16)
-
-
-def far_expert(x, near, gate, up0, up1, down):
-    rows, width = x.shape
-    hidden = gate.shape[1]
-    cuts = width // LANES
+    out_ref[...] = gated(mm(x, gate_ref[...]), mm(x, up_ref[...]))
+
+
+def far_hidden(x, gate, up):
     vmem = pl.BlockSpec(memory_space=pltpu.VMEM)
     return pl.pallas_call(
-        far_expert_kernel,
-        in_specs=[vmem] + [pl.BlockSpec(memory_space=pl.ANY)] * 5,
+        far_hidden_kernel,
+        in_specs=[vmem] * 3,
         out_specs=vmem,
+        out_shape=jax.ShapeDtypeStruct((x.shape[0], gate.shape[1]), BF16),
+        cost_estimate=pl.CostEstimate(flops=1_500_000_000, bytes_accessed=4_000_000, transcendentals=0),
+        compiler_params=ALL_VMEM,
+        name="far_hidden",
+    )(x, gate, up)
+
+
+def far_out_kernel(hidden_ref, near_ref, down0_ref, down1_ref, out_ref, near, down, ready, sems):
+    rows, width = near.shape
+    cuts = width // LANES
+    half = down.shape[0] // 2
+    tile = rows // ready.shape[0]
+    spans = [slice(t * tile, (t + 1) * tile) for t in range(ready.shape[0])]
+    loads = [
+        pltpu.make_async_copy(down0_ref, down.at[:half], sems.at[0]),
+        pltpu.make_async_copy(down1_ref, down.at[half:], sems.at[1]),
+    ] + [
+        pltpu.make_async_copy(near_ref.at[at], near.at[at], sems.at[2 + t])
+        for t, at in enumerate(spans)
+    ]
+    for copy in loads:
+        copy.start()
+    for copy in loads[:2]:
+        copy.wait()
+    stores = []
+    for t, at in enumerate(spans):
+        part = mm(hidden_ref[at, :], down[...])
+        loads[2 + t].wait()
+        ready[t] = spread(near[at, :] + part)
+        stores.append(
+            pltpu.make_async_copy(
+                ready.at[t],
+                out_ref.at[t * tile * cuts : (t + 1) * tile * cuts],
+                sems.at[2 + len(spans) + t],
+            )
+        )
+        stores[-1].start()
+    for copy in stores:
+        copy.wait()
+
+
+def far_out(hidden, near, down0, down1):
+    rows, width = near.shape
+    cuts = width // LANES
+    tiles = rows // 128
+    hbm = pl.BlockSpec(memory_space=pl.ANY)
+    return pl.pallas_call(
+        far_out_kernel,
+        in_specs=[pl.BlockSpec(memory_space=pltpu.VMEM), hbm, hbm, hbm],
+        out_specs=hbm,
         out_shape=jax.ShapeDtypeStruct((rows * cuts, LANES), BF16),
         scratch_shapes=[
-            pltpu.VMEM((128 * cuts, LANES), F32),
             pltpu.VMEM((rows, width), F32),
-            pltpu.VMEM((width, hidden), BF16),
-            pltpu.VMEM((width, hidden), BF16),
-            pltpu.VMEM((hidden, width), BF16),
-            pltpu.SemaphoreType.DMA((5,)),
-        ],
-        cost_estimate=pl.CostEstimate(flops=2_000_000_000, bytes_accessed=12_000_000, transcendentals=0),
-        name="far_expert",
-    )(x, near, gate, up0, up1, down)
-
-
-def spread(wide, rows, start, values):
-    cuts = values.shape[1] // LANES
-    for c in range(cuts):
-        wide[pl.ds(start * cuts + c, rows, stride=cuts), :] = values[:, c * LANES : (c + 1) * LANES]
-
-
-def gathered(wide, rows, cuts):
+            pltpu.VMEM((2 * down0.shape[0], width), BF16),
+            pltpu.VMEM((tiles, 128 * cuts, LANES), BF16),
+            pltpu.SemaphoreType.DMA((2 + 2 * tiles,)),
+        ],
+        cost_estimate=pl.CostEstimate(flops=1_500_000_000, bytes_accessed=8_000_000, transcendentals=0),
+        name="far_out",
+    )(hidden, near, down0, down1)
+
+
+def interleaving(cuts, back=False):
+    i = lax.broadcasted_iota(jnp.int32, (8 * cuts, 8 * cuts), 1 if back else 0)
+    j = lax.broadcasted_iota(jnp.int32, (8 * cuts, 8 * cuts), 0 if back else 1)
+    return ((lax.div(i, cuts) == lax.rem(j, 8)) & (lax.rem(i, cuts) == lax.div(j, 8))).astype(BF16)
+
+
+def spread(values):
+    rows, width = values.shape
+    cuts = width // LANES
+    order = interleaving(cuts)
+    blocks = [
+        jnp.concatenate(
+            [values[g : g + 8, c * LANES : (c + 1) * LANES] for c in range(cuts)], 0
+        ).astype(BF16)
+        for g in range(0, rows, 8)
+    ]
+    out = []
+    for g in range(0, len(blocks), 2):
+        two = mm(order, jnp.concatenate(blocks[g : g + 2], 1)).astype(BF16)
+        out += [two[:, :LANES], two[:, LANES:]]
+    return jnp.concatenate(out, 0)
+
+
+def gathered(tall, cuts):
+    order = interleaving(cuts, back=True)
+    size = 8 * cuts
+    blocks = [tall[g : g + size] for g in range(0, tall.shape[0], size)]
+    out = []
+    for g in range(0, len(blocks), 2):
+        two = mm(order, jnp.concatenate(blocks[g : g + 2], 1))
+        out += [two[:, :LANES], two[:, LANES:]]
     return jnp.concatenate(
-        [wide[pl.ds(c, rows, stride=cuts), :].astype(BF16) for c in range(cuts)], 1
-    )
-
-
-def dispatch_kernel(capacity, x_ref, gain_ref, routes_ref, weight_ref, xn_ref, out_ref, mix_ref, wide):
+        [jnp.concatenate([x[c * 8 : (c + 1) * 8] for x in out], 0) for c in range(cuts)], 1
+    ).astype(BF16)
+
+
+def dispatch_kernel(capacity, x_ref, gain_ref, routes_ref, weight_ref, xn_ref, out_ref, mix_ref):
     tokens, width = x_ref.shape
     slots = mix_ref.shape[1]
     x = x_ref[...].astype(F32)
@@ -553,8 +609,7 @@
     for base in range(0, slots, step):
         slot = (lax.broadcasted_iota(jnp.int32, (step, tokens), 0) + base).astype(F32)
         is0, is1 = slot == s0, slot == s1
-        spread(wide, step, 0, mm((is0 | is1).astype(BF16), xn))
-        out_ref[base * cuts : (base + step) * cuts, :] = wide[...].astype(BF16)
+        out_ref[base * cuts : (base + step) * cuts, :] = spread(mm((is0 | is1).astype(BF16), xn))
         mix = jnp.where(is0, weight_ref[0:1, :], 0.0) + jnp.where(is1, weight_ref[1:2, :], 0.0)
         mix_ref[:, base : base + step] = mix.T
 
@@ -569,72 +624,96 @@
             jax.ShapeDtypeStruct((slots * cuts, LANES), BF16),
             jax.ShapeDtypeStruct((tokens, slots), F32),
         ],
-        scratch_shapes=[pltpu.VMEM((128 * cuts, LANES), F32)],
         name="dispatch",
     )(x, gain.reshape(1, width), routes, weight)
 
 
-def mixer_sum_kernel(*refs):
-    *part_refs, out_ref = refs
-    total = part_refs[0][...].astype(F32)
+def sums_kernel(*refs):
+    *part_refs, mixer_ref, shared_ref = refs
+    tokens = mixer_ref.shape[0]
+    mixer, shared = part_refs[0][:tokens].astype(F32), part_refs[0][tokens:].astype(F32)
     for part in part_refs[1:]:
-        total = total + part[...].astype(F32)
-    out_ref[...] = total.astype(BF16)
-
-
-def mixer_sum(parts):
+        mixer = mixer + part[:tokens].astype(F32)
+        shared = shared + part[tokens:].astype(F32)
+    mixer_ref[...] = mixer.astype(BF16)
+    shared_ref[...] = shared
+
+
+def sums_of_parts(parts):
     rows, width = parts[0].shape
-    half = pl.BlockSpec((rows // 2, width), lambda c: (0, 0))
+    tile = 512
+    out = pl.BlockSpec((rows // 2, tile), lambda c: (0, c))
     return pl.pallas_call(
-        mixer_sum_kernel,
-        grid=(1,),
-        in_specs=[half] * len(parts),
-        out_specs=half,
-        out_shape=jax.ShapeDtypeStruct((rows // 2, width), BF16),
-        cost_estimate=pl.CostEstimate(flops=1_000_000_000, bytes_accessed=3_000_000, transcendentals=0),
-        name="mixer_sum",
+        sums_kernel,
+        grid=(width // tile,),
+        in_specs=[pl.BlockSpec((rows, tile), lambda c: (0, c))] * len(parts),
+        out_specs=[out, out],
+        out_shape=[
+            jax.ShapeDtypeStruct((rows // 2, width), BF16),
+            jax.ShapeDtypeStruct((rows // 2, width), F32),
+        ],
+        cost_estimate=pl.CostEstimate(flops=1_000_000_000, bytes_accessed=6_000_000, transcendentals=0),
+        compiler_params=ALL_VMEM,
+        name="sums_of_parts",
     )(*parts)
 
 
-def combine_kernel(*refs):
-    *part_refs, back_ref, mix_ref, out_ref, wide, total = refs
-    rows = mix_ref.shape[1]
-    cuts = total.shape[1] // LANES
-    step = pl.program_id(0)
-
-    @pl.when(step == 0)
-    def _():
-        shared = part_refs[0][...].astype(F32)
-        for part in part_refs[1:]:
-            shared = shared + part[...].astype(F32)
-        total[...] = shared
-
-    wide[...] = back_ref[...].astype(F32)
-    total[...] += dot2(mix_ref[...], gathered(wide, rows, cuts))
-
-    @pl.when(step == pl.num_programs(0) - 1)
-    def _():
-        out_ref[...] = total[...].astype(BF16)
-
-
-def combine(parts, back, mix):
-    tokens, slots = mix.shape
-    width = parts[0].shape[1]
+def combine_kernel(shared_hbm, back_hbm, mix_hbm, out_hbm, shared, back, mix, out, sems):
+    tiles = back.shape[0]
+    width = shared.shape[1]
+    cuts = width // LANES
+    tile = back.shape[1] // cuts
+    loads = [
+        pltpu.make_async_copy(
+            back_hbm.at[t * tile * cuts : (t + 1) * tile * cuts], back.at[t], sems.at[t]
+        )
+        for t in range(tiles)
+    ]
+    loads.insert(1, pltpu.make_async_copy(mix_hbm, mix, sems.at[tiles]))
+    loads.append(pltpu.make_async_copy(shared_hbm, shared, sems.at[tiles + 1]))
+    for copy in loads:
+        copy.start()
+    rows = []
+    for t, count in enumerate((2,) + (1,) * (tiles - 1)):
+        for _ in range(count):
+            loads.pop(0).wait()
+        rows.append(gathered(back[t], cuts))
+    loads.pop(0).wait()
+    rows = jnp.concatenate(rows, 0)
+    hi, lo = halves(mix[...])
+    both = jnp.concatenate([hi, lo], 1)
+    stores = []
+    for k in range(2):
+        at = slice(k * width // 2, (k + 1) * width // 2)
+        part = jnp.concatenate([rows[:, at], rows[:, at]], 0)
+        out[:, at] = (shared[:, at] + mm(both, part)).astype(BF16)
+        stores.append(pltpu.make_async_copy(out.at[:, at], out_hbm.at[:, at], sems.at[tiles + 2 + k]))
+        stores[-1].start()
+    for copy in stores:
+        copy.wait()
+
+
+def combine(shared, back, mix):
+    tokens, width = shared.shape
     cuts = width // LANES
     tile = 128
+    tiles = mix.shape[1] // tile
+    hbm = pl.BlockSpec(memory_space=pl.ANY)
     return pl.pallas_call(
         combine_kernel,
-        grid=(slots // tile,),
-        in_specs=[pl.BlockSpec((tokens, width), lambda c: (1, 0))] * len(parts)
-        + [
-            pl.BlockSpec((tile * cuts, LANES), lambda c: (c, 0)),
-            pl.BlockSpec((tokens, tile), lambda c: (0, c)),
-        ],
-        out_specs=pl.BlockSpec((tokens, width), lambda c: (0, 0)),
+        in_specs=[hbm, hbm, hbm],
+        out_specs=hbm,
         out_shape=jax.ShapeDtypeStruct((tokens, width), BF16),
-        scratch_shapes=[pltpu.VMEM((tile * cuts, LANES), F32), pltpu.VMEM((tokens, width), F32)],
+        scratch_shapes=[
+            pltpu.VMEM((tokens, width), F32),
+            pltpu.VMEM((tiles, tile * cuts, LANES), BF16),
+            pltpu.VMEM(mix.shape, F32),
+            pltpu.VMEM((tokens, width), BF16),
+            pltpu.SemaphoreType.DMA((tiles + 4,)),
+        ],
+        compiler_params=ALL_VMEM,
         name="combine",
-    )(*parts, back, mix)
+    )(shared, back, mix)
 
 
 def ring(axis):
@@ -654,12 +733,12 @@
 
 def far_shard(from_left, from_right, axis):
     right, left = ring(axis)
-    half = from_left[1].shape[0] // 2
+    half = from_left[2].shape[0] // 2
     return (
         lax.ppermute(from_left[0], axis, right),
-        lax.ppermute(from_left[1][:half], axis, right),
-        lax.ppermute(from_right[1][half:], axis, left),
-        lax.ppermute(from_right[2], axis, left),
+        lax.ppermute(from_right[1], axis, left),
+        lax.ppermute(from_left[2][:half], axis, right),
+        lax.ppermute(from_right[2][half:], axis, left),
     )
 
 
@@ -741,13 +820,15 @@
         common_down_weight,
     )
     rows, near = near_experts(arrived, (own, from_left, from_right))
-    parts, far, near = lax.optimization_barrier((parts, far, near))
+    hidden = far_hidden(rows, *far[:2])
+    parts, far, near, hidden = lax.optimization_barrier((parts, far, near, hidden))
     got = [parts[0]] + [
         lax.ppermute(parts[r], "tp", shift(r)) for r in range(1, peers)
     ]
-    slot_sums = far_expert(rows, near, *far)
+    slot_sums = far_out(hidden, near, *far[2:])
     back = to_peers(slot_sums)
-    return (mixer_sum(got), combine(got, back, mix))
+    mixer_out, shared = sums_of_parts(got)
+    return (mixer_out, combine(shared, back, mix))
 
 
 def solution(mesh):

time: 227 us -> 222 us (0.978)
  local copies, waits for them, and re-layouts: 8.21 us -> 4.46 us
  waiting for transfers between devices: 88 us -> 85.1 us
    ppermute x3, waiting for transfers between devices: 11.8 us -> 6.66 us  [the longest x1 6.66 us: far_shard(): lax.ppermute(from_left[2][:half], axis, right)]
    unnamed x14 -> x8, local copies, waits for them, and re-layouts: 3.81 us -> 0.02 us
    ppermute x1, waiting for transfers between devices: 0.01 us -> 2.7 us  [far_shard(): lax.ppermute(from_left[0], axis, right)]
    pallas_call x3 -> x4, Pallas kernels: 14.5 us -> 15.7 us  [the longest x1 4.52 us: far_out(): pl.pallas_call(far_out_kernel, in_specs=[pl.BlockSpec(memory_space=pltpu....]
  transfers between devices with their start and end apart: 18 -> 18, of which waited for: 5 -> 6; matrix products, arithmetic and copies ran while one was open for 2% -> 2% of each run, Pallas kernels for 33% -> 36%
where the time goes in v2:
time: 222 us
  Pallas kernels  86.8 us (39%)
  waiting for transfers between devices  85.1 us (38%)
  starting transfers between devices  44.4 us (20%)
  local copies, waits for them, and re-layouts  4.46 us (2%)
    ppermute x3, waiting for transfers between devices, shards(): lax.ppermute(parts[r], 'tp', shift(r))  46.3 us
    pallas_call x1, Pallas kernels, entry_state(): pl.pallas_call(entry_state_kernel, in_specs=[vmem, vmem], out_specs=vmem,...  35.9 us
    ppermute x3, waiting for transfers between devices, neighbours_shards(): from_left = [lax.ppermute(w, axis, right) for w in shard]  29.5 us
    all_to_all x2, starting transfers between devices, to_peers(): lax.all_to_all(parts, EP, split_axis=0, concat_axis=0, tiled=True)  21.2 us
    pallas_call x1, Pallas kernels, local_mixer(): pl.pallas_call(local_mixer_kernel, grid=(heads,), in_specs=[by_head, by_h...  13.7 us
    pallas_call x1, Pallas kernels, near_experts(): pl.pallas_call(near_experts_kernel, in_specs=[vmem] + [pl.BlockSpec(memor...  9.32 us
    pallas_call x1, Pallas kernels, parts_for_peers(): pl.pallas_call(functools.partial(parts_kernel, peers), in_specs=[pl.Block...  8.39 us
    ppermute x3, starting transfers between devices, neighbours_shards(): from_right = [lax.ppermute(w, axis, left) for w in shard]  8 us
  transfers between devices with their start and end apart: 18, of which 6 were waited for; matrix products, arithmetic and copies ran while one was open for 2% of the time, Pallas kernels for 36%

profile of v2, /device:TPU:8, one launch (start us, length us, event | category | flops | bytes accessed | tf_op | source)
XLA Modules:
  0.0 221.7 jit_solution(7687916377043692970)
XLA Ops:
  0.6 1.6 collective-permute-start
  2.2 1.7 collective-permute-start.3
  3.9 0.3 collective-permute-start.1
  4.2 3.0 %collective-permute-start.4 = (bf16[2048,256]{1,0:T(8,128)(2,1)}, bf16[2048,256]{1,0:T(8,128)(2,1)}, u32[]{:S(2)}, u32[]{:S(2)}) collective-permute-start(bf16[2048,256]{1,0:T(8,128)(2,1)} %bitcast.26), channel_id=1, source_target_pairs={{0,3},{1,0},{2,1},{3,2},{4,7},{5,4},{6,5},{7,6},{8,11},{9,8},{10,9... | collective-permute-start | bytes 3145736 | tf_op jit(solution)/shard_map/ppermute | solution.py:730
  7.2 0.0 collective-permute-start.2
  7.2 3.8 %dispatch.1 = (bf16[128,2048]{1,0:T(8,128)(2,1)}, bf16[6144,128]{1,0:T(8,128)(2,1)}, f32[128,384]{1,0:T(8,128)}) custom-call(bf16[128,2048]{1,0:T(8,128)(2,1)} %x_ref.1, f32[1,2048]{1,0:T(1,128)} %bitcast.18, s32[2,128]{1,0:T(2,128)} %bitcast.19, f32[2,128]{1,0:T(2,128)} %bitcast.20), custom_call_target="tpu_custom_call" | custom-call | tf_op jit(solution)/shard_map/dispatch/pallas_call | solution.py:620
  11.0 12.4 %all-to-all-start = ((bf16[64,96,128]{2,1,0:T(8,128)(2,1)}), bf16[64,96,128]{2,1,0:T(8,128)(2,1)}, u32[]{:S(2)}, u32[]{:S(2)}) async-start(bf16[64,96,128]{2,1,0:T(8,128)(2,1)} %bitcast.17), calls=%async_computation | async-start | bytes 3145728 | tf_op jit(solution)/shard_map/all_to_all | solution.py:787
  23.4 0.7 copy.21.speed_ref
  24.1 13.7 %local_mixer.1 = (f32[3,512,128]{2,1,0:T(8,128)}, f32[3,512,128]{2,1,0:T(8,128)}, f32[3,128,128]{2,1,0:T(8,128)}, f32[3,128,128]{2,1,0:T(8,128)}) custom-call(bf16[512,384]{1,0:T(8,128)(2,1)} %q_ref.1, bf16[512,384]{1,0:T(8,128)(2,1)} %k_ref.1, bf16[512,384]{1,0:T(8,128)(2,1)} %v_ref.1, f32[3,512]{1,0:T(4,128)} %bitcast.31, bf16[3,512]{1,0:T(4,128)(2,1)} %bitcast.33, ...), custom_call_target="tpu_custom_call" | custom-call | flops 30000001024 | bytes 4000000 | tf_op jit(solution)/shard_map/local_mixer/pallas_call | solution.py:178
  37.7 0.0 collective-permute-done.refs_3_
  37.7 3.3 %collective-permute-start.5 = (bf16[256,2048]{1,0:T(8,128)(2,1)}, bf16[256,2048]{1,0:T(8,128)(2,1)}, u32[]{:S(2)}, u32[]{:S(2)}) collective-permute-start(bf16[256,2048]{1,0:T(8,128)(2,1)} %bitcast.29), channel_id=1, source_target_pairs={{0,3},{1,0},{2,1},{3,2},{4,7},{5,4},{6,5},{7,6},{8,11},{9,8},{10,9... | collective-permute-start | bytes 3145736 | tf_op jit(solution)/shard_map/ppermute | solution.py:730
  41.0 9.7 %collective-permute-done.1.refs_4_ = bf16[2048,256]{1,0:T(8,128)(2,1)} collective-permute-done((bf16[2048,256]{1,0:T(8,128)(2,1)}, bf16[2048,256]{1,0:T(8,128)(2,1)}, u32[]{:S(2)}, u32[]{:S(2)}) %collective-permute-start.1) | collective-permute-done | bytes 1048608 | tf_op jit(solution)/shard_map/ppermute | solution.py:729
  50.7 1.5 collective-permute-start.6
  52.3 19.8 %collective-permute-done.2.refs_5_ = bf16[256,2048]{1,0:T(8,128)(2,1)} collective-permute-done((bf16[256,2048]{1,0:T(8,128)(2,1)}, bf16[256,2048]{1,0:T(8,128)(2,1)}, u32[]{:S(2)}, u32[]{:S(2)}) %collective-permute-start.2) | collective-permute-done | bytes 1048608 | tf_op jit(solution)/shard_map/ppermute | solution.py:729
  72.1 1.8 collective-permute-start.7
  73.9 0.0 collective-permute-done.3.refs_6_
  73.9 0.6 collective-permute-start.8
  74.5 35.9 %entry_state.1.state_ref = f32[3,128,128]{2,1,0:T(8,128)} custom-call(f32[3,128,128]{2,1,0:T(8,128)} %get-tuple-element.34.t_ref, f32[3,128,128]{2,1,0:T(8,128)} %get-tuple-element.35.i_ref), custom_call_target="tpu_custom_call" | custom-call | flops 30000001024 | bytes 4000000 | tf_op jit(solution)/shard_map/entry_state/pallas_call | solution.py:347
  110.4 0.0 collective-permute-done.4.refs_7_
  110.4 0.0 collective-permute-done.5.refs_8_
  110.4 2.7 %collective-permute-start.10 = (bf16[2048,256]{1,0:T(8,128)(2,1)}, bf16[2048,256]{1,0:T(8,128)(2,1)}, u32[]{:S(2)}, u32[]{:S(2)}) collective-permute-start(bf16[2048,256]{1,0:T(8,128)(2,1)} %collective-permute-done.4.refs_7_), channel_id=1, source_target_pairs={{0,3},{1,0},{2,1},{3,2},{4,7},{5,4},{6,5},{7,6},{8,11},{9,8},{10,9... | collective-permute-start | bytes 3145736 | tf_op jit(solution)/shard_map/ppermute | solution.py:739
  113.2 0.0 collective-permute-start.9
  113.2 1.9 slice.6
  115.1 1.9 slice.7
  117.0 0.0 collective-permute-done.6.refs_1_
  117.0 0.5 collective-permute-start.11
  117.4 0.0 collective-permute-done.7.refs_2_
  117.4 2.8 %collective-permute-start.12 = (bf16[128,2048]{1,0:T(8,128)(2,1)}, bf16[128,2048]{1,0:T(8,128)(2,1)}, u32[]{:S(2)}, u32[]{:S(2)}) collective-permute-start(bf16[128,2048]{1,0:T(8,128)(2,1)} %slice.7), channel_id=1, source_target_pairs={{0,3},{1,0},{2,1},{3,2},{4,7},{5,4},{6,5},{7,6},{8,11},{9,8},{10,9... | collective-permute-start | bytes 1572872 | tf_op jit(solution)/shard_map/ppermute | solution.py:741
  120.3 0.0 collective-permute-done.8.refs_3_
  120.3 8.4 %parts_for_peers.1 = (bf16[256,2048]{1,0:T(8,128)(2,1)}, bf16[256,2048]{1,0:T(8,128)(2,1)}, bf16[256,2048]{1,0:T(8,128)(2,1)}, bf16[256,2048]{1,0:T(8,128)(2,1)}) custom-call(s32[1]{0:T(128)} %bitcast.me_ref, f32[3,512,128]{2,1,0:T(8,128)} %get-tuple-element.32.qt_ref, f32[3,512,128]{2,1,0:T(8,128)} %get-tuple-element.33.ol_ref, ...), custom_call_target="tpu_custom_call" | custom-call | flops 6000000000 | bytes 12000000 | tf_op jit(solution)/shard_map/parts_for_peers/pallas_call | solution.py:409
  128.7 0.0 all-to-all-done
  128.7 9.3 %near_experts.1 = (bf16[384,2048]{1,0:T(8,128)(2,1)}, f32[384,2048]{1,0:T(8,128)}) custom-call(bf16[6144,128]{1,0:T(8,128)(2,1)} %bitcast.13.in_ref, bf16[2048,256]{1,0:T(8,128)(2,1)} %bitcast.24, bf16[2048,256]{1,0:T(8,128)(2,1)} %bitcast.27, bf16[256,2048]{1,0:T(8,128)(2,1)} %bitcast.30, bf16[2048,256]{1,0:T(8,128)(2,1)} %collective-permute-done.refs_3_, ...), custom_call_target="tpu_custom_call" | custom-call | flops 5000000000 | bytes 16000000 | tf_op jit(solution)/shard_map/near_experts/pallas_call | solution.py:464
  138.0 0.0 collective-permute-done.10.up_ref
  138.0 2.7 %collective-permute-done.9.gate_ref = bf16[2048,256]{1,0:T(8,128)(2,1)} collective-permute-done((bf16[2048,256]{1,0:T(8,128)(2,1)}, bf16[2048,256]{1,0:T(8,128)(2,1)}, u32[]{:S(2)}, u32[]{:S(2)}) %collective-permute-start.9) | collective-permute-done | bytes 1048608 | tf_op jit(solution)/shard_map/ppermute | solution.py:738
  140.7 3.7 %far_hidden.1.hidden_ref = bf16[384,256]{1,0:T(8,128)(2,1)} custom-call(bf16[384,2048]{1,0:T(8,128)(2,1)} %get-tuple-element.50.x_ref, bf16[2048,256]{1,0:T(8,128)(2,1)} %collective-permute-done.9.gate_ref, bf16[2048,256]{1,0:T(8,128)(2,1)} %collective-permute-done.10.up_ref), custom_call_target="tpu_custom_call" | custom-call | flops 1500000000 | bytes 4000000 | tf_op jit(solution)/shard_map/far_hidden/pallas_call | solution.py:491
  144.4 6.7 %collective-permute-done.11.down0_ref = bf16[128,2048]{1,0:T(8,128)(2,1)} collective-permute-done((bf16[128,2048]{1,0:T(8,128)(2,1)}, bf16[128,2048]{1,0:T(8,128)(2,1)}, u32[]{:S(2)}, u32[]{:S(2)}) %collective-permute-start.11) | collective-permute-done | bytes 524320 | tf_op jit(solution)/shard_map/ppermute | solution.py:740
  151.1 0.0 collective-permute-done.12.down1_ref
  151.1 4.5 %far_out.1 = bf16[6144,128]{1,0:T(8,128)(2,1)} custom-call(bf16[384,256]{1,0:T(8,128)(2,1)} %far_hidden.1.hidden_ref, f32[384,2048]{1,0:T(8,128)} %get-tuple-element.58.near_ref, bf16[128,2048]{1,0:T(8,128)(2,1)} %collective-permute-done.11.down0_ref, bf16[128,2048]{1,0:T(8,128)(2,1)} %collective-permute-done.12.down1_ref), custom_call_target="tpu_custom_call" | custom-call | flops 1500000000 | bytes 8000000 | tf_op jit(solution)/shard_map/far_out/pallas_call | solution.py:541
  155.6 8.8 %all-to-all-start.1 = ((bf16[64,96,128]{2,1,0:T(8,128)(2,1)}), bf16[64,96,128]{2,1,0:T(8,128)(2,1)}, u32[]{:S(2)}, u32[]{:S(2)}) async-start(bf16[64,96,128]{2,1,0:T(8,128)(2,1)} %bitcast.16), calls=%async_computation.1 | async-start | bytes 3145728 | tf_op jit(solution)/shard_map/all_to_all | solution.py:787
  164.4 0.1 collective-permute-start.13
  164.5 1.7 collective-permute-start.14
  166.3 1.6 collective-permute-start.15
  167.8 45.6 %collective-permute-done.13.refs_1_ = bf16[256,2048]{1,0:T(8,128)(2,1)} collective-permute-done((bf16[256,2048]{1,0:T(8,128)(2,1)S(1)}, bf16[256,2048]{1,0:T(8,128)(2,1)}, u32[]{:S(2)}, u32[]{:S(2)}) %collective-permute-start.13) | collective-permute-done | bytes 1048608 | tf_op jit(solution)/shard_map/ppermute | solution.py:826
  213.5 0.0 collective-permute-done.14.refs_2_
  213.5 0.6 collective-permute-done.15.refs_3_
  214.1 4.2 %sums_of_parts.1 = (bf16[128,2048]{1,0:T(8,128)(2,1)}, f32[128,2048]{1,0:T(8,128)}) custom-call(bf16[256,2048]{1,0:T(8,128)(2,1)} %get-tuple-element.51.refs_0_, bf16[256,2048]{1,0:T(8,128)(2,1)} %collective-permute-done.13.refs_1_, bf16[256,2048]{1,0:T(8,128)(2,1)} %collective-permute-done.14.refs_2_, bf16[256,2048]{1,0:T(8,128)(2,1)} %collective-permute-done.15.refs_3_), custom_call_target="tpu_custom_call" | custom-call | flops 1000000000 | bytes 6000000 | tf_op jit(solution)/shard_map/sums_of_parts/pallas_call | solution.py:646
  218.3 0.0 all-to-all-done.1
  218.3 3.3 %combine.1 = bf16[128,2048]{1,0:T(8,128)(2,1)} custom-call(f32[128,2048]{1,0:T(8,128)} %get-tuple-element.56.shared_hbm, bf16[6144,128]{1,0:T(8,128)(2,1)} %bitcast.15.back_hbm, f32[128,384]{1,0:T(8,128)} %get-tuple-element.61.mix_hbm), custom_call_target="tpu_custom_call" | custom-call | tf_op jit(solution)/shard_map/combine/pallas_call | solution.py:702
  (8 shorter events, 0.0 us)
Async XLA Ops:
  0.6 37.1 %collective-permute-start = (bf16[2048,256]{1,0:T(8,128)(2,1)}, bf16[2048,256]{1,0:T(8,128)(2,1)}, u32[]{:S(2)}, u32[]{:S(2)}) collective-permute-start(bf16[2048,256]{1,0:T(8,128)(2,1)} %bitcast.22), channel_id=1, source_target_pairs={{0,1},{1,2},{2,3},{3,0},{4,5},{5,6},{6,7},{7,4},{8,9},{9,10},{10,1... | collective-permute-start | bytes 3145736 | tf_op jit(solution)/shard_map/ppermute | solution.py:729
  2.2 71.7 %collective-permute-start.3 = (bf16[2048,256]{1,0:T(8,128)(2,1)}, bf16[2048,256]{1,0:T(8,128)(2,1)}, u32[]{:S(2)}, u32[]{:S(2)}) collective-permute-start(bf16[2048,256]{1,0:T(8,128)(2,1)} %bitcast.23), channel_id=1, source_target_pairs={{0,3},{1,0},{2,1},{3,2},{4,7},{5,4},{6,5},{7,6},{8,11},{9,8},{10,9... | collective-permute-start | bytes 3145736 | tf_op jit(solution)/shard_map/ppermute | solution.py:730
  3.9 46.8 %collective-permute-start.1 = (bf16[2048,256]{1,0:T(8,128)(2,1)}, bf16[2048,256]{1,0:T(8,128)(2,1)}, u32[]{:S(2)}, u32[]{:S(2)}) collective-permute-start(bf16[2048,256]{1,0:T(8,128)(2,1)} %bitcast.25), channel_id=1, source_target_pairs={{0,1},{1,2},{2,3},{3,0},{4,5},{5,6},{6,7},{7,4},{8,9},{9,10},{10,1... | collective-permute-start | bytes 3145736 | tf_op jit(solution)/shard_map/ppermute | solution.py:729
  4.2 106.2 %collective-permute-start.4 = (bf16[2048,256]{1,0:T(8,128)(2,1)}, bf16[2048,256]{1,0:T(8,128)(2,1)}, u32[]{:S(2)}, u32[]{:S(2)}) collective-permute-start(bf16[2048,256]{1,0:T(8,128)(2,1)} %bitcast.26), channel_id=1, source_target_pairs={{0,3},{1,0},{2,1},{3,2},{4,7},{5,4},{6,5},{7,6},{8,11},{9,8},{10,9... | collective-permute-start | bytes 3145736 | tf_op jit(solution)/shard_map/ppermute | solution.py:730
  7.2 64.9 %collective-permute-start.2 = (bf16[256,2048]{1,0:T(8,128)(2,1)}, bf16[256,2048]{1,0:T(8,128)(2,1)}, u32[]{:S(2)}, u32[]{:S(2)}) collective-permute-start(bf16[256,2048]{1,0:T(8,128)(2,1)} %bitcast.28), channel_id=1, source_target_pairs={{0,1},{1,2},{2,3},{3,0},{4,5},{5,6},{6,7},{7,4},{8,9},{9,10},{10,1... | collective-permute-start | bytes 3145736 | tf_op jit(solution)/shard_map/ppermute | solution.py:729
  11.0 12.4 %copy-start = (f32[3]{0:T(128)S(1)}, f32[3]{0:T(128)}, u32[]{:S(2)}) copy-start(f32[3]{0:T(128)} %param.24) | copy-start | bytes 40
  11.0 117.7 %all-to-all-start = ((bf16[64,96,128]{2,1,0:T(8,128)(2,1)}), bf16[64,96,128]{2,1,0:T(8,128)(2,1)}, u32[]{:S(2)}, u32[]{:S(2)}) async-start(bf16[64,96,128]{2,1,0:T(8,128)(2,1)} %bitcast.17), calls=%async_computation | async-start | bytes 3145728 | tf_op jit(solution)/shard_map/all_to_all | solution.py:787
  37.7 72.7 %collective-permute-start.5 = (bf16[256,2048]{1,0:T(8,128)(2,1)}, bf16[256,2048]{1,0:T(8,128)(2,1)}, u32[]{:S(2)}, u32[]{:S(2)}) collective-permute-start(bf16[256,2048]{1,0:T(8,128)(2,1)} %bitcast.29), channel_id=1, source_target_pairs={{0,3},{1,0},{2,1},{3,2},{4,7},{5,4},{6,5},{7,6},{8,11},{9,8},{10,9... | collective-permute-start | bytes 3145736 | tf_op jit(solution)/shard_map/ppermute | solution.py:730
  50.7 66.2 %collective-permute-start.6 = (bf16[128,2048]{1,0:T(8,128)(2,1)}, bf16[128,2048]{1,0:T(8,128)(2,1)}, u32[]{:S(2)}, u32[]{:S(2)}) collective-permute-start(bf16[128,2048]{1,0:T(8,128)(2,1)} %get-tuple-element.37.refs_0_), channel_id=1, source_target_pairs={{0,3},{1,0},{2,1},{3,2},{4,7},{5,4},{6,5},{7,6},{8,11},{9,8},{10,9... | collective-permute-start | bytes 1572872 | tf_op jit(solution)/shard_map/ppermute | solution.py:795
  72.1 45.4 %collective-permute-start.7 = (bf16[128,2048]{1,0:T(8,128)(2,1)}, bf16[128,2048]{1,0:T(8,128)(2,1)}, u32[]{:S(2)}, u32[]{:S(2)}) collective-permute-start(bf16[128,2048]{1,0:T(8,128)(2,1)} %get-tuple-element.37.refs_0_), channel_id=1, source_target_pairs={{0,2},{1,3},{2,0},{3,1},{4,6},{5,7},{6,4},{7,5},{8,10},{9,11},{10,... | collective-permute-start | bytes 1572872 | tf_op jit(solution)/shard_map/ppermute | solution.py:795
  73.9 46.4 %collective-permute-start.8 = (bf16[128,2048]{1,0:T(8,128)(2,1)}, bf16[128,2048]{1,0:T(8,128)(2,1)}, u32[]{:S(2)}, u32[]{:S(2)}) collective-permute-start(bf16[128,2048]{1,0:T(8,128)(2,1)} %get-tuple-element.37.refs_0_), channel_id=1, source_target_pairs={{0,1},{1,2},{2,3},{3,0},{4,5},{5,6},{6,7},{7,4},{8,9},{9,10},{10,1... | collective-permute-start | bytes 1572872 | tf_op jit(solution)/shard_map/ppermute | solution.py:795
  110.4 27.6 %collective-permute-start.10 = (bf16[2048,256]{1,0:T(8,128)(2,1)}, bf16[2048,256]{1,0:T(8,128)(2,1)}, u32[]{:S(2)}, u32[]{:S(2)}) collective-permute-start(bf16[2048,256]{1,0:T(8,128)(2,1)} %collective-permute-done.4.refs_7_), channel_id=1, source_target_pairs={{0,3},{1,0},{2,1},{3,2},{4,7},{5,4},{6,5},{7,6},{8,11},{9,8},{10,9... | collective-permute-start | bytes 3145736 | tf_op jit(solution)/shard_map/ppermute | solution.py:739
  113.2 27.6 %collective-permute-start.9 = (bf16[2048,256]{1,0:T(8,128)(2,1)}, bf16[2048,256]{1,0:T(8,128)(2,1)}, u32[]{:S(2)}, u32[]{:S(2)}) collective-permute-start(bf16[2048,256]{1,0:T(8,128)(2,1)} %collective-permute-done.refs_3_), channel_id=1, source_target_pairs={{0,1},{1,2},{2,3},{3,0},{4,5},{5,6},{6,7},{7,4},{8,9},{9,10},{10,1... | collective-permute-start | bytes 3145736 | tf_op jit(solution)/shard_map/ppermute | solution.py:738
  117.0 34.1 %collective-permute-start.11 = (bf16[128,2048]{1,0:T(8,128)(2,1)}, bf16[128,2048]{1,0:T(8,128)(2,1)}, u32[]{:S(2)}, u32[]{:S(2)}) collective-permute-start(bf16[128,2048]{1,0:T(8,128)(2,1)} %slice.6), channel_id=1, source_target_pairs={{0,1},{1,2},{2,3},{3,0},{4,5},{5,6},{6,7},{7,4},{8,9},{9,10},{10,1... | collective-permute-start | bytes 1572872 | tf_op jit(solution)/shard_map/ppermute | solution.py:740
  117.4 33.6 %collective-permute-start.12 = (bf16[128,2048]{1,0:T(8,128)(2,1)}, bf16[128,2048]{1,0:T(8,128)(2,1)}, u32[]{:S(2)}, u32[]{:S(2)}) collective-permute-start(bf16[128,2048]{1,0:T(8,128)(2,1)} %slice.7), channel_id=1, source_target_pairs={{0,3},{1,0},{2,1},{3,2},{4,7},{5,4},{6,5},{7,6},{8,11},{9,8},{10,9... | collective-permute-start | bytes 1572872 | tf_op jit(solution)/shard_map/ppermute | solution.py:741
  155.6 8.8 %copy-start.3 = (bf16[256,2048]{1,0:T(8,128)(2,1)S(1)}, bf16[256,2048]{1,0:T(8,128)(2,1)}, u32[]{:S(2)}) copy-start(bf16[256,2048]{1,0:T(8,128)(2,1)} %get-tuple-element.52) | copy-start | bytes 3145732
  155.6 8.9 %copy-start.2 = (bf16[256,2048]{1,0:T(8,128)(2,1)S(1)}, bf16[256,2048]{1,0:T(8,128)(2,1)}, u32[]{:S(2)}) copy-start(bf16[256,2048]{1,0:T(8,128)(2,1)} %get-tuple-element.53) | copy-start | bytes 3145732
  155.6 10.6 %copy-start.1 = (bf16[256,2048]{1,0:T(8,128)(2,1)S(1)}, bf16[256,2048]{1,0:T(8,128)(2,1)}, u32[]{:S(2)}) copy-start(bf16[256,2048]{1,0:T(8,128)(2,1)} %get-tuple-element.54) | copy-start | bytes 3145732
  155.6 62.7 %all-to-all-start.1 = ((bf16[64,96,128]{2,1,0:T(8,128)(2,1)}), bf16[64,96,128]{2,1,0:T(8,128)(2,1)}, u32[]{:S(2)}, u32[]{:S(2)}) async-start(bf16[64,96,128]{2,1,0:T(8,128)(2,1)} %bitcast.16), calls=%async_computation.1 | async-start | bytes 3145728 | tf_op jit(solution)/shard_map/all_to_all | solution.py:787
  164.4 49.0 %collective-permute-start.13 = (bf16[256,2048]{1,0:T(8,128)(2,1)S(1)}, bf16[256,2048]{1,0:T(8,128)(2,1)}, u32[]{:S(2)}, u32[]{:S(2)}) collective-permute-start(bf16[256,2048]{1,0:T(8,128)(2,1)S(1)} %copy-done.3), channel_id=1, source_target_pairs={{0,1},{1,2},{2,3},{3,0},{4,5},{5,6},{6,7},{7,4},{8,9},{9,10},{10,1... | collective-permute-start | bytes 3145736 | tf_op jit(solution)/shard_map/ppermute | solution.py:826
  164.5 48.9 %collective-permute-start.14 = (bf16[256,2048]{1,0:T(8,128)(2,1)S(1)}, bf16[256,2048]{1,0:T(8,128)(2,1)}, u32[]{:S(2)}, u32[]{:S(2)}) collective-permute-start(bf16[256,2048]{1,0:T(8,128)(2,1)S(1)} %copy-done.2), channel_id=1, source_target_pairs={{0,2},{1,3},{2,0},{3,1},{4,6},{5,7},{6,4},{7,5},{8,10},{9,11},{10,... | collective-permute-start | bytes 3145736 | tf_op jit(solution)/shard_map/ppermute | solution.py:826
  166.3 47.8 %collective-permute-start.15 = (bf16[256,2048]{1,0:T(8,128)(2,1)S(1)}, bf16[256,2048]{1,0:T(8,128)(2,1)}, u32[]{:S(2)}, u32[]{:S(2)}) collective-permute-start(bf16[256,2048]{1,0:T(8,128)(2,1)S(1)} %copy-done.1), channel_id=1, source_target_pairs={{0,3},{1,0},{2,1},{3,2},{4,7},{5,4},{6,5},{7,6},{8,11},{9,8},{10,9... | collective-permute-start | bytes 3145736 | tf_op jit(solution)/shard_map/ppermute | solution.py:826

commit v3 on v2

--- a/solution.py
+++ b/solution.py
@@ -367,11 +367,14 @@
 
 
 def parts_kernel(peers, me_ref, qt_ref, ol_ref, state_ref, gain_ref, w_ref, *refs):
-    hbm, refs = refs[: peers + 3], refs[peers + 3 :]
+    far = peers // 2
+    near = [r for r in range(peers) if r != far]
+    count = len(near)
+    hbm, refs = refs[: count + 3], refs[count + 3 :]
     out_refs, (x, gate, up, down, sems) = refs[:peers], refs[peers:]
     heads, rows, _ = qt_ref.shape
     tile = rows // peers
-    spots = [x.at[r * tile : (r + 1) * tile] for r in range(peers)] + [gate, up, down]
+    spots = [x.at[r * tile : (r + 1) * tile] for r in range(count)] + [gate, up, down]
     copies = [
         pltpu.make_async_copy(src, dst, sems.at[k]) for k, (src, dst) in enumerate(zip(hbm, spots))
     ]
@@ -395,14 +398,14 @@
         copy.wait()
     hidden = gated(mm(x[...], gate[...]), mm(x[...], up[...]))
     shared = mm(hidden, down[...]).astype(BF16)
-    for r in range(peers):
-        out_refs[r][tile:] = shared[r * tile : (r + 1) * tile]
+    for k, r in enumerate(near):
+        out_refs[r][tile:] = shared[k * tile : (k + 1) * tile]
 
 
 def parts_for_peers(me, qt, ol, state, gain, w, tokens, gate, up, down):
     _, rows, d = qt.shape
     width = w.shape[1]
-    peers = len(tokens)
+    peers = len(tokens) + 1
     tile = rows // peers
     vmem = pl.BlockSpec(memory_space=pltpu.VMEM)
     kept = (*tokens, gate, up, down)
@@ -412,9 +415,12 @@
         + [vmem] * 5
         + [pl.BlockSpec(memory_space=pl.ANY)] * len(kept),
         out_specs=[vmem] * peers,
-        out_shape=[jax.ShapeDtypeStruct((2 * tile, width), BF16)] * peers,
+        out_shape=[
+            jax.ShapeDtypeStruct((tile if r == peers // 2 else 2 * tile, width), BF16)
+            for r in range(peers)
+        ],
         scratch_shapes=[
-            pltpu.VMEM((rows, width), BF16),
+            pltpu.VMEM((len(tokens) * tile, width), BF16),
             pltpu.VMEM(gate.shape, BF16),
             pltpu.VMEM(up.shape, BF16),
             pltpu.VMEM(down.shape, BF16),
@@ -424,6 +430,29 @@
         compiler_params=ALL_VMEM,
         name="parts_for_peers",
     )(me, qt, ol, state, gain.reshape(1, d), w, *kept)
+
+
+def shared_part_kernel(x_ref, gate_ref, up_ref, down_hbm, out_ref, down, sem):
+    load = pltpu.make_async_copy(down_hbm, down, sem)
+    load.start()
+    x = x_ref[...]
+    hidden = gated(mm(x, gate_ref[...]), mm(x, up_ref[...]))
+    load.wait()
+    out_ref[...] = mm(hidden, down[...]).astype(BF16)
+
+
+def shared_part(x, gate, up, down):
+    vmem = pl.BlockSpec(memory_space=pltpu.VMEM)
+    return pl.pallas_call(
+        shared_part_kernel,
+        in_specs=[vmem] * 3 + [pl.BlockSpec(memory_space=pl.ANY)],
+        out_specs=vmem,
+        out_shape=jax.ShapeDtypeStruct((x.shape[0], down.shape[1]), BF16),
+        scratch_shapes=[pltpu.VMEM(down.shape, BF16), pltpu.SemaphoreType.DMA],
+        cost_estimate=pl.CostEstimate(flops=1_000_000_000, bytes_accessed=4_000_000, transcendentals=0),
+        compiler_params=ALL_VMEM,
+        name="shared_part",
+    )(x, gate, up, down)
 
 
 def near_experts_kernel(in_ref, *refs):
@@ -629,33 +658,33 @@
 
 
 def sums_kernel(*refs):
-    *part_refs, mixer_ref, shared_ref = refs
+    *part_refs, far_mixer_ref, far_shared_ref, mixer_ref, shared_ref = refs
     tokens = mixer_ref.shape[0]
-    mixer, shared = part_refs[0][:tokens].astype(F32), part_refs[0][tokens:].astype(F32)
-    for part in part_refs[1:]:
+    mixer, shared = far_mixer_ref[...].astype(F32), far_shared_ref[...].astype(F32)
+    for part in part_refs:
         mixer = mixer + part[:tokens].astype(F32)
         shared = shared + part[tokens:].astype(F32)
     mixer_ref[...] = mixer.astype(BF16)
     shared_ref[...] = shared
 
 
-def sums_of_parts(parts):
-    rows, width = parts[0].shape
+def sums_of_parts(parts, far_mixer, far_shared):
+    tokens, width = far_mixer.shape
     tile = 512
-    out = pl.BlockSpec((rows // 2, tile), lambda c: (0, c))
+    out = pl.BlockSpec((tokens, tile), lambda c: (0, c))
     return pl.pallas_call(
         sums_kernel,
         grid=(width // tile,),
-        in_specs=[pl.BlockSpec((rows, tile), lambda c: (0, c))] * len(parts),
+        in_specs=[pl.BlockSpec((2 * tokens, tile), lambda c: (0, c))] * len(parts) + [out, out],
         out_specs=[out, out],
         out_shape=[
-            jax.ShapeDtypeStruct((rows // 2, width), BF16),
-            jax.ShapeDtypeStruct((rows // 2, width), F32),
+            jax.ShapeDtypeStruct((tokens, width), BF16),
+            jax.ShapeDtypeStruct((tokens, width), F32),
         ],
         cost_estimate=pl.CostEstimate(flops=1_000_000_000, bytes_accessed=6_000_000, transcendentals=0),
         compiler_params=ALL_VMEM,
         name="sums_of_parts",
-    )(*parts)
+    )(*parts, far_mixer, far_shared)
 
 
 def combine_kernel(shared_hbm, back_hbm, mix_hbm, out_hbm, shared, back, mix, out, sems):
@@ -792,7 +821,9 @@
         return [(i, (i + r) % peers) for i in range(peers)]
 
     arrived = to_peers(outgoing)
-    group = [xn] + [lax.ppermute(xn, "tp", shift(peers - r)) for r in range(1, peers)]
+    opposite = peers // 2
+    near_peers = [r for r in range(1, peers) if r != opposite]
+    group = [xn] + [lax.ppermute(xn, "tp", shift(peers - r)) for r in near_peers]
 
     qt, ol, trans, inject = local_mixer(
         queries,
@@ -821,13 +852,16 @@
     )
     rows, near = near_experts(arrived, (own, from_left, from_right))
     hidden = far_hidden(rows, *far[:2])
-    parts, far, near, hidden = lax.optimization_barrier((parts, far, near, hidden))
-    got = [parts[0]] + [
-        lax.ppermute(parts[r], "tp", shift(r)) for r in range(1, peers)
-    ]
+    parts, far, near, hidden, xn = lax.optimization_barrier((parts, far, near, hidden, xn))
+    far_xn = lax.ppermute(xn, "tp", shift(opposite))
+    got = [parts[0]] + [lax.ppermute(parts[r], "tp", shift(r)) for r in near_peers]
+    far_mixer = lax.ppermute(parts[opposite], "tp", shift(opposite))
     slot_sums = far_out(hidden, near, *far[2:])
     back = to_peers(slot_sums)
-    mixer_out, shared = sums_of_parts(got)
+    far_xn, slot_sums = lax.optimization_barrier((far_xn, slot_sums))
+    late = shared_part(far_xn, common_gate_weight, common_up_weight, common_down_weight)
+    far_shared = lax.ppermute(late, "tp", shift(opposite))
+    mixer_out, shared = sums_of_parts(got, far_mixer, far_shared)
     return (mixer_out, combine(shared, back, mix))
 
 

time: 222 us -> 229 us (1.032)
  starting transfers between devices: 44.4 us -> 48.5 us
  Pallas kernels: 86.8 us -> 90.3 us
    ppermute x0 -> x3, waiting for transfers between devices: none -> 47.3 us  [the longest x1 26.6 us: shards(): far_mixer = lax.ppermute(parts[opposite], 'tp', shift(opposite))]
    ppermute x3 -> x2, waiting for transfers between devices: 46.3 us -> 0.01 us  [shards(): lax.ppermute(parts[r], 'tp', shift(r))]
    ppermute x0 -> x3, starting transfers between devices: none -> 6.02 us  [the longest x1 3.01 us: shards(): far_shared = lax.ppermute(late, 'tp', shift(opposite))]
    pallas_call x0 -> x1, Pallas kernels: none -> 4.05 us  [shared_part(): pl.pallas_call(shared_part_kernel, in_specs=[vmem] * 3 + [pl.BlockSpec(me...]
    ppermute x1, waiting for transfers between devices: 2.7 us -> 0.22 us  [far_shard(): lax.ppermute(from_left[0], axis, right)]
  transfers between devices with their start and end apart: 18 -> 19, of which waited for: 6 -> 8; matrix products, arithmetic and copies ran while one was open for 2% -> 2% of each run, Pallas kernels for 36% -> 36%
where the time goes in v3:
time: 229 us; the launch traced here: 228 us
  Pallas kernels  90.3 us (39%)
  waiting for transfers between devices  84 us (37%)
  starting transfers between devices  48.5 us (21%)
  local copies, waits for them, and re-layouts  4.43 us (2%)
    pallas_call x1, Pallas kernels, entry_state(): pl.pallas_call(entry_state_kernel, in_specs=[vmem, vmem], out_specs=vmem,...  36.1 us
    ppermute x3, waiting for transfers between devices, neighbours_shards(): from_left = [lax.ppermute(w, axis, right) for w in shard]  29.5 us
    ppermute x1, waiting for transfers between devices, shards(): far_mixer = lax.ppermute(parts[opposite], 'tp', shift(opposite))  26.6 us
    all_to_all x2, starting transfers between devices, to_peers(): lax.all_to_all(parts, EP, split_axis=0, concat_axis=0, tiled=True)  21 us
    pallas_call x1, Pallas kernels, local_mixer(): pl.pallas_call(local_mixer_kernel, grid=(heads,), in_specs=[by_head, by_h...  13.7 us
    ppermute x1, waiting for transfers between devices, shards(): far_shared = lax.ppermute(late, 'tp', shift(opposite))  10.4 us
    ppermute x1, waiting for transfers between devices, shards(): far_xn = lax.ppermute(xn, 'tp', shift(opposite))  10.3 us
    pallas_call x1, Pallas kernels, near_experts(): pl.pallas_call(near_experts_kernel, in_specs=[vmem] + [pl.BlockSpec(memor...  9.31 us
  transfers between devices with their start and end apart: 19, of which 8 were waited for; matrix products, arithmetic and copies ran while one was open for 2% of the time, Pallas kernels for 36%

profile of v3, /device:TPU:8, one launch (start us, length us, event | category | flops | bytes accessed | tf_op | source)
XLA Modules:
  0.0 228.2 jit_solution(17388381783013822319)
XLA Ops:
  0.6 1.6 collective-permute-start
  2.2 1.7 collective-permute-start.3
  3.9 0.3 collective-permute-start.1
  4.2 3.0 %collective-permute-start.4 = (bf16[2048,256]{1,0:T(8,128)(2,1)}, bf16[2048,256]{1,0:T(8,128)(2,1)}, u32[]{:S(2)}, u32[]{:S(2)}) collective-permute-start(bf16[2048,256]{1,0:T(8,128)(2,1)} %bitcast.26), channel_id=1, source_target_pairs={{0,3},{1,0},{2,1},{3,2},{4,7},{5,4},{6,5},{7,6},{8,11},{9,8},{10,9... | collective-permute-start | bytes 3145736 | tf_op jit(solution)/shard_map/ppermute | solution.py:759
  7.2 0.0 collective-permute-start.2
  7.2 3.8 %dispatch.1 = (bf16[128,2048]{1,0:T(8,128)(2,1)}, bf16[6144,128]{1,0:T(8,128)(2,1)}, f32[128,384]{1,0:T(8,128)}) custom-call(bf16[128,2048]{1,0:T(8,128)(2,1)} %x_ref.1, f32[1,2048]{1,0:T(1,128)} %bitcast.18, s32[2,128]{1,0:T(2,128)} %bitcast.19, f32[2,128]{1,0:T(2,128)} %bitcast.20), custom_call_target="tpu_custom_call" | custom-call | tf_op jit(solution)/shard_map/dispatch/pallas_call | solution.py:649
  11.0 12.4 %all-to-all-start = ((bf16[64,96,128]{2,1,0:T(8,128)(2,1)}), bf16[64,96,128]{2,1,0:T(8,128)(2,1)}, u32[]{:S(2)}, u32[]{:S(2)}) async-start(bf16[64,96,128]{2,1,0:T(8,128)(2,1)} %bitcast.17), calls=%async_computation | async-start | bytes 3145728 | tf_op jit(solution)/shard_map/all_to_all | solution.py:816
  23.4 0.7 copy.21.speed_ref
  24.1 13.7 %local_mixer.1 = (f32[3,512,128]{2,1,0:T(8,128)}, f32[3,512,128]{2,1,0:T(8,128)}, f32[3,128,128]{2,1,0:T(8,128)}, f32[3,128,128]{2,1,0:T(8,128)}) custom-call(bf16[512,384]{1,0:T(8,128)(2,1)} %q_ref.1, bf16[512,384]{1,0:T(8,128)(2,1)} %k_ref.1, bf16[512,384]{1,0:T(8,128)(2,1)} %v_ref.1, f32[3,512]{1,0:T(4,128)} %bitcast.31, bf16[3,512]{1,0:T(4,128)(2,1)} %bitcast.33, ...), custom_call_target="tpu_custom_call" | custom-call | flops 30000001024 | bytes 4000000 | tf_op jit(solution)/shard_map/local_mixer/pallas_call | solution.py:178
  37.7 0.0 collective-permute-done.refs_3_
  37.7 3.3 %collective-permute-start.5 = (bf16[256,2048]{1,0:T(8,128)(2,1)}, bf16[256,2048]{1,0:T(8,128)(2,1)}, u32[]{:S(2)}, u32[]{:S(2)}) collective-permute-start(bf16[256,2048]{1,0:T(8,128)(2,1)} %bitcast.29), channel_id=1, source_target_pairs={{0,3},{1,0},{2,1},{3,2},{4,7},{5,4},{6,5},{7,6},{8,11},{9,8},{10,9... | collective-permute-start | bytes 3145736 | tf_op jit(solution)/shard_map/ppermute | solution.py:759
  41.0 9.7 %collective-permute-done.1.refs_4_ = bf16[2048,256]{1,0:T(8,128)(2,1)} collective-permute-done((bf16[2048,256]{1,0:T(8,128)(2,1)}, bf16[2048,256]{1,0:T(8,128)(2,1)}, u32[]{:S(2)}, u32[]{:S(2)}) %collective-permute-start.1) | collective-permute-done | bytes 1048608 | tf_op jit(solution)/shard_map/ppermute | solution.py:758
  50.7 1.5 collective-permute-start.6
  52.3 19.8 %collective-permute-done.2.refs_5_ = bf16[256,2048]{1,0:T(8,128)(2,1)} collective-permute-done((bf16[256,2048]{1,0:T(8,128)(2,1)}, bf16[256,2048]{1,0:T(8,128)(2,1)}, u32[]{:S(2)}, u32[]{:S(2)}) %collective-permute-start.2) | collective-permute-done | bytes 1048608 | tf_op jit(solution)/shard_map/ppermute | solution.py:758
  72.1 0.3 collective-permute-start.7
  72.4 36.1 %entry_state.1.state_ref = f32[3,128,128]{2,1,0:T(8,128)} custom-call(f32[3,128,128]{2,1,0:T(8,128)} %get-tuple-element.36.t_ref, f32[3,128,128]{2,1,0:T(8,128)} %get-tuple-element.37.i_ref), custom_call_target="tpu_custom_call" | custom-call | flops 30000001024 | bytes 4000000 | tf_op jit(solution)/shard_map/entry_state/pallas_call | solution.py:347
  108.5 0.0 collective-permute-done.3.refs_6_
  108.5 0.0 collective-permute-done.4.refs_7_
  108.5 0.0 collective-permute-done.5.refs_8_
  108.5 1.6 collective-permute-start.8
  110.1 1.7 collective-permute-start.9
  111.8 1.9 slice.6
  113.7 0.3 collective-permute-start.10
  114.0 1.9 slice.7
  115.9 0.0 collective-permute-done.6.refs_1_
  115.9 2.9 %collective-permute-start.11 = (bf16[128,2048]{1,0:T(8,128)(2,1)}, bf16[128,2048]{1,0:T(8,128)(2,1)}, u32[]{:S(2)}, u32[]{:S(2)}) collective-permute-start(bf16[128,2048]{1,0:T(8,128)(2,1)} %slice.7), channel_id=1, source_target_pairs={{0,3},{1,0},{2,1},{3,2},{4,7},{5,4},{6,5},{7,6},{8,11},{9,8},{10,9... | collective-permute-start | bytes 1572872 | tf_op jit(solution)/shard_map/ppermute | solution.py:770
  118.8 0.0 collective-permute-done.7.refs_2_
  118.8 7.8 %parts_for_peers.1 = (bf16[256,2048]{1,0:T(8,128)(2,1)}, bf16[256,2048]{1,0:T(8,128)(2,1)}, bf16[128,2048]{1,0:T(8,128)(2,1)}, bf16[256,2048]{1,0:T(8,128)(2,1)}) custom-call(s32[1]{0:T(128)} %bitcast.me_ref, f32[3,512,128]{2,1,0:T(8,128)} %get-tuple-element.34.qt_ref, f32[3,512,128]{2,1,0:T(8,128)} %get-tuple-element.35.ol_ref, ...), custom_call_target="tpu_custom_call" | custom-call | flops 6000000000 | bytes 12000000 | tf_op jit(solution)/shard_map/parts_for_peers/pallas_call | solution.py:412
  126.6 0.0 all-to-all-done
  126.6 9.3 %near_experts.1 = (bf16[384,2048]{1,0:T(8,128)(2,1)}, f32[384,2048]{1,0:T(8,128)}) custom-call(bf16[6144,128]{1,0:T(8,128)(2,1)} %bitcast.13.in_ref, bf16[2048,256]{1,0:T(8,128)(2,1)} %bitcast.24, bf16[2048,256]{1,0:T(8,128)(2,1)} %bitcast.27, bf16[256,2048]{1,0:T(8,128)(2,1)} %bitcast.30, bf16[2048,256]{1,0:T(8,128)(2,1)} %collective-permute-done.refs_3_, ...), custom_call_target="tpu_custom_call" | custom-call | flops 5000000000 | bytes 16000000 | tf_op jit(solution)/shard_map/near_experts/pallas_call | solution.py:493
  135.9 0.2 collective-permute-done.8.gate_ref
  136.1 0.3 collective-permute-done.9.up_ref
  136.4 3.7 %far_hidden.1.hidden_ref = bf16[384,256]{1,0:T(8,128)(2,1)} custom-call(bf16[384,2048]{1,0:T(8,128)(2,1)} %get-tuple-element.52.x_ref, bf16[2048,256]{1,0:T(8,128)(2,1)} %collective-permute-done.8.gate_ref, bf16[2048,256]{1,0:T(8,128)(2,1)} %collective-permute-done.9.up_ref), custom_call_target="tpu_custom_call" | custom-call | flops 1500000000 | bytes 4000000 | tf_op jit(solution)/shard_map/far_hidden/pallas_call | solution.py:520
  140.1 6.7 %collective-permute-done.10.down0_ref = bf16[128,2048]{1,0:T(8,128)(2,1)} collective-permute-done((bf16[128,2048]{1,0:T(8,128)(2,1)}, bf16[128,2048]{1,0:T(8,128)(2,1)}, u32[]{:S(2)}, u32[]{:S(2)}) %collective-permute-start.10) | collective-permute-done | bytes 524320 | tf_op jit(solution)/shard_map/ppermute | solution.py:769
  146.8 4.5 %far_out.1 = bf16[6144,128]{1,0:T(8,128)(2,1)} custom-call(bf16[384,256]{1,0:T(8,128)(2,1)} %far_hidden.1.hidden_ref, f32[384,2048]{1,0:T(8,128)} %get-tuple-element.59.near_ref, bf16[128,2048]{1,0:T(8,128)(2,1)} %collective-permute-done.10.down0_ref, bf16[128,2048]{1,0:T(8,128)(2,1)} %collective-permute-done.11.down1_ref), custom_call_target="tpu_custom_call" | custom-call | flops 1500000000 | bytes 8000000 | tf_op jit(solution)/shard_map/far_out/pallas_call | solution.py:570
  151.3 0.0 copy-start.1
  151.3 8.6 %all-to-all-start.1 = ((bf16[64,96,128]{2,1,0:T(8,128)(2,1)}), bf16[64,96,128]{2,1,0:T(8,128)(2,1)}, u32[]{:S(2)}, u32[]{:S(2)}) async-start(bf16[64,96,128]{2,1,0:T(8,128)(2,1)} %bitcast.16), calls=%async_computation.1 | async-start | bytes 3145728 | tf_op jit(solution)/shard_map/all_to_all | solution.py:816
  159.9 3.0 %collective-permute-start.15 = (bf16[128,2048]{1,0:T(8,128)(2,1)S(1)}, bf16[128,2048]{1,0:T(8,128)(2,1)}, u32[]{:S(2)}, u32[]{:S(2)}) collective-permute-start(bf16[128,2048]{1,0:T(8,128)(2,1)S(1)} %copy-done.1), channel_id=1, source_target_pairs={{0,2},{1,3},{2,0},{3,1},{4,6},{5,7},{6,4},{7,5},{8,10},{9,11},{10,... | collective-permute-start | bytes 1572872 | tf_op jit(solution)/shard_map/ppermute | solution.py:856
  162.9 1.0 collective-permute-start.12
  163.9 2.3 collective-permute-start.13
  166.1 10.3 %collective-permute-done.15.x_ref = bf16[128,2048]{1,0:T(8,128)(2,1)} collective-permute-done((bf16[128,2048]{1,0:T(8,128)(2,1)S(1)}, bf16[128,2048]{1,0:T(8,128)(2,1)}, u32[]{:S(2)}, u32[]{:S(2)}) %collective-permute-start.15) | collective-permute-done | bytes 524320 | tf_op jit(solution)/shard_map/ppermute | solution.py:856
  176.4 4.0 %shared_part.1 = bf16[128,2048]{1,0:T(8,128)(2,1)} custom-call(bf16[128,2048]{1,0:T(8,128)(2,1)} %collective-permute-done.15.x_ref, bf16[2048,256]{1,0:T(8,128)(2,1)} %gate_ref.1, bf16[2048,256]{1,0:T(8,128)(2,1)} %up_ref.1, bf16[256,2048]{1,0:T(8,128)(2,1)} %down_hbm.1), custom_call_target="tpu_custom_call" | custom-call | flops 1000000000 | bytes 4000000 | tf_op jit(solution)/shard_map/shared_part/pallas_call | solution.py:446
  180.5 3.0 %collective-permute-start.16 = (bf16[128,2048]{1,0:T(8,128)(2,1)}, bf16[128,2048]{1,0:T(8,128)(2,1)}, u32[]{:S(2)}, u32[]{:S(2)}) collective-permute-start(bf16[128,2048]{1,0:T(8,128)(2,1)} %shared_part.1), channel_id=1, source_target_pairs={{0,2},{1,3},{2,0},{3,1},{4,6},{5,7},{6,4},{7,5},{8,10},{9,11},{10,... | collective-permute-start | bytes 1572872 | tf_op jit(solution)/shard_map/ppermute | solution.py:863
  183.5 26.6 %collective-permute-done.14.refs_3_ = bf16[128,2048]{1,0:T(8,128)(2,1)} collective-permute-done((bf16[128,2048]{1,0:T(8,128)(2,1)}, bf16[128,2048]{1,0:T(8,128)(2,1)}, u32[]{:S(2)}, u32[]{:S(2)}) %collective-permute-start.14) | collective-permute-done | bytes 524320 | tf_op jit(solution)/shard_map/ppermute | solution.py:858
  210.1 10.4 %collective-permute-done.16.refs_4_ = bf16[128,2048]{1,0:T(8,128)(2,1)} collective-permute-done((bf16[128,2048]{1,0:T(8,128)(2,1)}, bf16[128,2048]{1,0:T(8,128)(2,1)}, u32[]{:S(2)}, u32[]{:S(2)}) %collective-permute-start.16) | collective-permute-done | bytes 524320 | tf_op jit(solution)/shard_map/ppermute | solution.py:863
  220.5 0.0 collective-permute-done.13.refs_2_
  220.5 4.2 %sums_of_parts.1 = (bf16[128,2048]{1,0:T(8,128)(2,1)}, f32[128,2048]{1,0:T(8,128)}) custom-call(bf16[256,2048]{1,0:T(8,128)(2,1)} %get-tuple-element.53.refs_0_, bf16[256,2048]{1,0:T(8,128)(2,1)} %collective-permute-done.12.refs_1_, bf16[256,2048]{1,0:T(8,128)(2,1)} %collective-permute-done.13.refs_2_, bf16[128,2048]{1,0:T(8,128)(2,1)} %collective-permute-done.14.refs_3_, ...), custom_call_target="tpu_custom_call" | custom-call | flops 1000000000 | bytes 6000000 | tf_op jit(solution)/shard_map/sums_of_parts/pallas_call | solution.py:675
  224.7 3.3 %combine.1 = bf16[128,2048]{1,0:T(8,128)(2,1)} custom-call(f32[128,2048]{1,0:T(8,128)} %get-tuple-element.64.shared_hbm, bf16[6144,128]{1,0:T(8,128)(2,1)} %bitcast.15.back_hbm, f32[128,384]{1,0:T(8,128)} %get-tuple-element.65.mix_hbm), custom_call_target="tpu_custom_call" | custom-call | tf_op jit(solution)/shard_map/combine/pallas_call | solution.py:731
  (7 shorter events, 0.0 us)
Async XLA Ops:
  0.6 37.1 %collective-permute-start = (bf16[2048,256]{1,0:T(8,128)(2,1)}, bf16[2048,256]{1,0:T(8,128)(2,1)}, u32[]{:S(2)}, u32[]{:S(2)}) collective-permute-start(bf16[2048,256]{1,0:T(8,128)(2,1)} %bitcast.22), channel_id=1, source_target_pairs={{0,1},{1,2},{2,3},{3,0},{4,5},{5,6},{6,7},{7,4},{8,9},{9,10},{10,1... | collective-permute-start | bytes 3145736 | tf_op jit(solution)/shard_map/ppermute | solution.py:758
  2.2 106.3 %collective-permute-start.3 = (bf16[2048,256]{1,0:T(8,128)(2,1)}, bf16[2048,256]{1,0:T(8,128)(2,1)}, u32[]{:S(2)}, u32[]{:S(2)}) collective-permute-start(bf16[2048,256]{1,0:T(8,128)(2,1)} %bitcast.23), channel_id=1, source_target_pairs={{0,3},{1,0},{2,1},{3,2},{4,7},{5,4},{6,5},{7,6},{8,11},{9,8},{10,9... | collective-permute-start | bytes 3145736 | tf_op jit(solution)/shard_map/ppermute | solution.py:759
  3.9 46.8 %collective-permute-start.1 = (bf16[2048,256]{1,0:T(8,128)(2,1)}, bf16[2048,256]{1,0:T(8,128)(2,1)}, u32[]{:S(2)}, u32[]{:S(2)}) collective-permute-start(bf16[2048,256]{1,0:T(8,128)(2,1)} %bitcast.25), channel_id=1, source_target_pairs={{0,1},{1,2},{2,3},{3,0},{4,5},{5,6},{6,7},{7,4},{8,9},{9,10},{10,1... | collective-permute-start | bytes 3145736 | tf_op jit(solution)/shard_map/ppermute | solution.py:758
  4.2 104.2 %collective-permute-start.4 = (bf16[2048,256]{1,0:T(8,128)(2,1)}, bf16[2048,256]{1,0:T(8,128)(2,1)}, u32[]{:S(2)}, u32[]{:S(2)}) collective-permute-start(bf16[2048,256]{1,0:T(8,128)(2,1)} %bitcast.26), channel_id=1, source_target_pairs={{0,3},{1,0},{2,1},{3,2},{4,7},{5,4},{6,5},{7,6},{8,11},{9,8},{10,9... | collective-permute-start | bytes 3145736 | tf_op jit(solution)/shard_map/ppermute | solution.py:759
  7.2 64.9 %collective-permute-start.2 = (bf16[256,2048]{1,0:T(8,128)(2,1)}, bf16[256,2048]{1,0:T(8,128)(2,1)}, u32[]{:S(2)}, u32[]{:S(2)}) collective-permute-start(bf16[256,2048]{1,0:T(8,128)(2,1)} %bitcast.28), channel_id=1, source_target_pairs={{0,1},{1,2},{2,3},{3,0},{4,5},{5,6},{6,7},{7,4},{8,9},{9,10},{10,1... | collective-permute-start | bytes 3145736 | tf_op jit(solution)/shard_map/ppermute | solution.py:758
  11.0 12.4 %copy-start = (f32[3]{0:T(128)S(1)}, f32[3]{0:T(128)}, u32[]{:S(2)}) copy-start(f32[3]{0:T(128)} %param.24) | copy-start | bytes 40
  11.0 115.6 %all-to-all-start = ((bf16[64,96,128]{2,1,0:T(8,128)(2,1)}), bf16[64,96,128]{2,1,0:T(8,128)(2,1)}, u32[]{:S(2)}, u32[]{:S(2)}) async-start(bf16[64,96,128]{2,1,0:T(8,128)(2,1)} %bitcast.17), calls=%async_computation | async-start | bytes 3145728 | tf_op jit(solution)/shard_map/all_to_all | solution.py:816
  37.7 70.8 %collective-permute-start.5 = (bf16[256,2048]{1,0:T(8,128)(2,1)}, bf16[256,2048]{1,0:T(8,128)(2,1)}, u32[]{:S(2)}, u32[]{:S(2)}) collective-permute-start(bf16[256,2048]{1,0:T(8,128)(2,1)} %bitcast.29), channel_id=1, source_target_pairs={{0,3},{1,0},{2,1},{3,2},{4,7},{5,4},{6,5},{7,6},{8,11},{9,8},{10,9... | collective-permute-start | bytes 3145736 | tf_op jit(solution)/shard_map/ppermute | solution.py:759
  50.7 65.1 %collective-permute-start.6 = (bf16[128,2048]{1,0:T(8,128)(2,1)}, bf16[128,2048]{1,0:T(8,128)(2,1)}, u32[]{:S(2)}, u32[]{:S(2)}) collective-permute-start(bf16[128,2048]{1,0:T(8,128)(2,1)} %get-tuple-element.57.refs_0_), channel_id=1, source_target_pairs={{0,3},{1,0},{2,1},{3,2},{4,7},{5,4},{6,5},{7,6},{8,11},{9,8},{10,9... | collective-permute-start | bytes 1572872 | tf_op jit(solution)/shard_map/ppermute | solution.py:826
  72.1 46.7 %collective-permute-start.7 = (bf16[128,2048]{1,0:T(8,128)(2,1)}, bf16[128,2048]{1,0:T(8,128)(2,1)}, u32[]{:S(2)}, u32[]{:S(2)}) collective-permute-start(bf16[128,2048]{1,0:T(8,128)(2,1)} %get-tuple-element.57.refs_0_), channel_id=1, source_target_pairs={{0,1},{1,2},{2,3},{3,0},{4,5},{5,6},{6,7},{7,4},{8,9},{9,10},{10,1... | collective-permute-start | bytes 1572872 | tf_op jit(solution)/shard_map/ppermute | solution.py:826
  108.5 27.6 %collective-permute-start.8 = (bf16[2048,256]{1,0:T(8,128)(2,1)}, bf16[2048,256]{1,0:T(8,128)(2,1)}, u32[]{:S(2)}, u32[]{:S(2)}) collective-permute-start(bf16[2048,256]{1,0:T(8,128)(2,1)} %collective-permute-done.refs_3_), channel_id=1, source_target_pairs={{0,1},{1,2},{2,3},{3,0},{4,5},{5,6},{6,7},{7,4},{8,9},{9,10},{10,1... | collective-permute-start | bytes 3145736 | tf_op jit(solution)/shard_map/ppermute | solution.py:767
  110.1 26.3 %collective-permute-start.9 = (bf16[2048,256]{1,0:T(8,128)(2,1)}, bf16[2048,256]{1,0:T(8,128)(2,1)}, u32[]{:S(2)}, u32[]{:S(2)}) collective-permute-start(bf16[2048,256]{1,0:T(8,128)(2,1)} %collective-permute-done.4.refs_7_), channel_id=1, source_target_pairs={{0,3},{1,0},{2,1},{3,2},{4,7},{5,4},{6,5},{7,6},{8,11},{9,8},{10,9... | collective-permute-start | bytes 3145736 | tf_op jit(solution)/shard_map/ppermute | solution.py:768
  113.7 33.1 %collective-permute-start.10 = (bf16[128,2048]{1,0:T(8,128)(2,1)}, bf16[128,2048]{1,0:T(8,128)(2,1)}, u32[]{:S(2)}, u32[]{:S(2)}) collective-permute-start(bf16[128,2048]{1,0:T(8,128)(2,1)} %slice.6), channel_id=1, source_target_pairs={{0,1},{1,2},{2,3},{3,0},{4,5},{5,6},{6,7},{7,4},{8,9},{9,10},{10,1... | collective-permute-start | bytes 1572872 | tf_op jit(solution)/shard_map/ppermute | solution.py:769
  115.9 30.9 %collective-permute-start.11 = (bf16[128,2048]{1,0:T(8,128)(2,1)}, bf16[128,2048]{1,0:T(8,128)(2,1)}, u32[]{:S(2)}, u32[]{:S(2)}) collective-permute-start(bf16[128,2048]{1,0:T(8,128)(2,1)} %slice.7), channel_id=1, source_target_pairs={{0,3},{1,0},{2,1},{3,2},{4,7},{5,4},{6,5},{7,6},{8,11},{9,8},{10,9... | collective-permute-start | bytes 1572872 | tf_op jit(solution)/shard_map/ppermute | solution.py:770
  151.3 8.6 %copy-start.1 = (bf16[128,2048]{1,0:T(8,128)(2,1)S(1)}, bf16[128,2048]{1,0:T(8,128)(2,1)}, u32[]{:S(2)}) copy-start(bf16[128,2048]{1,0:T(8,128)(2,1)} %get-tuple-element.57.refs_0_) | copy-start | bytes 1572868
  151.3 73.4 %all-to-all-start.1 = ((bf16[64,96,128]{2,1,0:T(8,128)(2,1)}), bf16[64,96,128]{2,1,0:T(8,128)(2,1)}, u32[]{:S(2)}, u32[]{:S(2)}) async-start(bf16[64,96,128]{2,1,0:T(8,128)(2,1)} %bitcast.16), calls=%async_computation.1 | async-start | bytes 3145728 | tf_op jit(solution)/shard_map/all_to_all | solution.py:816
  159.9 16.5 %collective-permute-start.15 = (bf16[128,2048]{1,0:T(8,128)(2,1)S(1)}, bf16[128,2048]{1,0:T(8,128)(2,1)}, u32[]{:S(2)}, u32[]{:S(2)}) collective-permute-start(bf16[128,2048]{1,0:T(8,128)(2,1)S(1)} %copy-done.1), channel_id=1, source_target_pairs={{0,2},{1,3},{2,0},{3,1},{4,6},{5,7},{6,4},{7,5},{8,10},{9,11},{10,... | collective-permute-start | bytes 1572872 | tf_op jit(solution)/shard_map/ppermute | solution.py:856
  162.9 57.6 %collective-permute-start.12 = (bf16[256,2048]{1,0:T(8,128)(2,1)}, bf16[256,2048]{1,0:T(8,128)(2,1)}, u32[]{:S(2)}, u32[]{:S(2)}) collective-permute-start(bf16[256,2048]{1,0:T(8,128)(2,1)} %get-tuple-element.54), channel_id=1, source_target_pairs={{0,1},{1,2},{2,3},{3,0},{4,5},{5,6},{6,7},{7,4},{8,9},{9,10},{10,1... | collective-permute-start | bytes 3145736 | tf_op jit(solution)/shard_map/ppermute | solution.py:857
  163.9 56.6 %collective-permute-start.13 = (bf16[256,2048]{1,0:T(8,128)(2,1)}, bf16[256,2048]{1,0:T(8,128)(2,1)}, u32[]{:S(2)}, u32[]{:S(2)}) collective-permute-start(bf16[256,2048]{1,0:T(8,128)(2,1)} %get-tuple-element.55), channel_id=1, source_target_pairs={{0,3},{1,0},{2,1},{3,2},{4,7},{5,4},{6,5},{7,6},{8,11},{9,8},{10,9... | collective-permute-start | bytes 3145736 | tf_op jit(solution)/shard_map/ppermute | solution.py:857
  166.1 44.0 %collective-permute-start.14 = (bf16[128,2048]{1,0:T(8,128)(2,1)}, bf16[128,2048]{1,0:T(8,128)(2,1)}, u32[]{:S(2)}, u32[]{:S(2)}) collective-permute-start(bf16[128,2048]{1,0:T(8,128)(2,1)} %get-tuple-element.56), channel_id=1, source_target_pairs={{0,2},{1,3},{2,0},{3,1},{4,6},{5,7},{6,4},{7,5},{8,10},{9,11},{10,... | collective-permute-start | bytes 1572872 | tf_op jit(solution)/shard_map/ppermute | solution.py:858
  180.5 40.0 %collective-permute-start.16 = (bf16[128,2048]{1,0:T(8,128)(2,1)}, bf16[128,2048]{1,0:T(8,128)(2,1)}, u32[]{:S(2)}, u32[]{:S(2)}) collective-permute-start(bf16[128,2048]{1,0:T(8,128)(2,1)} %shared_part.1), channel_id=1, source_target_pairs={{0,2},{1,3},{2,0},{3,1},{4,6},{5,7},{6,4},{7,5},{8,10},{9,11},{10,... | collective-permute-start | bytes 1572872 | tf_op jit(solution)/shard_map/ppermute | solution.py:863

commit v4 on v3

--- a/solution.py
+++ b/solution.py
@@ -658,24 +658,25 @@
 
 
 def sums_kernel(*refs):
-    *part_refs, far_mixer_ref, far_shared_ref, mixer_ref, shared_ref = refs
+    *part_refs, far_mixer_ref, mixer_ref, shared_ref = refs
     tokens = mixer_ref.shape[0]
-    mixer, shared = far_mixer_ref[...].astype(F32), far_shared_ref[...].astype(F32)
+    mixer, shared = far_mixer_ref[...].astype(F32), None
     for part in part_refs:
         mixer = mixer + part[:tokens].astype(F32)
-        shared = shared + part[tokens:].astype(F32)
+        term = part[tokens:].astype(F32)
+        shared = term if shared is None else shared + term
     mixer_ref[...] = mixer.astype(BF16)
     shared_ref[...] = shared
 
 
-def sums_of_parts(parts, far_mixer, far_shared):
+def sums_of_parts(parts, far_mixer):
     tokens, width = far_mixer.shape
     tile = 512
     out = pl.BlockSpec((tokens, tile), lambda c: (0, c))
     return pl.pallas_call(
         sums_kernel,
         grid=(width // tile,),
-        in_specs=[pl.BlockSpec((2 * tokens, tile), lambda c: (0, c))] * len(parts) + [out, out],
+        in_specs=[pl.BlockSpec((2 * tokens, tile), lambda c: (0, c))] * len(parts) + [out],
         out_specs=[out, out],
         out_shape=[
             jax.ShapeDtypeStruct((tokens, width), BF16),
@@ -684,10 +685,12 @@
         cost_estimate=pl.CostEstimate(flops=1_000_000_000, bytes_accessed=6_000_000, transcendentals=0),
         compiler_params=ALL_VMEM,
         name="sums_of_parts",
-    )(*parts, far_mixer, far_shared)
-
-
-def combine_kernel(shared_hbm, back_hbm, mix_hbm, out_hbm, shared, back, mix, out, sems):
+    )(*parts, far_mixer)
+
+
+def combine_kernel(
+    shared_hbm, late_hbm, back_hbm, mix_hbm, out_hbm, shared, late, back, mix, out, sems
+):
     tiles = back.shape[0]
     width = shared.shape[1]
     cuts = width // LANES
@@ -700,6 +703,7 @@
     ]
     loads.insert(1, pltpu.make_async_copy(mix_hbm, mix, sems.at[tiles]))
     loads.append(pltpu.make_async_copy(shared_hbm, shared, sems.at[tiles + 1]))
+    loads.append(pltpu.make_async_copy(late_hbm, late, sems.at[tiles + 2]))
     for copy in loads:
         copy.start()
     rows = []
@@ -707,7 +711,8 @@
         for _ in range(count):
             loads.pop(0).wait()
         rows.append(gathered(back[t], cuts))
-    loads.pop(0).wait()
+    for copy in loads:
+        copy.wait()
     rows = jnp.concatenate(rows, 0)
     hi, lo = halves(mix[...])
     both = jnp.concatenate([hi, lo], 1)
@@ -715,14 +720,15 @@
     for k in range(2):
         at = slice(k * width // 2, (k + 1) * width // 2)
         part = jnp.concatenate([rows[:, at], rows[:, at]], 0)
-        out[:, at] = (shared[:, at] + mm(both, part)).astype(BF16)
-        stores.append(pltpu.make_async_copy(out.at[:, at], out_hbm.at[:, at], sems.at[tiles + 2 + k]))
+        total = shared[:, at] + late[:, at].astype(F32)
+        out[:, at] = (total + mm(both, part)).astype(BF16)
+        stores.append(pltpu.make_async_copy(out.at[:, at], out_hbm.at[:, at], sems.at[tiles + 3 + k]))
         stores[-1].start()
     for copy in stores:
         copy.wait()
 
 
-def combine(shared, back, mix):
+def combine(shared, late, back, mix):
     tokens, width = shared.shape
     cuts = width // LANES
     tile = 128
@@ -730,19 +736,20 @@
     hbm = pl.BlockSpec(memory_space=pl.ANY)
     return pl.pallas_call(
         combine_kernel,
-        in_specs=[hbm, hbm, hbm],
+        in_specs=[hbm] * 4,
         out_specs=hbm,
         out_shape=jax.ShapeDtypeStruct((tokens, width), BF16),
         scratch_shapes=[
             pltpu.VMEM((tokens, width), F32),
+            pltpu.VMEM((tokens, width), BF16),
             pltpu.VMEM((tiles, tile * cuts, LANES), BF16),
             pltpu.VMEM(mix.shape, F32),
             pltpu.VMEM((tokens, width), BF16),
-            pltpu.SemaphoreType.DMA((tiles + 4,)),
+            pltpu.SemaphoreType.DMA((tiles + 5,)),
         ],
         compiler_params=ALL_VMEM,
         name="combine",
-    )(shared, back, mix)
+    )(shared, late, back, mix)
 
 
 def ring(axis):
@@ -854,15 +861,15 @@
     hidden = far_hidden(rows, *far[:2])
     parts, far, near, hidden, xn = lax.optimization_barrier((parts, far, near, hidden, xn))
     far_xn = lax.ppermute(xn, "tp", shift(opposite))
-    got = [parts[0]] + [lax.ppermute(parts[r], "tp", shift(r)) for r in near_peers]
     far_mixer = lax.ppermute(parts[opposite], "tp", shift(opposite))
     slot_sums = far_out(hidden, near, *far[2:])
     back = to_peers(slot_sums)
+    got = [parts[0]] + [lax.ppermute(parts[r], "tp", shift(r)) for r in near_peers]
     far_xn, slot_sums = lax.optimization_barrier((far_xn, slot_sums))
     late = shared_part(far_xn, common_gate_weight, common_up_weight, common_down_weight)
     far_shared = lax.ppermute(late, "tp", shift(opposite))
-    mixer_out, shared = sums_of_parts(got, far_mixer, far_shared)
-    return (mixer_out, combine(shared, back, mix))
+    mixer_out, shared = sums_of_parts(got, far_mixer)
+    return (mixer_out, combine(shared, far_shared, back, mix))
 
 
 def solution(mesh):

time: 229 us -> 225 us (0.983)
  waiting for transfers between devices: 84 us -> 80 us
    ppermute x1, waiting for transfers between devices: 10.4 us -> 6.33 us  [shards(): far_shared = lax.ppermute(late, 'tp', shift(opposite))]
  transfers between devices with their start and end apart: 19 -> 19, of which waited for: 8 -> 8; matrix products, arithmetic and copies ran while one was open for 2% -> 2% of each run, Pallas kernels for 36% -> 37%
where the time goes in v4:
time: 225 us; the launch traced here: 224 us
  Pallas kernels  90.2 us (40%)
  waiting for transfers between devices  80 us (36%)
  starting transfers between devices  48.5 us (22%)
  local copies, waits for them, and re-layouts  4.43 us (2%)
    pallas_call x1, Pallas kernels, entry_state(): pl.pallas_call(entry_state_kernel, in_specs=[vmem, vmem], out_specs=vmem,...  36.1 us
    ppermute x3, waiting for transfers between devices, neighbours_shards(): from_left = [lax.ppermute(w, axis, right) for w in shard]  29.5 us
    ppermute x1, waiting for transfers between devices, shards(): far_mixer = lax.ppermute(parts[opposite], 'tp', shift(opposite))  26.6 us
    all_to_all x2, starting transfers between devices, to_peers(): lax.all_to_all(parts, EP, split_axis=0, concat_axis=0, tiled=True)  21 us
    pallas_call x1, Pallas kernels, local_mixer(): pl.pallas_call(local_mixer_kernel, grid=(heads,), in_specs=[by_head, by_h...  13.7 us
    ppermute x1, waiting for transfers between devices, shards(): far_xn = lax.ppermute(xn, 'tp', shift(opposite))  10.3 us
    pallas_call x1, Pallas kernels, near_experts(): pl.pallas_call(near_experts_kernel, in_specs=[vmem] + [pl.BlockSpec(memor...  9.31 us
    ppermute x3, starting transfers between devices, neighbours_shards(): from_right = [lax.ppermute(w, axis, left) for w in shard]  8 us
  transfers between devices with their start and end apart: 19, of which 8 were waited for; matrix products, arithmetic and copies ran while one was open for 2% of the time, Pallas kernels for 37%

profile of v4, /device:TPU:8, one launch (start us, length us, event | category | flops | bytes accessed | tf_op | source)
XLA Modules:
  0.0 224.0 jit_solution(13033746433589586404)
XLA Ops:
  0.6 1.6 collective-permute-start
  2.2 1.7 collective-permute-start.3
  3.9 0.3 collective-permute-start.1
  4.2 3.0 %collective-permute-start.4 = (bf16[2048,256]{1,0:T(8,128)(2,1)}, bf16[2048,256]{1,0:T(8,128)(2,1)}, u32[]{:S(2)}, u32[]{:S(2)}) collective-permute-start(bf16[2048,256]{1,0:T(8,128)(2,1)} %bitcast.26), channel_id=1, source_target_pairs={{0,3},{1,0},{2,1},{3,2},{4,7},{5,4},{6,5},{7,6},{8,11},{9,8},{10,9... | collective-permute-start | bytes 3145736 | tf_op jit(solution)/shard_map/ppermute | solution.py:766
  7.2 0.0 collective-permute-start.2
  7.2 3.8 %dispatch.1 = (bf16[128,2048]{1,0:T(8,128)(2,1)}, bf16[6144,128]{1,0:T(8,128)(2,1)}, f32[128,384]{1,0:T(8,128)}) custom-call(bf16[128,2048]{1,0:T(8,128)(2,1)} %x_ref.1, f32[1,2048]{1,0:T(1,128)} %bitcast.18, s32[2,128]{1,0:T(2,128)} %bitcast.19, f32[2,128]{1,0:T(2,128)} %bitcast.20), custom_call_target="tpu_custom_call" | custom-call | tf_op jit(solution)/shard_map/dispatch/pallas_call | solution.py:649
  11.0 12.4 %all-to-all-start = ((bf16[64,96,128]{2,1,0:T(8,128)(2,1)}), bf16[64,96,128]{2,1,0:T(8,128)(2,1)}, u32[]{:S(2)}, u32[]{:S(2)}) async-start(bf16[64,96,128]{2,1,0:T(8,128)(2,1)} %bitcast.17), calls=%async_computation | async-start | bytes 3145728 | tf_op jit(solution)/shard_map/all_to_all | solution.py:823
  23.4 0.7 copy.21.speed_ref
  24.1 13.7 %local_mixer.1 = (f32[3,512,128]{2,1,0:T(8,128)}, f32[3,512,128]{2,1,0:T(8,128)}, f32[3,128,128]{2,1,0:T(8,128)}, f32[3,128,128]{2,1,0:T(8,128)}) custom-call(bf16[512,384]{1,0:T(8,128)(2,1)} %q_ref.1, bf16[512,384]{1,0:T(8,128)(2,1)} %k_ref.1, bf16[512,384]{1,0:T(8,128)(2,1)} %v_ref.1, f32[3,512]{1,0:T(4,128)} %bitcast.31, bf16[3,512]{1,0:T(4,128)(2,1)} %bitcast.33, ...), custom_call_target="tpu_custom_call" | custom-call | flops 30000001024 | bytes 4000000 | tf_op jit(solution)/shard_map/local_mixer/pallas_call | solution.py:178
  37.7 0.0 collective-permute-done.refs_3_
  37.7 3.3 %collective-permute-start.5 = (bf16[256,2048]{1,0:T(8,128)(2,1)}, bf16[256,2048]{1,0:T(8,128)(2,1)}, u32[]{:S(2)}, u32[]{:S(2)}) collective-permute-start(bf16[256,2048]{1,0:T(8,128)(2,1)} %bitcast.29), channel_id=1, source_target_pairs={{0,3},{1,0},{2,1},{3,2},{4,7},{5,4},{6,5},{7,6},{8,11},{9,8},{10,9... | collective-permute-start | bytes 3145736 | tf_op jit(solution)/shard_map/ppermute | solution.py:766
  41.0 9.7 %collective-permute-done.1.refs_4_ = bf16[2048,256]{1,0:T(8,128)(2,1)} collective-permute-done((bf16[2048,256]{1,0:T(8,128)(2,1)}, bf16[2048,256]{1,0:T(8,128)(2,1)}, u32[]{:S(2)}, u32[]{:S(2)}) %collective-permute-start.1) | collective-permute-done | bytes 1048608 | tf_op jit(solution)/shard_map/ppermute | solution.py:765
  50.7 1.5 collective-permute-start.6
  52.3 19.8 %collective-permute-done.2.refs_5_ = bf16[256,2048]{1,0:T(8,128)(2,1)} collective-permute-done((bf16[256,2048]{1,0:T(8,128)(2,1)}, bf16[256,2048]{1,0:T(8,128)(2,1)}, u32[]{:S(2)}, u32[]{:S(2)}) %collective-permute-start.2) | collective-permute-done | bytes 1048608 | tf_op jit(solution)/shard_map/ppermute | solution.py:765
  72.1 0.3 collective-permute-start.7
  72.4 36.1 %entry_state.1.state_ref = f32[3,128,128]{2,1,0:T(8,128)} custom-call(f32[3,128,128]{2,1,0:T(8,128)} %get-tuple-element.36.t_ref, f32[3,128,128]{2,1,0:T(8,128)} %get-tuple-element.37.i_ref), custom_call_target="tpu_custom_call" | custom-call | flops 30000001024 | bytes 4000000 | tf_op jit(solution)/shard_map/entry_state/pallas_call | solution.py:347
  108.5 0.0 collective-permute-done.4.refs_7_
  108.5 0.0 collective-permute-done.5.refs_8_
  108.5 1.6 collective-permute-start.8
  110.1 1.7 collective-permute-start.9
  111.8 1.9 slice.6
  113.7 0.3 collective-permute-start.10
  114.0 1.9 slice.7
  115.9 0.0 collective-permute-done.6.refs_1_
  115.9 2.9 %collective-permute-start.11 = (bf16[128,2048]{1,0:T(8,128)(2,1)}, bf16[128,2048]{1,0:T(8,128)(2,1)}, u32[]{:S(2)}, u32[]{:S(2)}) collective-permute-start(bf16[128,2048]{1,0:T(8,128)(2,1)} %slice.7), channel_id=1, source_target_pairs={{0,3},{1,0},{2,1},{3,2},{4,7},{5,4},{6,5},{7,6},{8,11},{9,8},{10,9... | collective-permute-start | bytes 1572872 | tf_op jit(solution)/shard_map/ppermute | solution.py:777
  118.8 0.0 collective-permute-done.7.refs_2_
  118.8 7.8 %parts_for_peers.1 = (bf16[256,2048]{1,0:T(8,128)(2,1)}, bf16[256,2048]{1,0:T(8,128)(2,1)}, bf16[128,2048]{1,0:T(8,128)(2,1)}, bf16[256,2048]{1,0:T(8,128)(2,1)}) custom-call(s32[1]{0:T(128)} %bitcast.me_ref, f32[3,512,128]{2,1,0:T(8,128)} %get-tuple-element.34.qt_ref, f32[3,512,128]{2,1,0:T(8,128)} %get-tuple-element.35.ol_ref, ...), custom_call_target="tpu_custom_call" | custom-call | flops 6000000000 | bytes 12000000 | tf_op jit(solution)/shard_map/parts_for_peers/pallas_call | solution.py:412
  126.6 0.0 all-to-all-done
  126.6 9.3 %near_experts.1 = (bf16[384,2048]{1,0:T(8,128)(2,1)}, f32[384,2048]{1,0:T(8,128)}) custom-call(bf16[6144,128]{1,0:T(8,128)(2,1)} %bitcast.13.in_ref, bf16[2048,256]{1,0:T(8,128)(2,1)} %bitcast.24, bf16[2048,256]{1,0:T(8,128)(2,1)} %bitcast.27, bf16[256,2048]{1,0:T(8,128)(2,1)} %bitcast.30, bf16[2048,256]{1,0:T(8,128)(2,1)} %collective-permute-done.refs_3_, ...), custom_call_target="tpu_custom_call" | custom-call | flops 5000000000 | bytes 16000000 | tf_op jit(solution)/shard_map/near_experts/pallas_call | solution.py:493
  135.9 0.2 collective-permute-done.8.gate_ref
  136.1 0.3 collective-permute-done.9.up_ref
  136.4 3.7 %far_hidden.1.hidden_ref = bf16[384,256]{1,0:T(8,128)(2,1)} custom-call(bf16[384,2048]{1,0:T(8,128)(2,1)} %get-tuple-element.52.x_ref, bf16[2048,256]{1,0:T(8,128)(2,1)} %collective-permute-done.8.gate_ref, bf16[2048,256]{1,0:T(8,128)(2,1)} %collective-permute-done.9.up_ref), custom_call_target="tpu_custom_call" | custom-call | flops 1500000000 | bytes 4000000 | tf_op jit(solution)/shard_map/far_hidden/pallas_call | solution.py:520
  140.1 6.7 %collective-permute-done.10.down0_ref = bf16[128,2048]{1,0:T(8,128)(2,1)} collective-permute-done((bf16[128,2048]{1,0:T(8,128)(2,1)}, bf16[128,2048]{1,0:T(8,128)(2,1)}, u32[]{:S(2)}, u32[]{:S(2)}) %collective-permute-start.10) | collective-permute-done | bytes 524320 | tf_op jit(solution)/shard_map/ppermute | solution.py:776
  146.8 4.5 %far_out.1 = bf16[6144,128]{1,0:T(8,128)(2,1)} custom-call(bf16[384,256]{1,0:T(8,128)(2,1)} %far_hidden.1.hidden_ref, f32[384,2048]{1,0:T(8,128)} %get-tuple-element.61.near_ref, bf16[128,2048]{1,0:T(8,128)(2,1)} %collective-permute-done.10.down0_ref, bf16[128,2048]{1,0:T(8,128)(2,1)} %collective-permute-done.11.down1_ref), custom_call_target="tpu_custom_call" | custom-call | flops 1500000000 | bytes 8000000 | tf_op jit(solution)/shard_map/far_out/pallas_call | solution.py:570
  151.3 0.0 copy-start.1
  151.3 8.6 %all-to-all-start.1 = ((bf16[64,96,128]{2,1,0:T(8,128)(2,1)}), bf16[64,96,128]{2,1,0:T(8,128)(2,1)}, u32[]{:S(2)}, u32[]{:S(2)}) async-start(bf16[64,96,128]{2,1,0:T(8,128)(2,1)} %bitcast.16), calls=%async_computation.1 | async-start | bytes 3145728 | tf_op jit(solution)/shard_map/all_to_all | solution.py:823
  159.9 3.0 %collective-permute-start.15 = (bf16[128,2048]{1,0:T(8,128)(2,1)S(1)}, bf16[128,2048]{1,0:T(8,128)(2,1)}, u32[]{:S(2)}, u32[]{:S(2)}) collective-permute-start(bf16[128,2048]{1,0:T(8,128)(2,1)S(1)} %copy-done.1), channel_id=1, source_target_pairs={{0,2},{1,3},{2,0},{3,1},{4,6},{5,7},{6,4},{7,5},{8,10},{9,11},{10,... | collective-permute-start | bytes 1572872 | tf_op jit(solution)/shard_map/ppermute | solution.py:863
  162.9 1.0 collective-permute-start.12
  163.9 2.3 %collective-permute-start.13 = (bf16[256,2048]{1,0:T(8,128)(2,1)}, bf16[256,2048]{1,0:T(8,128)(2,1)}, u32[]{:S(2)}, u32[]{:S(2)}) collective-permute-start(bf16[256,2048]{1,0:T(8,128)(2,1)} %get-tuple-element.55), channel_id=1, source_target_pairs={{0,3},{1,0},{2,1},{3,2},{4,7},{5,4},{6,5},{7,6},{8,11},{9,8},{10,9... | collective-permute-start | bytes 3145736 | tf_op jit(solution)/shard_map/ppermute | solution.py:867
  166.1 10.3 %collective-permute-done.15.x_ref = bf16[128,2048]{1,0:T(8,128)(2,1)} collective-permute-done((bf16[128,2048]{1,0:T(8,128)(2,1)S(1)}, bf16[128,2048]{1,0:T(8,128)(2,1)}, u32[]{:S(2)}, u32[]{:S(2)}) %collective-permute-start.15) | collective-permute-done | bytes 524320 | tf_op jit(solution)/shard_map/ppermute | solution.py:863
  176.4 4.0 %shared_part.1 = bf16[128,2048]{1,0:T(8,128)(2,1)} custom-call(bf16[128,2048]{1,0:T(8,128)(2,1)} %collective-permute-done.15.x_ref, bf16[2048,256]{1,0:T(8,128)(2,1)} %gate_ref.1, bf16[2048,256]{1,0:T(8,128)(2,1)} %up_ref.1, bf16[256,2048]{1,0:T(8,128)(2,1)} %down_hbm.1), custom_call_target="tpu_custom_call" | custom-call | flops 1000000000 | bytes 4000000 | tf_op jit(solution)/shard_map/shared_part/pallas_call | solution.py:446
  180.5 3.0 %collective-permute-start.16 = (bf16[128,2048]{1,0:T(8,128)(2,1)}, bf16[128,2048]{1,0:T(8,128)(2,1)}, u32[]{:S(2)}, u32[]{:S(2)}) collective-permute-start(bf16[128,2048]{1,0:T(8,128)(2,1)} %shared_part.1), channel_id=1, source_target_pairs={{0,2},{1,3},{2,0},{3,1},{4,6},{5,7},{6,4},{7,5},{8,10},{9,11},{10,... | collective-permute-start | bytes 1572872 | tf_op jit(solution)/shard_map/ppermute | solution.py:870
  183.5 26.6 %collective-permute-done.14.refs_3_ = bf16[128,2048]{1,0:T(8,128)(2,1)} collective-permute-done((bf16[128,2048]{1,0:T(8,128)(2,1)}, bf16[128,2048]{1,0:T(8,128)(2,1)}, u32[]{:S(2)}, u32[]{:S(2)}) %collective-permute-start.14) | collective-permute-done | bytes 524320 | tf_op jit(solution)/shard_map/ppermute | solution.py:864
  210.1 0.0 collective-permute-done.12.refs_1_
  210.1 0.0 collective-permute-done.13.refs_2_
  210.1 4.0 %sums_of_parts.1 = (bf16[128,2048]{1,0:T(8,128)(2,1)}, f32[128,2048]{1,0:T(8,128)}) custom-call(bf16[256,2048]{1,0:T(8,128)(2,1)} %get-tuple-element.53.refs_0_, bf16[256,2048]{1,0:T(8,128)(2,1)} %collective-permute-done.12.refs_1_, bf16[256,2048]{1,0:T(8,128)(2,1)} %collective-permute-done.13.refs_2_, bf16[128,2048]{1,0:T(8,128)(2,1)} %collective-permute-done.14.refs_3_), custom_call_target="tpu_custom_call" | custom-call | flops 1000000000 | bytes 6000000 | tf_op jit(solution)/shard_map/sums_of_parts/pallas_call | solution.py:676
  214.2 6.3 %collective-permute-done.16.late_hbm = bf16[128,2048]{1,0:T(8,128)(2,1)} collective-permute-done((bf16[128,2048]{1,0:T(8,128)(2,1)}, bf16[128,2048]{1,0:T(8,128)(2,1)}, u32[]{:S(2)}, u32[]{:S(2)}) %collective-permute-start.16) | collective-permute-done | bytes 524320 | tf_op jit(solution)/shard_map/ppermute | solution.py:870
  220.5 3.3 %combine.1 = bf16[128,2048]{1,0:T(8,128)(2,1)} custom-call(f32[128,2048]{1,0:T(8,128)} %get-tuple-element.58.shared_hbm, bf16[128,2048]{1,0:T(8,128)(2,1)} %collective-permute-done.16.late_hbm, bf16[6144,128]{1,0:T(8,128)(2,1)} %bitcast.15.back_hbm, f32[128,384]{1,0:T(8,128)} %get-tuple-element.65.mix_hbm), custom_call_target="tpu_custom_call" | custom-call | tf_op jit(solution)/shard_map/combine/pallas_call | solution.py:737
  (7 shorter events, 0.0 us)
Async XLA Ops:
  0.6 37.1 %collective-permute-start = (bf16[2048,256]{1,0:T(8,128)(2,1)}, bf16[2048,256]{1,0:T(8,128)(2,1)}, u32[]{:S(2)}, u32[]{:S(2)}) collective-permute-start(bf16[2048,256]{1,0:T(8,128)(2,1)} %bitcast.22), channel_id=1, source_target_pairs={{0,1},{1,2},{2,3},{3,0},{4,5},{5,6},{6,7},{7,4},{8,9},{9,10},{10,1... | collective-permute-start | bytes 3145736 | tf_op jit(solution)/shard_map/ppermute | solution.py:765
  2.2 106.3 %collective-permute-start.3 = (bf16[2048,256]{1,0:T(8,128)(2,1)}, bf16[2048,256]{1,0:T(8,128)(2,1)}, u32[]{:S(2)}, u32[]{:S(2)}) collective-permute-start(bf16[2048,256]{1,0:T(8,128)(2,1)} %bitcast.23), channel_id=1, source_target_pairs={{0,3},{1,0},{2,1},{3,2},{4,7},{5,4},{6,5},{7,6},{8,11},{9,8},{10,9... | collective-permute-start | bytes 3145736 | tf_op jit(solution)/shard_map/ppermute | solution.py:766
  3.9 46.8 %collective-permute-start.1 = (bf16[2048,256]{1,0:T(8,128)(2,1)}, bf16[2048,256]{1,0:T(8,128)(2,1)}, u32[]{:S(2)}, u32[]{:S(2)}) collective-permute-start(bf16[2048,256]{1,0:T(8,128)(2,1)} %bitcast.25), channel_id=1, source_target_pairs={{0,1},{1,2},{2,3},{3,0},{4,5},{5,6},{6,7},{7,4},{8,9},{9,10},{10,1... | collective-permute-start | bytes 3145736 | tf_op jit(solution)/shard_map/ppermute | solution.py:765
  4.2 104.2 %collective-permute-start.4 = (bf16[2048,256]{1,0:T(8,128)(2,1)}, bf16[2048,256]{1,0:T(8,128)(2,1)}, u32[]{:S(2)}, u32[]{:S(2)}) collective-permute-start(bf16[2048,256]{1,0:T(8,128)(2,1)} %bitcast.26), channel_id=1, source_target_pairs={{0,3},{1,0},{2,1},{3,2},{4,7},{5,4},{6,5},{7,6},{8,11},{9,8},{10,9... | collective-permute-start | bytes 3145736 | tf_op jit(solution)/shard_map/ppermute | solution.py:766
  7.2 64.9 %collective-permute-start.2 = (bf16[256,2048]{1,0:T(8,128)(2,1)}, bf16[256,2048]{1,0:T(8,128)(2,1)}, u32[]{:S(2)}, u32[]{:S(2)}) collective-permute-start(bf16[256,2048]{1,0:T(8,128)(2,1)} %bitcast.28), channel_id=1, source_target_pairs={{0,1},{1,2},{2,3},{3,0},{4,5},{5,6},{6,7},{7,4},{8,9},{9,10},{10,1... | collective-permute-start | bytes 3145736 | tf_op jit(solution)/shard_map/ppermute | solution.py:765
  11.0 12.4 %copy-start = (f32[3]{0:T(128)S(1)}, f32[3]{0:T(128)}, u32[]{:S(2)}) copy-start(f32[3]{0:T(128)} %param.24) | copy-start | bytes 40
  11.0 115.6 %all-to-all-start = ((bf16[64,96,128]{2,1,0:T(8,128)(2,1)}), bf16[64,96,128]{2,1,0:T(8,128)(2,1)}, u32[]{:S(2)}, u32[]{:S(2)}) async-start(bf16[64,96,128]{2,1,0:T(8,128)(2,1)} %bitcast.17), calls=%async_computation | async-start | bytes 3145728 | tf_op jit(solution)/shard_map/all_to_all | solution.py:823
  37.7 70.8 %collective-permute-start.5 = (bf16[256,2048]{1,0:T(8,128)(2,1)}, bf16[256,2048]{1,0:T(8,128)(2,1)}, u32[]{:S(2)}, u32[]{:S(2)}) collective-permute-start(bf16[256,2048]{1,0:T(8,128)(2,1)} %bitcast.29), channel_id=1, source_target_pairs={{0,3},{1,0},{2,1},{3,2},{4,7},{5,4},{6,5},{7,6},{8,11},{9,8},{10,9... | collective-permute-start | bytes 3145736 | tf_op jit(solution)/shard_map/ppermute | solution.py:766
  50.7 65.1 %collective-permute-start.6 = (bf16[128,2048]{1,0:T(8,128)(2,1)}, bf16[128,2048]{1,0:T(8,128)(2,1)}, u32[]{:S(2)}, u32[]{:S(2)}) collective-permute-start(bf16[128,2048]{1,0:T(8,128)(2,1)} %get-tuple-element.59.refs_0_), channel_id=1, source_target_pairs={{0,3},{1,0},{2,1},{3,2},{4,7},{5,4},{6,5},{7,6},{8,11},{9,8},{10,9... | collective-permute-start | bytes 1572872 | tf_op jit(solution)/shard_map/ppermute | solution.py:833
  72.1 46.7 %collective-permute-start.7 = (bf16[128,2048]{1,0:T(8,128)(2,1)}, bf16[128,2048]{1,0:T(8,128)(2,1)}, u32[]{:S(2)}, u32[]{:S(2)}) collective-permute-start(bf16[128,2048]{1,0:T(8,128)(2,1)} %get-tuple-element.59.refs_0_), channel_id=1, source_target_pairs={{0,1},{1,2},{2,3},{3,0},{4,5},{5,6},{6,7},{7,4},{8,9},{9,10},{10,1... | collective-permute-start | bytes 1572872 | tf_op jit(solution)/shard_map/ppermute | solution.py:833
  108.5 27.6 %collective-permute-start.8 = (bf16[2048,256]{1,0:T(8,128)(2,1)}, bf16[2048,256]{1,0:T(8,128)(2,1)}, u32[]{:S(2)}, u32[]{:S(2)}) collective-permute-start(bf16[2048,256]{1,0:T(8,128)(2,1)} %collective-permute-done.refs_3_), channel_id=1, source_target_pairs={{0,1},{1,2},{2,3},{3,0},{4,5},{5,6},{6,7},{7,4},{8,9},{9,10},{10,1... | collective-permute-start | bytes 3145736 | tf_op jit(solution)/shard_map/ppermute | solution.py:774
  110.1 26.3 %collective-permute-start.9 = (bf16[2048,256]{1,0:T(8,128)(2,1)}, bf16[2048,256]{1,0:T(8,128)(2,1)}, u32[]{:S(2)}, u32[]{:S(2)}) collective-permute-start(bf16[2048,256]{1,0:T(8,128)(2,1)} %collective-permute-done.4.refs_7_), channel_id=1, source_target_pairs={{0,3},{1,0},{2,1},{3,2},{4,7},{5,4},{6,5},{7,6},{8,11},{9,8},{10,9... | collective-permute-start | bytes 3145736 | tf_op jit(solution)/shard_map/ppermute | solution.py:775
  113.7 33.1 %collective-permute-start.10 = (bf16[128,2048]{1,0:T(8,128)(2,1)}, bf16[128,2048]{1,0:T(8,128)(2,1)}, u32[]{:S(2)}, u32[]{:S(2)}) collective-permute-start(bf16[128,2048]{1,0:T(8,128)(2,1)} %slice.6), channel_id=1, source_target_pairs={{0,1},{1,2},{2,3},{3,0},{4,5},{5,6},{6,7},{7,4},{8,9},{9,10},{10,1... | collective-permute-start | bytes 1572872 | tf_op jit(solution)/shard_map/ppermute | solution.py:776
  115.9 30.9 %collective-permute-start.11 = (bf16[128,2048]{1,0:T(8,128)(2,1)}, bf16[128,2048]{1,0:T(8,128)(2,1)}, u32[]{:S(2)}, u32[]{:S(2)}) collective-permute-start(bf16[128,2048]{1,0:T(8,128)(2,1)} %slice.7), channel_id=1, source_target_pairs={{0,3},{1,0},{2,1},{3,2},{4,7},{5,4},{6,5},{7,6},{8,11},{9,8},{10,9... | collective-permute-start | bytes 1572872 | tf_op jit(solution)/shard_map/ppermute | solution.py:777
  151.3 8.6 %copy-start.1 = (bf16[128,2048]{1,0:T(8,128)(2,1)S(1)}, bf16[128,2048]{1,0:T(8,128)(2,1)}, u32[]{:S(2)}) copy-start(bf16[128,2048]{1,0:T(8,128)(2,1)} %get-tuple-element.59.refs_0_) | copy-start | bytes 1572868
  151.3 69.2 %all-to-all-start.1 = ((bf16[64,96,128]{2,1,0:T(8,128)(2,1)}), bf16[64,96,128]{2,1,0:T(8,128)(2,1)}, u32[]{:S(2)}, u32[]{:S(2)}) async-start(bf16[64,96,128]{2,1,0:T(8,128)(2,1)} %bitcast.16), calls=%async_computation.1 | async-start | bytes 3145728 | tf_op jit(solution)/shard_map/all_to_all | solution.py:823
  159.9 16.5 %collective-permute-start.15 = (bf16[128,2048]{1,0:T(8,128)(2,1)S(1)}, bf16[128,2048]{1,0:T(8,128)(2,1)}, u32[]{:S(2)}, u32[]{:S(2)}) collective-permute-start(bf16[128,2048]{1,0:T(8,128)(2,1)S(1)} %copy-done.1), channel_id=1, source_target_pairs={{0,2},{1,3},{2,0},{3,1},{4,6},{5,7},{6,4},{7,5},{8,10},{9,11},{10,... | collective-permute-start | bytes 1572872 | tf_op jit(solution)/shard_map/ppermute | solution.py:863
  162.9 47.2 %collective-permute-start.12 = (bf16[256,2048]{1,0:T(8,128)(2,1)}, bf16[256,2048]{1,0:T(8,128)(2,1)}, u32[]{:S(2)}, u32[]{:S(2)}) collective-permute-start(bf16[256,2048]{1,0:T(8,128)(2,1)} %get-tuple-element.54), channel_id=1, source_target_pairs={{0,1},{1,2},{2,3},{3,0},{4,5},{5,6},{6,7},{7,4},{8,9},{9,10},{10,1... | collective-permute-start | bytes 3145736 | tf_op jit(solution)/shard_map/ppermute | solution.py:867
  163.9 46.3 %collective-permute-start.13 = (bf16[256,2048]{1,0:T(8,128)(2,1)}, bf16[256,2048]{1,0:T(8,128)(2,1)}, u32[]{:S(2)}, u32[]{:S(2)}) collective-permute-start(bf16[256,2048]{1,0:T(8,128)(2,1)} %get-tuple-element.55), channel_id=1, source_target_pairs={{0,3},{1,0},{2,1},{3,2},{4,7},{5,4},{6,5},{7,6},{8,11},{9,8},{10,9... | collective-permute-start | bytes 3145736 | tf_op jit(solution)/shard_map/ppermute | solution.py:867
  166.1 44.0 %collective-permute-start.14 = (bf16[128,2048]{1,0:T(8,128)(2,1)}, bf16[128,2048]{1,0:T(8,128)(2,1)}, u32[]{:S(2)}, u32[]{:S(2)}) collective-permute-start(bf16[128,2048]{1,0:T(8,128)(2,1)} %get-tuple-element.56), channel_id=1, source_target_pairs={{0,2},{1,3},{2,0},{3,1},{4,6},{5,7},{6,4},{7,5},{8,10},{9,11},{10,... | collective-permute-start | bytes 1572872 | tf_op jit(solution)/shard_map/ppermute | solution.py:864
  180.5 40.0 %collective-permute-start.16 = (bf16[128,2048]{1,0:T(8,128)(2,1)}, bf16[128,2048]{1,0:T(8,128)(2,1)}, u32[]{:S(2)}, u32[]{:S(2)}) collective-permute-start(bf16[128,2048]{1,0:T(8,128)(2,1)} %shared_part.1), channel_id=1, source_target_pairs={{0,2},{1,3},{2,0},{3,1},{4,6},{5,7},{6,4},{7,5},{8,10},{9,11},{10,... | collective-permute-start | bytes 1572872 | tf_op jit(solution)/shard_map/ppermute | solution.py:870

commit v5 on v4

--- a/solution.py
+++ b/solution.py
@@ -371,7 +371,7 @@
     near = [r for r in range(peers) if r != far]
     count = len(near)
     hbm, refs = refs[: count + 3], refs[count + 3 :]
-    out_refs, (x, gate, up, down, sems) = refs[:peers], refs[peers:]
+    out_refs, far_b, (x, gate, up, down, sems) = refs[:peers], refs[peers], refs[peers + 1 :]
     heads, rows, _ = qt_ref.shape
     tile = rows // peers
     spots = [x.at[r * tile : (r + 1) * tile] for r in range(count)] + [gate, up, down]
@@ -392,8 +392,10 @@
         out = out * lax.rsqrt(jnp.mean(out * out, axis=1, keepdims=True) + EPS) * gain_ref[...]
         normed.append(out.astype(BF16))
     mixer = mm(jnp.concatenate(normed, 1), w_ref[...]).astype(BF16)
-    for r in range(peers):
+    for r in near:
         out_refs[r][:tile] = mixer[r * tile : (r + 1) * tile]
+    out_refs[far][...] = mixer[far * tile : far * tile + tile // 2]
+    far_b[...] = mixer[far * tile + tile // 2 : (far + 1) * tile]
     for copy in copies:
         copy.wait()
     hidden = gated(mm(x[...], gate[...]), mm(x[...], up[...]))
@@ -414,10 +416,10 @@
         in_specs=[pl.BlockSpec(memory_space=pltpu.SMEM)]
         + [vmem] * 5
         + [pl.BlockSpec(memory_space=pl.ANY)] * len(kept),
-        out_specs=[vmem] * peers,
+        out_specs=[vmem] * (peers + 1),
         out_shape=[
-            jax.ShapeDtypeStruct((tile if r == peers // 2 else 2 * tile, width), BF16)
-            for r in range(peers)
+            jax.ShapeDtypeStruct((tile // 2 if r in (peers // 2, peers) else 2 * tile, width), BF16)
+            for r in range(peers + 1)
         ],
         scratch_shapes=[
             pltpu.VMEM((len(tokens) * tile, width), BF16),
@@ -658,25 +660,24 @@
 
 
 def sums_kernel(*refs):
-    *part_refs, far_mixer_ref, mixer_ref, shared_ref = refs
+    *part_refs, mixer_ref, shared_ref = refs
     tokens = mixer_ref.shape[0]
-    mixer, shared = far_mixer_ref[...].astype(F32), None
-    for part in part_refs:
+    mixer, shared = [part_refs[0][at].astype(F32) for at in (slice(tokens), slice(tokens, None))]
+    for part in part_refs[1:]:
         mixer = mixer + part[:tokens].astype(F32)
-        term = part[tokens:].astype(F32)
-        shared = term if shared is None else shared + term
+        shared = shared + part[tokens:].astype(F32)
     mixer_ref[...] = mixer.astype(BF16)
     shared_ref[...] = shared
 
 
-def sums_of_parts(parts, far_mixer):
-    tokens, width = far_mixer.shape
+def sums_of_parts(parts):
+    tokens, width = parts[0].shape[0] // 2, parts[0].shape[1]
     tile = 512
     out = pl.BlockSpec((tokens, tile), lambda c: (0, c))
     return pl.pallas_call(
         sums_kernel,
         grid=(width // tile,),
-        in_specs=[pl.BlockSpec((2 * tokens, tile), lambda c: (0, c))] * len(parts) + [out],
+        in_specs=[pl.BlockSpec((2 * tokens, tile), lambda c: (0, c))] * len(parts),
         out_specs=[out, out],
         out_shape=[
             jax.ShapeDtypeStruct((tokens, width), BF16),
@@ -685,7 +686,36 @@
         cost_estimate=pl.CostEstimate(flops=1_000_000_000, bytes_accessed=6_000_000, transcendentals=0),
         compiler_params=ALL_VMEM,
         name="sums_of_parts",
-    )(*parts, far_mixer)
+    )(*parts)
+
+
+def joined_kernel(right_ref, left_ref, a_ref, b_ref, right_out, left_out):
+    half = a_ref.shape[0]
+    rows = right_ref.shape[0]
+    right_out[:half] = (right_ref[:half].astype(F32) + a_ref[...].astype(F32)).astype(BF16)
+    right_out[half:] = right_ref[half:]
+    left_out[:half] = left_ref[:half]
+    left_out[half : 2 * half] = (
+        left_ref[half : 2 * half].astype(F32) + b_ref[...].astype(F32)
+    ).astype(BF16)
+    left_out[2 * half : rows] = left_ref[2 * half : rows]
+
+
+def joined(right, left, a, b):
+    rows, width = right.shape
+    tile = 512
+    whole = pl.BlockSpec((rows, tile), lambda c: (0, c))
+    half = pl.BlockSpec((a.shape[0], tile), lambda c: (0, c))
+    return pl.pallas_call(
+        joined_kernel,
+        grid=(width // tile,),
+        in_specs=[whole, whole, half, half],
+        out_specs=[whole, whole],
+        out_shape=[jax.ShapeDtypeStruct(right.shape, BF16)] * 2,
+        cost_estimate=pl.CostEstimate(flops=500_000_000, bytes_accessed=5_000_000, transcendentals=0),
+        compiler_params=ALL_VMEM,
+        name="joined",
+    )(right, left, a, b)
 
 
 def combine_kernel(
@@ -861,14 +891,20 @@
     hidden = far_hidden(rows, *far[:2])
     parts, far, near, hidden, xn = lax.optimization_barrier((parts, far, near, hidden, xn))
     far_xn = lax.ppermute(xn, "tp", shift(opposite))
-    far_mixer = lax.ppermute(parts[opposite], "tp", shift(opposite))
+    far_a = lax.ppermute(parts[opposite], "tp", shift(1))
+    far_b = lax.ppermute(parts[peers], "tp", shift(peers - 1))
     slot_sums = far_out(hidden, near, *far[2:])
     back = to_peers(slot_sums)
-    got = [parts[0]] + [lax.ppermute(parts[r], "tp", shift(r)) for r in near_peers]
-    far_xn, slot_sums = lax.optimization_barrier((far_xn, slot_sums))
+    far_xn, far_a, slot_sums = lax.optimization_barrier((far_xn, far_a, slot_sums))
+    to_right, to_left = joined(parts[1], parts[peers - 1], far_a, far_b)
+    got = [
+        parts[0],
+        lax.ppermute(to_right, "tp", shift(1)),
+        lax.ppermute(to_left, "tp", shift(peers - 1)),
+    ]
     late = shared_part(far_xn, common_gate_weight, common_up_weight, common_down_weight)
     far_shared = lax.ppermute(late, "tp", shift(opposite))
-    mixer_out, shared = sums_of_parts(got, far_mixer)
+    mixer_out, shared = sums_of_parts(got)
     return (mixer_out, combine(shared, far_shared, back, mix))
 
 

time: 225 us -> 232 us (1.031)
  Pallas kernels: 90.2 us -> 94 us
    ppermute x3 -> x4, waiting for transfers between devices: 26.6 us -> 44.3 us  [the longest x1 18 us: shards(): lax.ppermute(to_right, 'tp', shift(1))]
    ppermute x1, waiting for transfers between devices: 10.3 us -> 0.01 us  [shards(): far_xn = lax.ppermute(xn, 'tp', shift(opposite))]
    ppermute x1, waiting for transfers between devices: 6.33 us -> 0.01 us  [shards(): far_shared = lax.ppermute(late, 'tp', shift(opposite))]
    pallas_call x0 -> x1, Pallas kernels: none -> 3.89 us  [joined(): pl.pallas_call(joined_kernel, grid=(width // tile,), in_specs=[whole, who...]
    ppermute x3 -> x4, starting transfers between devices: 3.24 us -> 6.47 us  [the longest x1 2.25 us: shards(): far_b = lax.ppermute(parts[peers], 'tp', shift(peers - 1))]
  transfers between devices with their start and end apart: 19 -> 20, of which waited for: 8 -> 9; matrix products, arithmetic and copies ran while one was open for 2% -> 2% of each run, Pallas kernels for 37% -> 37%
where the time goes in v5:
time: 232 us; the launch traced here: 230 us
  Pallas kernels  94 us (41%)
  waiting for transfers between devices  81 us (35%)
  starting transfers between devices  49.6 us (21%)
  local copies, waits for them, and re-layouts  4.48 us (2%)
    pallas_call x1, Pallas kernels, entry_state(): pl.pallas_call(entry_state_kernel, in_specs=[vmem, vmem], out_specs=vmem,...  36.1 us
    ppermute x3, waiting for transfers between devices, neighbours_shards(): from_left = [lax.ppermute(w, axis, right) for w in shard]  29.5 us
    all_to_all x2, starting transfers between devices, to_peers(): lax.all_to_all(parts, EP, split_axis=0, concat_axis=0, tiled=True)  21 us
    ppermute x1, waiting for transfers between devices, shards(): lax.ppermute(to_right, 'tp', shift(1))  18 us
    ppermute x1, waiting for transfers between devices, shards(): far_a = lax.ppermute(parts[opposite], 'tp', shift(1))  15 us
    pallas_call x1, Pallas kernels, local_mixer(): pl.pallas_call(local_mixer_kernel, grid=(heads,), in_specs=[by_head, by_h...  13.7 us
    ppermute x1, waiting for transfers between devices, shards(): lax.ppermute(to_left, 'tp', shift(peers - 1))  10.9 us
    pallas_call x1, Pallas kernels, near_experts(): pl.pallas_call(near_experts_kernel, in_specs=[vmem] + [pl.BlockSpec(memor...  9.33 us
  transfers between devices with their start and end apart: 20, of which 9 were waited for; matrix products, arithmetic and copies ran while one was open for 2% of the time, Pallas kernels for 37%

profile of v5, /device:TPU:8, one launch (start us, length us, event | category | flops | bytes accessed | tf_op | source)
XLA Modules:
  0.0 230.1 jit_solution(339609924511225741)
XLA Ops:
  0.6 1.6 collective-permute-start
  2.2 1.7 collective-permute-start.3
  3.9 0.3 collective-permute-start.1
  4.2 3.0 %collective-permute-start.4 = (bf16[2048,256]{1,0:T(8,128)(2,1)}, bf16[2048,256]{1,0:T(8,128)(2,1)}, u32[]{:S(2)}, u32[]{:S(2)}) collective-permute-start(bf16[2048,256]{1,0:T(8,128)(2,1)} %bitcast.26), channel_id=1, source_target_pairs={{0,3},{1,0},{2,1},{3,2},{4,7},{5,4},{6,5},{7,6},{8,11},{9,8},{10,9... | collective-permute-start | bytes 3145736 | tf_op jit(solution)/shard_map/ppermute | solution.py:796
  7.2 0.0 collective-permute-start.2
  7.2 3.8 %dispatch.1 = (bf16[128,2048]{1,0:T(8,128)(2,1)}, bf16[6144,128]{1,0:T(8,128)(2,1)}, f32[128,384]{1,0:T(8,128)}) custom-call(bf16[128,2048]{1,0:T(8,128)(2,1)} %x_ref.1, f32[1,2048]{1,0:T(1,128)} %bitcast.18, s32[2,128]{1,0:T(2,128)} %bitcast.19, f32[2,128]{1,0:T(2,128)} %bitcast.20), custom_call_target="tpu_custom_call" | custom-call | tf_op jit(solution)/shard_map/dispatch/pallas_call | solution.py:651
  11.0 12.4 %all-to-all-start = ((bf16[64,96,128]{2,1,0:T(8,128)(2,1)}), bf16[64,96,128]{2,1,0:T(8,128)(2,1)}, u32[]{:S(2)}, u32[]{:S(2)}) async-start(bf16[64,96,128]{2,1,0:T(8,128)(2,1)} %bitcast.17), calls=%async_computation | async-start | bytes 3145728 | tf_op jit(solution)/shard_map/all_to_all | solution.py:853
  23.4 0.7 copy.21.speed_ref
  24.1 13.7 %local_mixer.1 = (f32[3,512,128]{2,1,0:T(8,128)}, f32[3,512,128]{2,1,0:T(8,128)}, f32[3,128,128]{2,1,0:T(8,128)}, f32[3,128,128]{2,1,0:T(8,128)}) custom-call(bf16[512,384]{1,0:T(8,128)(2,1)} %q_ref.1, bf16[512,384]{1,0:T(8,128)(2,1)} %k_ref.1, bf16[512,384]{1,0:T(8,128)(2,1)} %v_ref.1, f32[3,512]{1,0:T(4,128)} %bitcast.31, bf16[3,512]{1,0:T(4,128)(2,1)} %bitcast.33, ...), custom_call_target="tpu_custom_call" | custom-call | flops 30000001024 | bytes 4000000 | tf_op jit(solution)/shard_map/local_mixer/pallas_call | solution.py:178
  37.7 3.3 %collective-permute-start.5 = (bf16[256,2048]{1,0:T(8,128)(2,1)}, bf16[256,2048]{1,0:T(8,128)(2,1)}, u32[]{:S(2)}, u32[]{:S(2)}) collective-permute-start(bf16[256,2048]{1,0:T(8,128)(2,1)} %bitcast.29), channel_id=1, source_target_pairs={{0,3},{1,0},{2,1},{3,2},{4,7},{5,4},{6,5},{7,6},{8,11},{9,8},{10,9... | collective-permute-start | bytes 3145736 | tf_op jit(solution)/shard_map/ppermute | solution.py:796
  41.1 9.7 %collective-permute-done.1.refs_4_ = bf16[2048,256]{1,0:T(8,128)(2,1)} collective-permute-done((bf16[2048,256]{1,0:T(8,128)(2,1)}, bf16[2048,256]{1,0:T(8,128)(2,1)}, u32[]{:S(2)}, u32[]{:S(2)}) %collective-permute-start.1) | collective-permute-done | bytes 1048608 | tf_op jit(solution)/shard_map/ppermute | solution.py:795
  50.7 1.5 collective-permute-start.6
  52.3 19.8 %collective-permute-done.2.refs_5_ = bf16[256,2048]{1,0:T(8,128)(2,1)} collective-permute-done((bf16[256,2048]{1,0:T(8,128)(2,1)}, bf16[256,2048]{1,0:T(8,128)(2,1)}, u32[]{:S(2)}, u32[]{:S(2)}) %collective-permute-start.2) | collective-permute-done | bytes 1048608 | tf_op jit(solution)/shard_map/ppermute | solution.py:795
  72.1 0.3 collective-permute-start.7
  72.4 36.1 %entry_state.1.state_ref = f32[3,128,128]{2,1,0:T(8,128)} custom-call(f32[3,128,128]{2,1,0:T(8,128)} %get-tuple-element.41.t_ref, f32[3,128,128]{2,1,0:T(8,128)} %get-tuple-element.42.i_ref), custom_call_target="tpu_custom_call" | custom-call | flops 30000001024 | bytes 4000000 | tf_op jit(solution)/shard_map/entry_state/pallas_call | solution.py:347
  108.5 0.0 collective-permute-done.3.refs_6_
  108.5 1.6 collective-permute-start.8
  110.1 1.7 collective-permute-start.9
  111.8 1.9 slice.6
  113.7 0.3 collective-permute-start.10
  114.0 1.9 slice.7
  115.9 0.0 collective-permute-done.6.refs_1_
  115.9 2.9 %collective-permute-start.11 = (bf16[128,2048]{1,0:T(8,128)(2,1)}, bf16[128,2048]{1,0:T(8,128)(2,1)}, u32[]{:S(2)}, u32[]{:S(2)}) collective-permute-start(bf16[128,2048]{1,0:T(8,128)(2,1)} %slice.7), channel_id=1, source_target_pairs={{0,3},{1,0},{2,1},{3,2},{4,7},{5,4},{6,5},{7,6},{8,11},{9,8},{10,9... | collective-permute-start | bytes 1572872 | tf_op jit(solution)/shard_map/ppermute | solution.py:807
  118.8 0.0 collective-permute-done.7.refs_2_
  118.8 7.7 %parts_for_peers.1 = (bf16[256,2048]{1,0:T(8,128)(2,1)}, bf16[256,2048]{1,0:T(8,128)(2,1)}, bf16[64,2048]{1,0:T(8,128)(2,1)}, bf16[256,2048]{1,0:T(8,128)(2,1)}, bf16[64,2048]{1,0:T(8,128)(2,1)}) custom-call(s32[1]{0:T(128)} %bitcast.me_ref, f32[3,512,128]{2,1,0:T(8,128)} %get-tuple-element.39.qt_ref, f32[3,512,128]{2,1,0:T(8,128)} %get-tuple-element.40.ol_ref, ...), custom_call_target="tpu_custom_call" | custom-call | flops 6000000000 | bytes 12000000 | tf_op jit(solution)/shard_map/parts_for_peers/pallas_call | solution.py:414
  126.6 0.0 all-to-all-done
  126.6 9.3 %near_experts.1 = (bf16[384,2048]{1,0:T(8,128)(2,1)}, f32[384,2048]{1,0:T(8,128)}) custom-call(bf16[6144,128]{1,0:T(8,128)(2,1)} %bitcast.13.in_ref, bf16[2048,256]{1,0:T(8,128)(2,1)} %bitcast.24, bf16[2048,256]{1,0:T(8,128)(2,1)} %bitcast.27, bf16[256,2048]{1,0:T(8,128)(2,1)} %bitcast.30, bf16[2048,256]{1,0:T(8,128)(2,1)} %collective-permute-done.refs_3_, ...), custom_call_target="tpu_custom_call" | custom-call | flops 5000000000 | bytes 16000000 | tf_op jit(solution)/shard_map/near_experts/pallas_call | solution.py:495
  135.9 0.2 collective-permute-done.8.gate_ref
  136.1 0.3 collective-permute-done.9.up_ref
  136.4 3.7 %far_hidden.1.hidden_ref = bf16[384,256]{1,0:T(8,128)(2,1)} custom-call(bf16[384,2048]{1,0:T(8,128)(2,1)} %get-tuple-element.58.x_ref, bf16[2048,256]{1,0:T(8,128)(2,1)} %collective-permute-done.8.gate_ref, bf16[2048,256]{1,0:T(8,128)(2,1)} %collective-permute-done.9.up_ref), custom_call_target="tpu_custom_call" | custom-call | flops 1500000000 | bytes 4000000 | tf_op jit(solution)/shard_map/far_hidden/pallas_call | solution.py:522
  140.1 6.7 %collective-permute-done.10.down0_ref = bf16[128,2048]{1,0:T(8,128)(2,1)} collective-permute-done((bf16[128,2048]{1,0:T(8,128)(2,1)}, bf16[128,2048]{1,0:T(8,128)(2,1)}, u32[]{:S(2)}, u32[]{:S(2)}) %collective-permute-start.10) | collective-permute-done | bytes 524320 | tf_op jit(solution)/shard_map/ppermute | solution.py:806
  146.8 4.5 %far_out.1 = bf16[6144,128]{1,0:T(8,128)(2,1)} custom-call(bf16[384,256]{1,0:T(8,128)(2,1)} %far_hidden.1.hidden_ref, f32[384,2048]{1,0:T(8,128)} %get-tuple-element.65.near_ref, bf16[128,2048]{1,0:T(8,128)(2,1)} %collective-permute-done.10.down0_ref, bf16[128,2048]{1,0:T(8,128)(2,1)} %collective-permute-done.11.down1_ref), custom_call_target="tpu_custom_call" | custom-call | flops 1500000000 | bytes 8000000 | tf_op jit(solution)/shard_map/far_out/pallas_call | solution.py:572
  151.3 0.0 copy-start.1
  151.3 8.6 %all-to-all-start.1 = ((bf16[64,96,128]{2,1,0:T(8,128)(2,1)}), bf16[64,96,128]{2,1,0:T(8,128)(2,1)}, u32[]{:S(2)}, u32[]{:S(2)}) async-start(bf16[64,96,128]{2,1,0:T(8,128)(2,1)} %bitcast.16), calls=%async_computation.1 | async-start | bytes 3145728 | tf_op jit(solution)/shard_map/all_to_all | solution.py:853
  159.9 3.0 %collective-permute-start.12 = (bf16[128,2048]{1,0:T(8,128)(2,1)S(1)}, bf16[128,2048]{1,0:T(8,128)(2,1)}, u32[]{:S(2)}, u32[]{:S(2)}) collective-permute-start(bf16[128,2048]{1,0:T(8,128)(2,1)S(1)} %copy-done.1), channel_id=1, source_target_pairs={{0,2},{1,3},{2,0},{3,1},{4,6},{5,7},{6,4},{7,5},{8,10},{9,11},{10,... | collective-permute-start | bytes 1572872 | tf_op jit(solution)/shard_map/ppermute | solution.py:893
  162.9 1.0 collective-permute-start.13
  163.9 2.3 collective-permute-start.14
  166.2 15.0 %collective-permute-done.13.a_ref = bf16[64,2048]{1,0:T(8,128)(2,1)} collective-permute-done((bf16[64,2048]{1,0:T(8,128)(2,1)S(1)}, bf16[64,2048]{1,0:T(8,128)(2,1)}, u32[]{:S(2)}, u32[]{:S(2)}) %collective-permute-start.13) | collective-permute-done | bytes 262176 | tf_op jit(solution)/shard_map/ppermute | solution.py:894
  181.2 0.4 collective-permute-done.14.b_ref
  181.6 3.9 %joined.1 = (bf16[256,2048]{1,0:T(8,128)(2,1)}, bf16[256,2048]{1,0:T(8,128)(2,1)}) custom-call(bf16[256,2048]{1,0:T(8,128)(2,1)} %get-tuple-element.60.right_ref, bf16[256,2048]{1,0:T(8,128)(2,1)} %get-tuple-element.61.left_ref, bf16[64,2048]{1,0:T(8,128)(2,1)} %collective-permute-done.13.a_ref, bf16[64,2048]{1,0:T(8,128)(2,1)} %collective-permute-done.14.b_ref), custom_call_target="tpu_custom_call" | custom-call | flops 500000000 | bytes 5000000 | tf_op jit(solution)/shard_map/joined/pallas_call | solution.py:709
  185.5 1.1 collective-permute-start.15
  186.6 2.2 collective-permute-start.16
  188.7 4.0 %shared_part.1 = bf16[128,2048]{1,0:T(8,128)(2,1)} custom-call(bf16[128,2048]{1,0:T(8,128)(2,1)} %collective-permute-done.12.x_ref, bf16[2048,256]{1,0:T(8,128)(2,1)} %gate_ref.1, bf16[2048,256]{1,0:T(8,128)(2,1)} %up_ref.1, bf16[256,2048]{1,0:T(8,128)(2,1)} %down_hbm.1), custom_call_target="tpu_custom_call" | custom-call | flops 1000000000 | bytes 4000000 | tf_op jit(solution)/shard_map/shared_part/pallas_call | solution.py:448
  192.8 0.9 collective-permute-start.17
  193.7 18.0 %collective-permute-done.15.refs_1_ = bf16[256,2048]{1,0:T(8,128)(2,1)} collective-permute-done((bf16[256,2048]{1,0:T(8,128)(2,1)}, bf16[256,2048]{1,0:T(8,128)(2,1)}, u32[]{:S(2)}, u32[]{:S(2)}) %collective-permute-start.15) | collective-permute-done | bytes 1048608 | tf_op jit(solution)/shard_map/ppermute | solution.py:902
  211.8 10.9 %collective-permute-done.16.refs_2_ = bf16[256,2048]{1,0:T(8,128)(2,1)} collective-permute-done((bf16[256,2048]{1,0:T(8,128)(2,1)}, bf16[256,2048]{1,0:T(8,128)(2,1)}, u32[]{:S(2)}, u32[]{:S(2)}) %collective-permute-start.16) | collective-permute-done | bytes 1048608 | tf_op jit(solution)/shard_map/ppermute | solution.py:903
  222.6 3.9 %sums_of_parts.1 = (bf16[128,2048]{1,0:T(8,128)(2,1)}, f32[128,2048]{1,0:T(8,128)}) custom-call(bf16[256,2048]{1,0:T(8,128)(2,1)} %get-tuple-element.59.refs_0_, bf16[256,2048]{1,0:T(8,128)(2,1)} %collective-permute-done.15.refs_1_, bf16[256,2048]{1,0:T(8,128)(2,1)} %collective-permute-done.16.refs_2_), custom_call_target="tpu_custom_call" | custom-call | flops 1000000000 | bytes 6000000 | tf_op jit(solution)/shard_map/sums_of_parts/pallas_call | solution.py:677
  226.6 3.3 %combine.1 = bf16[128,2048]{1,0:T(8,128)(2,1)} custom-call(f32[128,2048]{1,0:T(8,128)} %get-tuple-element.73.shared_hbm, bf16[128,2048]{1,0:T(8,128)(2,1)} %collective-permute-done.17.late_hbm, bf16[6144,128]{1,0:T(8,128)(2,1)} %bitcast.15.back_hbm, f32[128,384]{1,0:T(8,128)} %get-tuple-element.75.mix_hbm), custom_call_target="tpu_custom_call" | custom-call | tf_op jit(solution)/shard_map/combine/pallas_call | solution.py:767
  (14 shorter events, 0.0 us)
Async XLA Ops:
  0.6 37.1 %collective-permute-start = (bf16[2048,256]{1,0:T(8,128)(2,1)}, bf16[2048,256]{1,0:T(8,128)(2,1)}, u32[]{:S(2)}, u32[]{:S(2)}) collective-permute-start(bf16[2048,256]{1,0:T(8,128)(2,1)} %bitcast.22), channel_id=1, source_target_pairs={{0,1},{1,2},{2,3},{3,0},{4,5},{5,6},{6,7},{7,4},{8,9},{9,10},{10,1... | collective-permute-start | bytes 3145736 | tf_op jit(solution)/shard_map/ppermute | solution.py:795
  2.2 106.3 %collective-permute-start.3 = (bf16[2048,256]{1,0:T(8,128)(2,1)}, bf16[2048,256]{1,0:T(8,128)(2,1)}, u32[]{:S(2)}, u32[]{:S(2)}) collective-permute-start(bf16[2048,256]{1,0:T(8,128)(2,1)} %bitcast.23), channel_id=1, source_target_pairs={{0,3},{1,0},{2,1},{3,2},{4,7},{5,4},{6,5},{7,6},{8,11},{9,8},{10,9... | collective-permute-start | bytes 3145736 | tf_op jit(solution)/shard_map/ppermute | solution.py:796
  3.9 46.8 %collective-permute-start.1 = (bf16[2048,256]{1,0:T(8,128)(2,1)}, bf16[2048,256]{1,0:T(8,128)(2,1)}, u32[]{:S(2)}, u32[]{:S(2)}) collective-permute-start(bf16[2048,256]{1,0:T(8,128)(2,1)} %bitcast.25), channel_id=1, source_target_pairs={{0,1},{1,2},{2,3},{3,0},{4,5},{5,6},{6,7},{7,4},{8,9},{9,10},{10,1... | collective-permute-start | bytes 3145736 | tf_op jit(solution)/shard_map/ppermute | solution.py:795
  4.2 104.2 %collective-permute-start.4 = (bf16[2048,256]{1,0:T(8,128)(2,1)}, bf16[2048,256]{1,0:T(8,128)(2,1)}, u32[]{:S(2)}, u32[]{:S(2)}) collective-permute-start(bf16[2048,256]{1,0:T(8,128)(2,1)} %bitcast.26), channel_id=1, source_target_pairs={{0,3},{1,0},{2,1},{3,2},{4,7},{5,4},{6,5},{7,6},{8,11},{9,8},{10,9... | collective-permute-start | bytes 3145736 | tf_op jit(solution)/shard_map/ppermute | solution.py:796
  7.2 64.9 %collective-permute-start.2 = (bf16[256,2048]{1,0:T(8,128)(2,1)}, bf16[256,2048]{1,0:T(8,128)(2,1)}, u32[]{:S(2)}, u32[]{:S(2)}) collective-permute-start(bf16[256,2048]{1,0:T(8,128)(2,1)} %bitcast.28), channel_id=1, source_target_pairs={{0,1},{1,2},{2,3},{3,0},{4,5},{5,6},{6,7},{7,4},{8,9},{9,10},{10,1... | collective-permute-start | bytes 3145736 | tf_op jit(solution)/shard_map/ppermute | solution.py:795
  11.0 12.4 %copy-start = (f32[3]{0:T(128)S(1)}, f32[3]{0:T(128)}, u32[]{:S(2)}) copy-start(f32[3]{0:T(128)} %param.24) | copy-start | bytes 40
  11.0 115.6 %all-to-all-start = ((bf16[64,96,128]{2,1,0:T(8,128)(2,1)}), bf16[64,96,128]{2,1,0:T(8,128)(2,1)}, u32[]{:S(2)}, u32[]{:S(2)}) async-start(bf16[64,96,128]{2,1,0:T(8,128)(2,1)} %bitcast.17), calls=%async_computation | async-start | bytes 3145728 | tf_op jit(solution)/shard_map/all_to_all | solution.py:853
  37.7 70.7 %collective-permute-start.5 = (bf16[256,2048]{1,0:T(8,128)(2,1)}, bf16[256,2048]{1,0:T(8,128)(2,1)}, u32[]{:S(2)}, u32[]{:S(2)}) collective-permute-start(bf16[256,2048]{1,0:T(8,128)(2,1)} %bitcast.29), channel_id=1, source_target_pairs={{0,3},{1,0},{2,1},{3,2},{4,7},{5,4},{6,5},{7,6},{8,11},{9,8},{10,9... | collective-permute-start | bytes 3145736 | tf_op jit(solution)/shard_map/ppermute | solution.py:796
  50.7 65.2 %collective-permute-start.6 = (bf16[128,2048]{1,0:T(8,128)(2,1)}, bf16[128,2048]{1,0:T(8,128)(2,1)}, u32[]{:S(2)}, u32[]{:S(2)}) collective-permute-start(bf16[128,2048]{1,0:T(8,128)(2,1)} %get-tuple-element.62.refs_0_), channel_id=1, source_target_pairs={{0,3},{1,0},{2,1},{3,2},{4,7},{5,4},{6,5},{7,6},{8,11},{9,8},{10,9... | collective-permute-start | bytes 1572872 | tf_op jit(solution)/shard_map/ppermute | solution.py:863
  72.1 46.8 %collective-permute-start.7 = (bf16[128,2048]{1,0:T(8,128)(2,1)}, bf16[128,2048]{1,0:T(8,128)(2,1)}, u32[]{:S(2)}, u32[]{:S(2)}) collective-permute-start(bf16[128,2048]{1,0:T(8,128)(2,1)} %get-tuple-element.62.refs_0_), channel_id=1, source_target_pairs={{0,1},{1,2},{2,3},{3,0},{4,5},{5,6},{6,7},{7,4},{8,9},{9,10},{10,1... | collective-permute-start | bytes 1572872 | tf_op jit(solution)/shard_map/ppermute | solution.py:863
  108.5 27.6 %collective-permute-start.8 = (bf16[2048,256]{1,0:T(8,128)(2,1)}, bf16[2048,256]{1,0:T(8,128)(2,1)}, u32[]{:S(2)}, u32[]{:S(2)}) collective-permute-start(bf16[2048,256]{1,0:T(8,128)(2,1)} %collective-permute-done.refs_3_), channel_id=1, source_target_pairs={{0,1},{1,2},{2,3},{3,0},{4,5},{5,6},{6,7},{7,4},{8,9},{9,10},{10,1... | collective-permute-start | bytes 3145736 | tf_op jit(solution)/shard_map/ppermute | solution.py:804
  110.1 26.3 %collective-permute-start.9 = (bf16[2048,256]{1,0:T(8,128)(2,1)}, bf16[2048,256]{1,0:T(8,128)(2,1)}, u32[]{:S(2)}, u32[]{:S(2)}) collective-permute-start(bf16[2048,256]{1,0:T(8,128)(2,1)} %collective-permute-done.4.refs_7_), channel_id=1, source_target_pairs={{0,3},{1,0},{2,1},{3,2},{4,7},{5,4},{6,5},{7,6},{8,11},{9,8},{10,9... | collective-permute-start | bytes 3145736 | tf_op jit(solution)/shard_map/ppermute | solution.py:805
  113.7 33.1 %collective-permute-start.10 = (bf16[128,2048]{1,0:T(8,128)(2,1)}, bf16[128,2048]{1,0:T(8,128)(2,1)}, u32[]{:S(2)}, u32[]{:S(2)}) collective-permute-start(bf16[128,2048]{1,0:T(8,128)(2,1)} %slice.6), channel_id=1, source_target_pairs={{0,1},{1,2},{2,3},{3,0},{4,5},{5,6},{6,7},{7,4},{8,9},{9,10},{10,1... | collective-permute-start | bytes 1572872 | tf_op jit(solution)/shard_map/ppermute | solution.py:806
  115.9 30.9 %collective-permute-start.11 = (bf16[128,2048]{1,0:T(8,128)(2,1)}, bf16[128,2048]{1,0:T(8,128)(2,1)}, u32[]{:S(2)}, u32[]{:S(2)}) collective-permute-start(bf16[128,2048]{1,0:T(8,128)(2,1)} %slice.7), channel_id=1, source_target_pairs={{0,3},{1,0},{2,1},{3,2},{4,7},{5,4},{6,5},{7,6},{8,11},{9,8},{10,9... | collective-permute-start | bytes 1572872 | tf_op jit(solution)/shard_map/ppermute | solution.py:807
  151.3 8.6 %copy-start.1 = (bf16[128,2048]{1,0:T(8,128)(2,1)S(1)}, bf16[128,2048]{1,0:T(8,128)(2,1)}, u32[]{:S(2)}) copy-start(bf16[128,2048]{1,0:T(8,128)(2,1)} %get-tuple-element.62.refs_0_) | copy-start | bytes 1572868
  151.3 11.6 %copy-start.3 = (bf16[64,2048]{1,0:T(8,128)(2,1)S(1)}, bf16[64,2048]{1,0:T(8,128)(2,1)}, u32[]{:S(2)}) copy-start(bf16[64,2048]{1,0:T(8,128)(2,1)} %get-tuple-element.63) | copy-start | bytes 786436
  151.3 12.6 %copy-start.2 = (bf16[64,2048]{1,0:T(8,128)(2,1)S(1)}, bf16[64,2048]{1,0:T(8,128)(2,1)}, u32[]{:S(2)}) copy-start(bf16[64,2048]{1,0:T(8,128)(2,1)} %get-tuple-element.69) | copy-start | bytes 786436
  151.3 75.2 %all-to-all-start.1 = ((bf16[64,96,128]{2,1,0:T(8,128)(2,1)}), bf16[64,96,128]{2,1,0:T(8,128)(2,1)}, u32[]{:S(2)}, u32[]{:S(2)}) async-start(bf16[64,96,128]{2,1,0:T(8,128)(2,1)} %bitcast.16), calls=%async_computation.1 | async-start | bytes 3145728 | tf_op jit(solution)/shard_map/all_to_all | solution.py:853
  159.9 21.3 %collective-permute-start.12 = (bf16[128,2048]{1,0:T(8,128)(2,1)S(1)}, bf16[128,2048]{1,0:T(8,128)(2,1)}, u32[]{:S(2)}, u32[]{:S(2)}) collective-permute-start(bf16[128,2048]{1,0:T(8,128)(2,1)S(1)} %copy-done.1), channel_id=1, source_target_pairs={{0,2},{1,3},{2,0},{3,1},{4,6},{5,7},{6,4},{7,5},{8,10},{9,11},{10,... | collective-permute-start | bytes 1572872 | tf_op jit(solution)/shard_map/ppermute | solution.py:893
  162.9 18.3 %collective-permute-start.13 = (bf16[64,2048]{1,0:T(8,128)(2,1)S(1)}, bf16[64,2048]{1,0:T(8,128)(2,1)}, u32[]{:S(2)}, u32[]{:S(2)}) collective-permute-start(bf16[64,2048]{1,0:T(8,128)(2,1)S(1)} %copy-done.3), channel_id=1, source_target_pairs={{0,1},{1,2},{2,3},{3,0},{4,5},{5,6},{6,7},{7,4},{8,9},{9,10},{10,1... | collective-permute-start | bytes 786440 | tf_op jit(solution)/shard_map/ppermute | solution.py:894
  163.9 17.7 %collective-permute-start.14 = (bf16[64,2048]{1,0:T(8,128)(2,1)S(1)}, bf16[64,2048]{1,0:T(8,128)(2,1)}, u32[]{:S(2)}, u32[]{:S(2)}) collective-permute-start(bf16[64,2048]{1,0:T(8,128)(2,1)S(1)} %copy-done.2), channel_id=1, source_target_pairs={{0,3},{1,0},{2,1},{3,2},{4,7},{5,4},{6,5},{7,6},{8,11},{9,8},{10,9... | collective-permute-start | bytes 786440 | tf_op jit(solution)/shard_map/ppermute | solution.py:895
  185.5 26.3 %collective-permute-start.15 = (bf16[256,2048]{1,0:T(8,128)(2,1)}, bf16[256,2048]{1,0:T(8,128)(2,1)}, u32[]{:S(2)}, u32[]{:S(2)}) collective-permute-start(bf16[256,2048]{1,0:T(8,128)(2,1)} %get-tuple-element.70), channel_id=1, source_target_pairs={{0,1},{1,2},{2,3},{3,0},{4,5},{5,6},{6,7},{7,4},{8,9},{9,10},{10,1... | collective-permute-start | bytes 3145736 | tf_op jit(solution)/shard_map/ppermute | solution.py:902
  186.6 36.1 %collective-permute-start.16 = (bf16[256,2048]{1,0:T(8,128)(2,1)}, bf16[256,2048]{1,0:T(8,128)(2,1)}, u32[]{:S(2)}, u32[]{:S(2)}) collective-permute-start(bf16[256,2048]{1,0:T(8,128)(2,1)} %get-tuple-element.71), channel_id=1, source_target_pairs={{0,3},{1,0},{2,1},{3,2},{4,7},{5,4},{6,5},{7,6},{8,11},{9,8},{10,9... | collective-permute-start | bytes 3145736 | tf_op jit(solution)/shard_map/ppermute | solution.py:903
  192.8 33.8 %collective-permute-start.17 = (bf16[128,2048]{1,0:T(8,128)(2,1)}, bf16[128,2048]{1,0:T(8,128)(2,1)}, u32[]{:S(2)}, u32[]{:S(2)}) collective-permute-start(bf16[128,2048]{1,0:T(8,128)(2,1)} %shared_part.1), channel_id=1, source_target_pairs={{0,2},{1,3},{2,0},{3,1},{4,6},{5,7},{6,4},{7,5},{8,10},{9,11},{10,... | collective-permute-start | bytes 1572872 | tf_op jit(solution)/shard_map/ppermute | solution.py:906
